TPU v7x, 512 devices: a whole 4x8x8 slice. The times are simulated.
512 devices in a mesh: rep: 2 (over z_hi), fs: 32 (over z_lo, y), tp: 8 (over x, core).
Axes of the slice: x: 4, y: 8, z: 8 (z_hi: 2, z_lo: 4; z = z_hi * 4 + z_lo), core: 2. Of those that a mesh axis runs over, the one named last changes fastest.
Arguments:
- late_rows: bfloat16 [16384, 2048], P(('rep', 'fs')), parts along dimension 0, may hold values from -6 to 6
- early_rows: bfloat16 [16384, 2048], P(('rep', 'fs')), parts along dimension 0, may hold values from -6 to 6
- hidden_cot: bfloat16 [16384, 5632], P(('rep', 'fs'), 'tp'), parts along dimension 0, may hold values from -6 to 6
- gate_weight: bfloat16 [2048, 5632], P('fs', 'tp'), may hold values from -0.125 to 0.125
- up_weight: bfloat16 [2048, 5632], P('fs', 'tp'), may hold values from -0.125 to 0.125
- gate_taps: bfloat16 [3, 5632], P(None, 'tp'), may hold values from -3.5 to 3.5
- up_taps: bfloat16 [3, 5632], P(None, 'tp'), may hold values from -3.5 to 3.5
- gate_grad_sum: float32 [4096, 5632], P(('rep', 'fs'), 'tp'), parts along dimension 0, may hold values from -6 to 6
- up_grad_sum: float32 [4096, 5632], P(('rep', 'fs'), 'tp'), parts along dimension 0, may hold values from -6 to 6
- gate_taps_sum: float32 [6, 5632], P('rep', 'tp'), parts along dimension 0, may hold values from -6 to 6
- up_taps_sum: float32 [6, 5632], P('rep', 'tp'), parts along dimension 0, may hold values from -6 to 6
Outputs:
- late_hidden: bfloat16 [16384, 5632], P(('rep', 'fs'), 'tp'), parts along dimension 0
- early_grad: bfloat16 [16384, 2048], P(('rep', 'fs')), parts along dimension 0
- gate_grad_next: float32 [4096, 5632], P(('rep', 'fs'), 'tp'), parts along dimension 0
- up_grad_next: float32 [4096, 5632], P(('rep', 'fs'), 'tp'), parts along dimension 0
- gate_taps_next: float32 [6, 5632], P('rep', 'tp'), parts along dimension 0
- up_taps_next: float32 [6, 5632], P('rep', 'tp'), parts along dimension 0
There are 2 independent parts, one for each index of `rep`. A program takes and returns all parts, laid end to end along the dimension named above; an argument that names none is the same for every part. Nothing has to cross between parts.
All inputs are finite; a program needn't handle non-finite values.
Results may differ from a plain program's by a relative error of at most 0.02.
Values may be sent and summed in bfloat16 or wider, within the bound.
No kernel may reach another device: no remote copies, remote signals or barrier semaphores. Data moves between devices by JAX's collectives and lax.ppermute only.
A program may use at most 64 MiB of HBM per device.

v0:
```python
import jax
import jax.numpy as jnp
from jax import lax
from jax.sharding import Mesh
from jax.sharding import PartitionSpec as P

FS = ("fs_0", "fs_1")
REP_FS = ("rep", "fs_0", "fs_1")


contract_last = (((1,), (1,)), ((), ()))
contract_first = (((0,), (0,)), ((), ()))


def in_order(pieces, dim):
    pieces = jnp.moveaxis(pieces, 0, dim)
    dims = pieces.shape
    return pieces.reshape(*dims[:dim], dims[dim] * dims[dim + 1], *dims[dim + 2 :])


def all_blocks(array, axes, order):
    pieces = array
    for k in order:
        pieces = lax.all_gather(pieces, axes[k])
    done = order[::-1]
    back = [done.index(k) for k in range(len(axes))]
    pieces = pieces.transpose(*back, *range(len(axes), pieces.ndim))
    return pieces.reshape(-1, *array.shape)


def whole_of(array, axes, order, dim):
    return in_order(all_blocks(array, axes, order), dim)


def cut_along(array, dim, size):
    before, after = (array.shape[:dim], array.shape[dim + 1 :])
    return jnp.moveaxis(array.reshape(*before, size, -1, *after), dim, 0)


def sent_and_summed(array, axis, dim):
    size = lax.axis_size(axis)
    pieces = lax.all_to_all(cut_along(array, dim, size), axis, 0, 0, tiled=True)
    return jnp.sum(pieces.astype(jnp.float32), axis=0)


def copy_for_each(array, axis):
    size = lax.axis_size(axis)
    return lax.all_to_all(
        jnp.broadcast_to(array[None], (size, *array.shape)), axis, 0, 0, tiled=True
    )


def gathered_copies(array, axis, dim):
    pieces = copy_for_each(array, axis)
    return in_order(pieces, dim)


def reduced_to_own(pieces, axes, order):
    inside = pieces.shape[1:]
    pieces = pieces.reshape(*(lax.axis_size(a) for a in axes), *inside)
    pieces = jnp.moveaxis(pieces, order, range(len(axes))).reshape(-1, *inside)
    for k in order:
        pieces = lax.psum_scatter(pieces, axes[k], scatter_dimension=0, tiled=True)
    return pieces[0]


def summed_rows(array, axes, order, dim):
    size = lax.axis_size(axes)
    return reduced_to_own(cut_along(array, dim, size), axes, order)


def taken_together(array, axis):
    everything = copy_for_each(array, axis)
    return jnp.sum(everything, axis=0)


def in_one(arrays, axis):
    ends = [0]
    for a in arrays:
        ends.append(ends[-1] + a.size)
    subtotal = taken_together(jnp.concatenate([a.ravel() for a in arrays]), axis)
    return tuple((subtotal[b:e].reshape(a.shape) for a, b, e in zip(arrays, ends, ends[1:])))


def causal_mix(values, filter_taps):
    length = values.shape[-2]
    widths = [(0, 0)] * values.ndim
    widths[-2] = (2, 0)
    padded = jnp.pad(values, widths)
    return (
        filter_taps[0] * padded[..., 0:length, :]
        + filter_taps[1] * padded[..., 1 : length + 1, :]
        + filter_taps[2] * padded[..., 2 : length + 2, :]
    )


def mix_back(grads, filter_taps):
    length = grads.shape[-2]
    widths = [(0, 0)] * grads.ndim
    widths[-2] = (0, 2)
    padded = jnp.pad(grads, widths)
    return (
        filter_taps[2] * padded[..., 0:length, :]
        + filter_taps[1] * padded[..., 1 : length + 1, :]
        + filter_taps[0] * padded[..., 2 : length + 2, :]
    )


def tap_products(grads, values):
    length = values.shape[-2]
    widths = [(0, 0)] * values.ndim
    widths[-2] = (2, 0)
    padded = jnp.pad(values, widths)
    axes = tuple(range(values.ndim - 1))
    return jnp.stack(
        [
            jnp.sum(grads * padded[..., offset : offset + length, :], axis=axes)
            for offset in range(3)
        ]
    )


def stored(product):
    return lax.optimization_barrier(product.astype(jnp.bfloat16)).astype(jnp.float32)


def per_device(
    late_rows,
    early_rows,
    hidden_cot,
    gate_weight,
    up_weight,
    gate_taps,
    up_taps,
    gate_grad_sum,
    up_grad_sum,
    gate_taps_sum,
    up_taps_sum,
):
    row_count = late_rows.shape[0]
    width_local = gate_weight.shape[1]
    rows_scale = (row_count * lax.axis_size(FS)) ** (-0.5)
    gate_filter = gate_taps.astype(jnp.float32)
    up_filter = up_taps.astype(jnp.float32)
    joined_weight = jnp.concatenate([gate_weight, up_weight], axis=1)
    both_rows = jnp.concatenate([late_rows, early_rows], axis=0)
    whole_joined = whole_of(joined_weight, FS, (0, 1), 0)
    projected = jnp.dot(both_rows, whole_joined, preferred_element_type=jnp.float32)
    projected = stored(projected)
    late_gate = projected[:row_count, :width_local]
    late_up = projected[:row_count, width_local:]
    early_gate = projected[row_count:, :width_local]
    early_up = projected[row_count:, width_local:]
    late_hidden = (
        jax.nn.gelu(causal_mix(late_gate, gate_filter), approximate=True)
        * causal_mix(late_up, up_filter)
    ).astype(jnp.bfloat16)
    gate_mix = causal_mix(early_gate, gate_filter)
    up_mix = causal_mix(early_up, up_filter)
    cotangent = hidden_cot.astype(jnp.float32)
    activated, gelu_back = jax.vjp(
        lambda mixed_value: jax.nn.gelu(mixed_value, approximate=True), gate_mix
    )
    d_gate_mix = gelu_back(cotangent * up_mix)[0]
    d_up_mix = cotangent * activated
    d_gate_pre = mix_back(d_gate_mix, gate_filter).astype(jnp.bfloat16)
    d_up_pre = mix_back(d_up_mix, up_filter).astype(jnp.bfloat16)
    both_grads = jnp.concatenate([d_gate_pre, d_up_pre], axis=1)
    own_rows = sent_and_summed(
        lax.dot_general(
            both_grads, whole_joined, contract_last, preferred_element_type=jnp.float32
        ).astype(jnp.bfloat16),
        "tp",
        0,
    )
    early_grad = gathered_copies(own_rows.astype(jnp.bfloat16), "tp", 0)
    summed = summed_rows(
        (
            lax.dot_general(
                early_rows, both_grads, contract_first, preferred_element_type=jnp.float32
            )
            * rows_scale
        ).astype(jnp.bfloat16),
        FS,
        (1, 0),
        0,
    ).astype(jnp.float32)
    gate_tap_sums, up_tap_sums = in_one(
        (
            rows_scale * tap_products(d_gate_mix, early_gate),
            rows_scale * tap_products(d_up_mix, early_up),
        ),
        FS,
    )
    return (
        late_hidden,
        early_grad,
        gate_grad_sum + summed[:, :width_local],
        up_grad_sum + summed[:, width_local:],
        gate_taps_sum + gate_tap_sums,
        up_taps_sum + up_tap_sums,
    )


def solution(mesh):
    split = Mesh(
        mesh.devices.reshape(mesh.shape["rep"], 4, 8, mesh.shape["tp"]),
        ("rep", "fs_0", "fs_1", "tp"),
    )
    placed = (
        P(REP_FS, None),
        P(REP_FS, None),
        P(REP_FS, "tp"),
        P(FS, "tp"),
        P(FS, "tp"),
        P(None, "tp"),
        P(None, "tp"),
        P(REP_FS, "tp"),
        P(REP_FS, "tp"),
        P("rep", "tp"),
        P("rep", "tp"),
    )
    return jax.shard_map(
        per_device,
        mesh=split,
        in_specs=placed,
        out_specs=(
            P(REP_FS, "tp"),
            P(REP_FS, None),
            P(REP_FS, "tp"),
            P(REP_FS, "tp"),
            P("rep", "tp"),
            P("rep", "tp"),
        ),
        check_vma=False,
    )
```

profile of v0, /device:TPU:6, one launch (start us, length us, event | category | flops | bytes accessed | tf_op | source)
XLA Modules:
  0.0 258.7 jit_solution(8951374495315372138)
XLA Ops:
  7.2 1.0 pad_maximum_fusion.3
  8.3 21.9 %all-gather = bf16[256,1408]{1,0:T(8,128)(2,1)} all-gather(bf16[64,1408]{1,0:T(8,128)(2,1)S(1)} %pad_maximum_fusion.3), channel_id=2, replica_groups=mesh['rep'=2,'fs_0'=4,'fs_1'=8,'tp'=8] {'fs_0'}, dimensions={0}, use_global_device_ids=true | all-gather | bytes 901120 | tf_op jit(solution)/shard_map/all_gather | solution.py:24
  31.6 1.2 copy.39
  32.8 71.0 %all-gather.4.cloned.1.call-done = bf16[32,64,1408]{2,1,0:T(8,128)(2,1)} async-done(((bf16[4,64,1408]{2,1,0:T(8,128)(2,1)}), bf16[32,64,1408]{2,1,0:T(8,128)(2,1)}) %all-gather.4.cloned.1.call-update) | async-done | bytes 5767184 | tf_op jit(solution)/shard_map/all_gather | solution.py:24
  103.8 3.3 %copy.38 = bf16[4,8,64,1408]{3,2,1,0:T(8,128)(2,1)S(1)} copy(bf16[4,8,64,1408]{3,2,0,1:T(8,128)(2,1)} %bitcast.23) | data formatting | bytes 11534336 | tf_op jit(solution)/shard_map/transpose | solution.py:27
  107.1 3.4 %convolution_convert_fusion = bf16[512,1408]{1,0:T(8,128)(2,1)S(1)} fusion(bf16[2048,1408]{1,0:T(8,128)(2,1)S(1)} %bitcast.21, bf16[256,2048]{1,0:T(8,128)(2,1)S(1)} %copy-done.6, bf16[256,2048]{1,0:T(8,128)(2,1)S(1)} %copy-done.5), kind=kOutput, calls=%fused_computation.2 | convolution fusion | flops 2957705216 | bytes 9306112 | tf_op jit(solution)/shard_map/dot_general | solution.py:148
  111.2 1.8 multiply_reduce_fusion.5
  113.1 1.2 add_convert_fusion.1
  114.3 4.4 %fusion = bf16[2048,1408]{0,1:T(8,128)(2,1)} fusion(bf16[256,2048]{1,0:T(8,128)(2,1)S(1)} %copy-done.6, bf16[256,704]{1,0:T(8,128)(2,1)S(1)} %get-tuple-element.72, bf16[256,704]{1,0:T(8,128)(2,1)S(1)} %get-tuple-element.70), kind=kOutput, calls=%fused_computation.1 | convolution fusion | flops 1483603968 | bytes 7536640 | tf_op jit(solution)/shard_map/dot_general | solution.py:179
  118.7 8.4 %copy.40 = bf16[2048,1408]{1,0:T(8,128)(2,1)} copy(bf16[2048,1408]{0,1:T(8,128)(2,1)} %fusion) | data formatting | bytes 11534336 | tf_op jit(solution)/shard_map/convert_element_type | solution.py:183
  127.1 5.8 %copy.41 = bf16[8,4,64,1408]{3,2,1,0:T(8,128)(2,1)} copy(bf16[8,4,64,1408]{3,2,0,1:T(8,128)(2,1)} %bitcast.20) | data formatting | bytes 11534336 | tf_op jit(solution)/shard_map/transpose | solution.py:61
  132.8 5.4 %convolution_convert_fusion.1 = bf16[256,2048]{1,0:T(8,128)(2,1)} fusion(bf16[2048,1408]{1,0:T(8,128)(2,1)} %bitcast.22, bf16[256,704]{1,0:T(8,128)(2,1)S(1)} %get-tuple-element.72, bf16[256,704]{1,0:T(8,128)(2,1)S(1)} %get-tuple-element.70), kind=kOutput, calls=%fused_computation.3 | convolution fusion | flops 1478361088 | bytes 7536640 | tf_op jit(solution)/shard_map/dot_general | solution.py:170
  138.3 4.8 %all-to-all-start = ((bf16[8,32,2048]{2,1,0:T(8,128)(2,1)}), bf16[8,32,2048]{2,1,0:T(8,128)(2,1)S(1)}, u32[]{:S(2)}, u32[]{:S(2)}) async-start(bf16[8,32,2048]{2,1,0:T(8,128)(2,1)} %bitcast.4), calls=%async_computation | async-start | bytes 2097152 | tf_op jit(solution)/shard_map/all_to_all | solution.py:42
  143.4 13.5 %all-to-all-done = bf16[8,32,2048]{2,1,0:T(8,128)(2,1)S(1)} async-done(((bf16[8,32,2048]{2,1,0:T(8,128)(2,1)}), bf16[8,32,2048]{2,1,0:T(8,128)(2,1)S(1)}, u32[]{:S(2)}, u32[]{:S(2)}) %all-to-all-start) | async-done | bytes 1048608 | tf_op jit(solution)/shard_map/all_to_all | solution.py:42
  156.9 1.1 broadcast_in_dim.5
  158.0 8.2 %all-to-all-start.2 = ((f32[32,1,4224]{2,1,0:T(1,128)}), f32[32,1,4224]{2,1,0:T(1,128)S(1)}, u32[]{:S(2)}, u32[]{:S(2)}) async-start(f32[32,1,4224]{2,1,0:T(1,128)} %broadcast_in_dim.5), calls=%async_computation.4 | async-start | bytes 1081344 | tf_op jit(solution)/shard_map/all_to_all | solution.py:48
  166.3 49.8 %reduce-scatter.3.cloned.1.call-done = bf16[4,64,1408]{2,1,0:T(8,128)(2,1)} async-done(((bf16[32,64,1408]{2,1,0:T(8,128)(2,1)}), bf16[4,64,1408]{2,1,0:T(8,128)(2,1)}) %reduce-scatter.3.cloned.1.call-update) | async-done | bytes 720912 | tf_op jit(solution)/shard_map/reduce_scatter | solution.py:63
  216.3 1.1 broadcast_in_dim.4
  217.4 4.8 %all-to-all-start.1 = ((bf16[8,32,2048]{2,1,0:T(8,128)(2,1)}), bf16[8,32,2048]{2,1,0:T(8,128)(2,1)S(1)}, u32[]{:S(2)}, u32[]{:S(2)}) async-start(bf16[8,32,2048]{2,1,0:T(8,128)(2,1)} %broadcast_in_dim.4), calls=%async_computation.1 | async-start | bytes 2097152 | tf_op jit(solution)/shard_map/all_to_all | solution.py:48
  222.2 0.9 copy.43
  224.8 11.2 %all-to-all-done.1 = bf16[8,32,2048]{2,1,0:T(8,128)(2,1)S(1)} async-done(((bf16[8,32,2048]{2,1,0:T(8,128)(2,1)}), bf16[8,32,2048]{2,1,0:T(8,128)(2,1)S(1)}, u32[]{:S(2)}, u32[]{:S(2)}) %all-to-all-start.1) | async-done | bytes 1048608 | tf_op jit(solution)/shard_map/all_to_all | solution.py:48
  236.0 13.4 %reduce-scatter.5.cloned.1.call-done = bf16[1,64,1408]{2,1,0:T(8,128)(2,1)} async-done(((bf16[4,64,1408]{2,1,0:T(8,128)(2,1)}), bf16[1,64,1408]{2,1,0:T(8,128)(2,1)}) %reduce-scatter.5.cloned.1.call-update) | async-done | bytes 180240 | tf_op jit(solution)/shard_map/reduce_scatter | solution.py:63
  249.4 0.9 bitcast_convert_fusion
  251.2 1.0 copy.48
  (45 shorter events, 5.3 us)
Async XLA Ops:
  7.2 96.6 %all-gather.4.cloned.1.call-start = ((), (), s32[]{:S(2)}) async-start(), calls=%async_computation.7 | async-start | bytes 6488064 | tf_op jit(solution)/shard_map/all_gather | solution.py:24
  30.2 185.9 %reduce-scatter.3.cloned.1.call-start = ((), (), s32[]{:S(2)}) async-start(), calls=%async_computation.5 | async-start | bytes 6488064 | tf_op jit(solution)/shard_map/reduce_scatter | solution.py:63
  103.8 3.3 %copy-start.5 = (bf16[256,2048]{1,0:T(8,128)(2,1)S(1)}, bf16[256,2048]{1,0:T(8,128)(2,1)}, u32[]{:S(2)}) copy-start(bf16[256,2048]{1,0:T(8,128)(2,1)} %param.11) | copy-start | bytes 3145732
  103.8 3.3 %copy-start.6 = (bf16[256,2048]{1,0:T(8,128)(2,1)S(1)}, bf16[256,2048]{1,0:T(8,128)(2,1)}, u32[]{:S(2)}) copy-start(bf16[256,2048]{1,0:T(8,128)(2,1)} %param.12) | copy-start | bytes 3145732
  107.1 3.5 %copy-start = (bf16[4,8,64,1408]{3,2,1,0:T(8,128)(2,1)}, bf16[4,8,64,1408]{3,2,1,0:T(8,128)(2,1)S(1)}, u32[]{:S(2)}) copy-start(bf16[4,8,64,1408]{3,2,1,0:T(8,128)(2,1)S(1)} %copy.38) | copy-start | bytes 17301508
  138.3 18.7 %all-to-all-start = ((bf16[8,32,2048]{2,1,0:T(8,128)(2,1)}), bf16[8,32,2048]{2,1,0:T(8,128)(2,1)S(1)}, u32[]{:S(2)}, u32[]{:S(2)}) async-start(bf16[8,32,2048]{2,1,0:T(8,128)(2,1)} %bitcast.4), calls=%async_computation | async-start | bytes 2097152 | tf_op jit(solution)/shard_map/all_to_all | solution.py:42
  143.1 80.5 %copy-start.3 = (f32[3,704]{1,0:T(4,128)S(1)}, f32[3,704]{1,0:T(4,128)}, u32[]{:S(2)}) copy-start(f32[3,704]{1,0:T(4,128)} %param.21) | copy-start | bytes 25348
  143.2 81.0 %copy-start.4 = (f32[3,704]{1,0:T(4,128)S(1)}, f32[3,704]{1,0:T(4,128)}, u32[]{:S(2)}) copy-start(f32[3,704]{1,0:T(4,128)} %param.20) | copy-start | bytes 25348
  158.0 92.4 %copy-start.1 = (f32[64,704]{1,0:T(8,128)S(1)}, f32[64,704]{1,0:T(8,128)}, u32[]{:S(2)}) copy-start(f32[64,704]{1,0:T(8,128)} %param.19) | copy-start | bytes 540676
  158.0 92.4 %copy-start.2 = (f32[64,704]{1,0:T(8,128)S(1)}, f32[64,704]{1,0:T(8,128)}, u32[]{:S(2)}) copy-start(f32[64,704]{1,0:T(8,128)} %param.18) | copy-start | bytes 540676
  158.0 58.3 %all-to-all-start.2 = ((f32[32,1,4224]{2,1,0:T(1,128)}), f32[32,1,4224]{2,1,0:T(1,128)S(1)}, u32[]{:S(2)}, u32[]{:S(2)}) async-start(f32[32,1,4224]{2,1,0:T(1,128)} %broadcast_in_dim.5), calls=%async_computation.4 | async-start | bytes 1081344 | tf_op jit(solution)/shard_map/all_to_all | solution.py:48
  166.2 83.2 %reduce-scatter.5.cloned.1.call-start = ((), (), s32[]{:S(2)}) async-start(), calls=%async_computation.6 | async-start | bytes 901120 | tf_op jit(solution)/shard_map/reduce_scatter | solution.py:63
  217.4 18.7 %all-to-all-start.1 = ((bf16[8,32,2048]{2,1,0:T(8,128)(2,1)}), bf16[8,32,2048]{2,1,0:T(8,128)(2,1)S(1)}, u32[]{:S(2)}, u32[]{:S(2)}) async-start(bf16[8,32,2048]{2,1,0:T(8,128)(2,1)} %broadcast_in_dim.4), calls=%async_computation.1 | async-start | bytes 2097152 | tf_op jit(solution)/shard_map/all_to_all | solution.py:48
Sparse Core Ops, SparseCore 0:
  30.3 73.4 all-gather.3
  133.0 83.0 reduce-scatter.2
  218.9 30.4 reduce-scatter.4
where the time goes:
time: 259 us
  waiting for transfers between devices  159 us (61%)
  local copies, waits for them, and re-layouts  23.5 us (9%)
  blocking collectives  21.9 us (8%)
  starting transfers between devices  17.9 us (7%)
  between operations  13.9 us (5%)
  matrix products  13.3 us (5%)
  other arithmetic  9.24 us (4%)
    all_gather x1, waiting for transfers between devices, all_blocks(): pieces = lax.all_gather(pieces, axes[k])  71 us
    reduce_scatter x2, waiting for transfers between devices, reduced_to_own(): pieces = lax.psum_scatter(pieces, axes[k], scatter_dimension=0, tiled=True)  63.2 us
    all_gather x1, blocking collectives, all_blocks(): pieces = lax.all_gather(pieces, axes[k])  21.9 us
    all_to_all x1, waiting for transfers between devices, sent_and_summed(): pieces = lax.all_to_all(cut_along(array, dim, size), axis, 0, 0, tiled=True)  13.5 us
    all_to_all x2, starting transfers between devices, copy_for_each(): lax.all_to_all(jnp.broadcast_to(array[None], (size, *array.shape)), axis,...  13 us
    all_to_all x2, waiting for transfers between devices, copy_for_each(): lax.all_to_all(jnp.broadcast_to(array[None], (size, *array.shape)), axis,...  11.2 us
    convert_element_type x1, local copies, waits for them, and re-layouts, per_device(): summed = summed_rows((lax.dot_general(early_rows, both_grads, contract_fi...  8.36 us
    transpose x1, local copies, waits for them, and re-layouts, reduced_to_own(): pieces = jnp.moveaxis(pieces, order, range(len(axes))).reshape(-1, *inside)  5.75 us
  transfers between devices with their start and end apart: 6, of which 5 were waited for; matrix products, arithmetic and copies ran while one was open for 5% of the time, Pallas kernels for 0%

commit v1 on v0

v1 whole, which is shorter than its diff:
```python
import jax
import jax.numpy as jnp
from jax import lax
from jax.sharding import Mesh
from jax.sharding import PartitionSpec as P

Z_ALL = ("rep", "zp", "zb")
FS = ("zp", "zb", "y")
REP_FS = ("rep", "zp", "zb", "y")
TP = ("x", "c")

contract_last = (((1,), (1,)), ((), ()))
contract_first = (((0,), (0,)), ((), ()))


def shifted(values, axis, by):
    size = lax.axis_size(axis)
    return lax.ppermute(values, axis, [(k, (k + by) % size) for k in range(size)])


def swapped(values, axis):
    return lax.ppermute(values, axis, [(0, 1), (1, 0)])


def pick(flag, first, second):
    return jnp.where(flag, first, second)


def causal_mix(values, filter_taps):
    length = values.shape[-2]
    widths = [(0, 0)] * values.ndim
    widths[-2] = (2, 0)
    padded = jnp.pad(values, widths)
    return (
        filter_taps[0] * padded[..., 0:length, :]
        + filter_taps[1] * padded[..., 1 : length + 1, :]
        + filter_taps[2] * padded[..., 2 : length + 2, :]
    )


def mix_back(grads, filter_taps):
    length = grads.shape[-2]
    widths = [(0, 0)] * grads.ndim
    widths[-2] = (0, 2)
    padded = jnp.pad(grads, widths)
    return (
        filter_taps[2] * padded[..., 0:length, :]
        + filter_taps[1] * padded[..., 1 : length + 1, :]
        + filter_taps[0] * padded[..., 2 : length + 2, :]
    )


def tap_products(grads, values):
    length = values.shape[-2]
    widths = [(0, 0)] * values.ndim
    widths[-2] = (2, 0)
    padded = jnp.pad(values, widths)
    axes = tuple(range(values.ndim - 1))
    return jnp.stack(
        [
            jnp.sum(grads * padded[..., offset : offset + length, :], axis=axes)
            for offset in range(3)
        ]
    )


def stored(product):
    return lax.optimization_barrier(product.astype(jnp.bfloat16)).astype(jnp.float32)


def rolled(blocks, by):
    size = blocks.shape[0]
    twice = jnp.concatenate([blocks, blocks], axis=0)
    return lax.dynamic_slice_in_dim(twice, (size - by) % size, size, 0)


def gathered_ring(block, axis):
    size = lax.axis_size(axis)
    half = size // 2
    cut = block.shape[0] // 2
    from_below, from_above = [block], [block]
    for step in range(1, half):
        from_below.append(shifted(from_below[-1], axis, 1))
        from_above.append(shifted(from_above[-1], axis, -1))
    far = jnp.concatenate(
        [shifted(from_below[-1][:cut], axis, 1), shifted(from_above[-1][cut:], axis, -1)]
    )
    return jnp.stack(from_above + [far] + from_below[:0:-1])


def summed_ring(block_of, axis):
    size = lax.axis_size(axis)
    half = size // 2
    far = block_of(half)
    cut = far.shape[0] // 2
    up = shifted(far[:cut], axis, 1)
    down = shifted(far[cut:], axis, -1)
    for step in range(half - 1, 0, -1):
        above, below = block_of(step), block_of(-step)
        if step == half - 1:
            above = jnp.concatenate([above[:cut] + up, above[cut:]])
            below = jnp.concatenate([below[:cut], below[cut:] + down])
        else:
            above = above + up
            below = below + down
        up = shifted(above, axis, 1)
        down = shifted(below, axis, -1)
    wide = jnp.float32
    return block_of(0).astype(wide) + up.astype(wide) + down.astype(wide)


def per_device(
    late_rows,
    early_rows,
    hidden_cot,
    gate_weight,
    up_weight,
    gate_taps,
    up_taps,
    gate_grad_sum,
    up_grad_sum,
    gate_taps_sum,
    up_taps_sum,
):
    row_count, depth = late_rows.shape
    shard_rows, width_local = gate_weight.shape
    width = width_local // 2
    n_z = lax.axis_size("zp") * lax.axis_size("zb")
    n_y = lax.axis_size("y")
    n_x = lax.axis_size("x")
    zb = lax.axis_index("zb")
    z = lax.axis_index("zp") * 2 + zb
    y = lax.axis_index("y")
    first_z = zb == 0
    first_c = lax.axis_index("c") == 0
    rows_scale = (row_count * n_z * n_y) ** (-0.5)

    def halves(array):
        low, high = array[..., :width], array[..., width:]
        return pick(first_z, low, high), pick(first_z, high, low)

    def columns_joined(mine, other):
        return pick(
            first_z,
            jnp.concatenate([mine, other], axis=-1),
            jnp.concatenate([other, mine], axis=-1),
        )

    def partner_rows(rows):
        cut = row_count // 2
        sent = pick(first_c, rows[:cut], rows[cut:])
        here = swapped(sent, "zb")
        there = swapped(here, "c")
        return jnp.concatenate([pick(first_c, here, there), pick(first_c, there, here)])

    gate_mine, gate_other = halves(gate_weight)
    up_mine, up_other = halves(up_weight)
    weight_mine = jnp.concatenate([gate_mine, up_mine], axis=1)
    weight_other = jnp.concatenate([gate_other, up_other], axis=1)
    next_one = shifted(weight_other, Z_ALL, -1)
    previous_one = shifted(weight_other, Z_ALL, 1)
    opposite = shifted(weight_mine, Z_ALL, -2)
    block = rolled(jnp.stack([weight_mine, next_one, opposite, previous_one]), z)
    early_pair = jnp.concatenate([early_rows, partner_rows(early_rows)])
    cot_mine, cot_other = halves(hidden_cot)
    cotangent = jnp.stack([cot_mine, swapped(cot_other, "zb")]).astype(jnp.float32)
    late_pair = jnp.concatenate([late_rows, partner_rows(late_rows)])
    gate_filter = halves(gate_taps)[0].astype(jnp.float32)
    up_filter = halves(up_taps)[0].astype(jnp.float32)

    weight = rolled(gathered_ring(block, "y"), y)
    weight = weight.transpose(1, 0, 2, 3).reshape(depth, 2 * width)

    def project(rows):
        product = stored(jnp.dot(rows, weight, preferred_element_type=jnp.float32))
        product = product.reshape(2, row_count, 2 * width)
        return product[..., :width], product[..., width:]

    early_gate, early_up = project(early_pair)
    gate_mix = causal_mix(early_gate, gate_filter)
    up_mix = causal_mix(early_up, up_filter)
    activated, gelu_back = jax.vjp(
        lambda mixed_value: jax.nn.gelu(mixed_value, approximate=True), gate_mix
    )
    d_gate_mix = gelu_back(cotangent * up_mix)[0]
    d_up_mix = cotangent * activated
    d_gate_pre = mix_back(d_gate_mix, gate_filter).astype(jnp.bfloat16)
    d_up_pre = mix_back(d_up_mix, up_filter).astype(jnp.bfloat16)
    both_grads = jnp.concatenate([d_gate_pre, d_up_pre], axis=-1)
    both_grads = both_grads.reshape(2 * row_count, 2 * width)

    terms = (
        lax.dot_general(
            early_pair, both_grads, contract_first, preferred_element_type=jnp.float32
        )
        * rows_scale
    ).astype(jnp.bfloat16)
    terms = terms.reshape(n_z, n_y, shard_rows, 2 * width)

    def terms_for(offset):
        at = (y + offset + n_y) % n_y
        return lax.dynamic_index_in_dim(terms, at, 1, keepdims=False)

    reduced = summed_ring(terms_for, "y").astype(jnp.bfloat16)
    pieces = lax.all_to_all(reduced, ("zp", "zb"), 0, 0, tiled=True)
    pieces = pieces.reshape(2, 2, shard_rows, 2 * width).astype(jnp.float32)
    pieces = jnp.sum(pieces, axis=0)
    gate_sum = jnp.concatenate([pieces[0, :, :width], pieces[1, :, :width]], axis=1)
    up_sum = jnp.concatenate([pieces[0, :, width:], pieces[1, :, width:]], axis=1)

    partial = lax.dot_general(
        both_grads, weight, contract_last, preferred_element_type=jnp.float32
    )
    cut = depth // 2
    kept = pick(first_c, partial[:, :cut], partial[:, cut:])
    given = pick(first_c, partial[:, cut:], partial[:, :cut]).astype(jnp.bfloat16)
    chip = (kept + swapped(given, "c").astype(jnp.float32)).astype(jnp.bfloat16)
    chip = chip.reshape(2, n_x, row_count // n_x, cut)
    chip = jnp.stack([pick(first_z, chip[0], chip[1]), pick(first_z, chip[1], chip[0])])
    spread = lax.all_to_all(
        chip.reshape(2 * n_x, row_count // n_x, cut), ("zb", "x"), 0, 0, tiled=True
    )
    own = jnp.sum(spread.astype(jnp.float32), axis=0).astype(jnp.bfloat16)
    copies = jnp.broadcast_to(own[None], (2 * n_x, *own.shape))
    finished = lax.all_to_all(copies, TP, 0, 0, tiled=True)
    finished = finished.reshape(n_x, 2, row_count // n_x, cut)
    early_grad = finished.transpose(0, 2, 1, 3).reshape(row_count, depth)

    taps = rows_scale * jnp.concatenate(
        [tap_products(d_gate_mix, early_gate), tap_products(d_up_mix, early_up)], axis=0
    )
    n_fs = n_z * n_y
    all_taps = lax.all_to_all(
        jnp.broadcast_to(taps.reshape(1, -1), (n_fs, taps.size)), FS, 0, 0, tiled=True
    )
    all_taps = jnp.sum(all_taps.reshape(n_z // 2, 2, n_y, taps.size), axis=(0, 2))
    all_taps = all_taps.reshape(2, 6, width).transpose(1, 0, 2).reshape(6, width_local)

    late_gate, late_up = project(late_pair)
    late = (
        jax.nn.gelu(causal_mix(late_gate, gate_filter), approximate=True)
        * causal_mix(late_up, up_filter)
    ).astype(jnp.bfloat16)
    late_hidden = columns_joined(late[0], swapped(late[1], "zb"))
    return (
        late_hidden,
        early_grad,
        gate_grad_sum + gate_sum,
        up_grad_sum + up_sum,
        gate_taps_sum + all_taps[:3],
        up_taps_sum + all_taps[3:],
    )


def solution(mesh):
    split = Mesh(
        mesh.devices.reshape(mesh.shape["rep"], 2, 2, 8, 4, 2),
        ("rep", "zp", "zb", "y", "x", "c"),
    )
    placed = (
        P(REP_FS, None),
        P(REP_FS, None),
        P(REP_FS, TP),
        P(FS, TP),
        P(FS, TP),
        P(None, TP),
        P(None, TP),
        P(REP_FS, TP),
        P(REP_FS, TP),
        P("rep", TP),
        P("rep", TP),
    )
    return jax.shard_map(
        per_device,
        mesh=split,
        in_specs=placed,
        out_specs=(
            P(REP_FS, TP),
            P(REP_FS, None),
            P(REP_FS, TP),
            P(REP_FS, TP),
            P("rep", TP),
            P("rep", TP),
        ),
        check_vma=False,
    )
```

time: 259 us -> 249 us (0.961); the launches traced: 259 us -> 245 us
  waiting for transfers between devices: 159 us -> 46 us
  starting transfers between devices: 17.9 us -> 115 us
  other arithmetic: 9.24 us -> 37.6 us
  blocking collectives: 21.9 us -> 0 us
  between operations: 13.9 us -> 1.6 us
  local copies, waits for them, and re-layouts: 23.5 us -> 35.2 us
  matrix products: 13.3 us -> 9.41 us
    ppermute x0 -> x26, starting transfers between devices: none -> 94.7 us  [the longest x19 74.5 us: shifted(): lax.ppermute(values, axis, [(k, (k + by) % size) for k in range(size)])]
    all_gather x1 -> x0, waiting for transfers between devices: 71 us -> none  [all_blocks(): pieces = lax.all_gather(pieces, axes[k])]
    reduce_scatter x2 -> x0, waiting for transfers between devices: 63.2 us -> none  [reduced_to_own(): pieces = lax.psum_scatter(pieces, axes[k], scatter_dimension=0, tiled=True)]
    ppermute x0 -> x26, waiting for transfers between devices: none -> 35.3 us  [the longest x19 29.1 us: shifted(): lax.ppermute(values, axis, [(k, (k + by) % size) for k in range(size)])]
    all_gather x1 -> x0, blocking collectives: 21.9 us -> none  [all_blocks(): pieces = lax.all_gather(pieces, axes[k])]
    unnamed x17 -> x62, local copies, waits for them, and re-layouts: 3.06 us -> 18 us
    all_to_all x3 -> x4, waiting for transfers between devices: 24.7 us -> 10.7 us  [the longest x1 10.7 us: per_device(): finished = lax.all_to_all(copies, TP, 0, 0, tiled=True)]
    select_n x0 -> x7, other arithmetic: none -> 9.65 us  [pick(): return jnp.where(flag, first, second)]
  transfers between devices with their start and end apart: 6 -> 30, of which waited for: 5 -> 12; matrix products, arithmetic and copies ran while one was open for 5% -> 26% of each run, Pallas kernels for 0% -> 0%
where the time goes in v1:
time: 249 us; the launch traced here: 245 us
  starting transfers between devices  115 us (46%)
  waiting for transfers between devices  46 us (18%)
  other arithmetic  37.6 us (15%)
  local copies, waits for them, and re-layouts  35.2 us (14%)
  matrix products  9.41 us (4%)
    ppermute x19, starting transfers between devices, shifted(): lax.ppermute(values, axis, [(k, (k + by) % size) for k in range(size)])  74.5 us
    ppermute x19, waiting for transfers between devices, shifted(): lax.ppermute(values, axis, [(k, (k + by) % size) for k in range(size)])  29.1 us
    ppermute x7, starting transfers between devices, swapped(): return lax.ppermute(values, axis, [(0, 1), (1, 0)])  20.2 us
    unnamed x62, local copies, waits for them, and re-layouts  18 us
    all_to_all x1, waiting for transfers between devices, per_device(): finished = lax.all_to_all(copies, TP, 0, 0, tiled=True)  10.7 us
    select_n x7, other arithmetic, pick(): return jnp.where(flag, first, second)  9.65 us
    ppermute x7, waiting for transfers between devices, swapped(): return lax.ppermute(values, axis, [(0, 1), (1, 0)])  6.21 us
    all_to_all x1, starting transfers between devices, per_device(): lax.all_to_all(chip.reshape(2 * n_x, row_count // n_x, cut), ('zb', 'x'),...  5.41 us
  transfers between devices with their start and end apart: 30, of which 12 were waited for; matrix products, arithmetic and copies ran while one was open for 26% of the time, Pallas kernels for 0%

profile of v1, /device:TPU:6, one launch (start us, length us, event | category | flops | bytes accessed | tf_op | source)
XLA Modules:
  0.0 244.7 jit_solution(6275405309461053284)
XLA Ops:
  1.8 10.9 %collective-permute-start.2 = (bf16[64,704]{1,0:T(8,128)(2,1)S(1)}, bf16[64,704]{1,0:T(8,128)(2,1)S(1)}, u32[]{:S(2)}, u32[]{:S(2)}) collective-permute-start(bf16[64,704]{1,0:T(8,128)(2,1)S(1)} %pad_maximum_fusion.8), channel_id=1, source_target_pairs={{0,448},{64,0},{128,64},{192,128},{256,192},{320,256},{384,320},{4... | collective-permute-start | bytes 270344 | tf_op jit(solution)/shard_map/ppermute | solution.py:18
  14.8 3.9 %collective-permute-start.3 = (bf16[64,704]{1,0:T(8,128)(2,1)S(1)}, bf16[64,704]{1,0:T(8,128)(2,1)S(1)}, u32[]{:S(2)}, u32[]{:S(2)}) collective-permute-start(bf16[64,704]{1,0:T(8,128)(2,1)S(1)} %pad_maximum_fusion.7), channel_id=1, source_target_pairs={{0,384},{64,448},{128,0},{192,64},{256,128},{320,192},{384,256},{4... | collective-permute-start | bytes 270344 | tf_op jit(solution)/shard_map/ppermute | solution.py:18
  20.7 4.6 %collective-permute-start.15 = (bf16[128,2048]{1,0:T(8,128)(2,1)}, bf16[128,2048]{1,0:T(8,128)(2,1)S(1)}, u32[]{:S(2)}, u32[]{:S(2)}) collective-permute-start(bf16[128,2048]{1,0:T(8,128)(2,1)} %slice_select_fusion), channel_id=1, source_target_pairs={{0,64},{64,0},{1,65},{65,1},{2,66},{66,2},{3,67},{67,3},{4,68},{68... | collective-permute-start | bytes 1572872 | tf_op jit(solution)/shard_map/ppermute | solution.py:22
  29.5 5.4 %collective-permute-start.5 = (bf16[4,64,704]{2,1,0:T(8,128)(2,1)S(1)}, bf16[4,64,704]{2,1,0:T(8,128)(2,1)S(1)}, u32[]{:S(2)}, u32[]{:S(2)}) collective-permute-start(bf16[4,64,704]{2,1,0:T(8,128)(2,1)S(1)} %get-tuple-element.22), channel_id=1, source_target_pairs={{0,56},{8,0},{16,8},{24,16},{32,24},{40,32},{48,40},{56,48},{1,57}... | collective-permute-start | bytes 1081352 | tf_op jit(solution)/shard_map/ppermute | solution.py:18
  36.9 3.9 %collective-permute-start = (bf16[128,2048]{1,0:T(8,128)(2,1)}, bf16[128,2048]{1,0:T(8,128)(2,1)}, u32[]{:S(2)}, u32[]{:S(2)}) collective-permute-start(bf16[128,2048]{1,0:T(8,128)(2,1)} %slice_select_fusion.1), channel_id=1, source_target_pairs={{0,64},{64,0},{1,65},{65,1},{2,66},{66,2},{3,67},{67,3},{4,68},{68... | collective-permute-start | bytes 1572872 | tf_op jit(solution)/shard_map/ppermute | solution.py:22
  42.9 5.1 %collective-permute-start.6 = (bf16[4,64,704]{2,1,0:T(8,128)(2,1)S(1)}, bf16[4,64,704]{2,1,0:T(8,128)(2,1)S(1)}, u32[]{:S(2)}, u32[]{:S(2)}) collective-permute-start(bf16[4,64,704]{2,1,0:T(8,128)(2,1)S(1)} %collective-permute-done.5), channel_id=1, source_target_pairs={{0,56},{8,0},{16,8},{24,16},{32,24},{40,32},{48,40},{56,48},{1,57}... | collective-permute-start | bytes 1081352 | tf_op jit(solution)/shard_map/ppermute | solution.py:18
  57.4 5.1 %collective-permute-start.7 = (bf16[4,64,704]{2,1,0:T(8,128)(2,1)S(1)}, bf16[4,64,704]{2,1,0:T(8,128)(2,1)S(1)}, u32[]{:S(2)}, u32[]{:S(2)}) collective-permute-start(bf16[4,64,704]{2,1,0:T(8,128)(2,1)S(1)} %collective-permute-done.6), channel_id=1, source_target_pairs={{0,56},{8,0},{16,8},{24,16},{32,24},{40,32},{48,40},{56,48},{1,57}... | collective-permute-start | bytes 1081352 | tf_op jit(solution)/shard_map/ppermute | solution.py:18
  70.2 7.5 %collective-permute-done.10 = bf16[4,64,704]{2,1,0:T(8,128)(2,1)S(1)} collective-permute-done((bf16[4,64,704]{2,1,0:T(8,128)(2,1)S(1)}, bf16[4,64,704]{2,1,0:T(8,128)(2,1)S(1)}, u32[]{:S(2)}, u32[]{:S(2)}) %collective-permute-start.10) | collective-permute-done | bytes 360480 | tf_op jit(solution)/shard_map/ppermute | solution.py:18
  79.7 5.1 %collective-permute-start.12 = (bf16[2,64,704]{2,1,0:T(8,128)(2,1)S(1)}, bf16[2,64,704]{2,1,0:T(8,128)(2,1)S(1)}, u32[]{:S(2)}, u32[]{:S(2)}) collective-permute-start(bf16[2,64,704]{2,1,0:T(8,128)(2,1)S(1)} %slice.288), channel_id=1, source_target_pairs={{0,56},{8,0},{16,8},{24,16},{32,24},{40,32},{48,40},{56,48},{1,57}... | collective-permute-start | bytes 540680 | tf_op jit(solution)/shard_map/ppermute | solution.py:18
  125.6 3.3 %multiply_convert_fusion = bf16[2048,704]{0,1:T(8,128)(2,1)} fusion(bf16[512,704]{0,1:T(8,128)(2,1)S(1)} %bitcast.141, bf16[128,2048]{1,0:T(8,128)(2,1)S(1)} %copy-done.10, bf16[128,2048]{1,0:T(8,128)(2,1)S(1)} %copy-done.8, bf16[256,2048]{1,0:T(8,128)(2,1)S(1)} %copy-done.6), kind=kOutput, calls=%fused_computation | convolution fusion | flops 1485570048 | bytes 5701632 | tf_op jit(solution)/shard_map/dot_general | solution.py:193
  134.9 5.6 %collective-permute-start.22 = (bf16[2,64,704]{2,1,0:T(8,128)(2,1)}, bf16[2,64,704]{2,1,0:T(8,128)(2,1)}, u32[]{:S(2)}, u32[]{:S(2)}) collective-permute-start(bf16[2,64,704]{2,1,0:T(8,128)(2,1)} %get-tuple-element.32), channel_id=1, source_target_pairs={{0,56},{8,0},{16,8},{24,16},{32,24},{40,32},{48,40},{56,48},{1,57}... | collective-permute-start | bytes 540680 | tf_op jit(solution)/shard_map/ppermute | solution.py:18
  141.5 4.6 %all-to-all-start.3 = ((f32[32,1,2112]{2,1,0:T(1,128)}), f32[32,1,2112]{2,1,0:T(1,128)}, u32[]{:S(2)}, u32[]{:S(2)}) async-start(f32[32,1,2112]{2,1,0:T(1,128)} %broadcast_in_dim.5), calls=%async_computation.3 | async-start | bytes 557056 | tf_op jit(solution)/shard_map/all_to_all | solution.py:233
  148.9 5.1 %collective-permute-start.23 = (bf16[4,64,704]{2,1,0:T(8,128)(2,1)}, bf16[4,64,704]{2,1,0:T(8,128)(2,1)}, u32[]{:S(2)}, u32[]{:S(2)}) collective-permute-start(bf16[4,64,704]{2,1,0:T(8,128)(2,1)} %pad_maximum_fusion.5), channel_id=1, source_target_pairs={{0,56},{8,0},{16,8},{24,16},{32,24},{40,32},{48,40},{56,48},{1,57}... | collective-permute-start | bytes 1081352 | tf_op jit(solution)/shard_map/ppermute | solution.py:18
  157.7 3.1 %add_convert_fusion = bf16[512,1024]{1,0:T(8,128)(2,1)S(1)} fusion(bf16[512,1024]{1,0:T(8,128)(2,1)} %collective-permute-done.17, f32[512,2048]{1,0:T(8,128)} %copy-done, pred[]{:T(512)S(6)} %eq.18), kind=kLoop, calls=%fused_computation.9 | loop fusion | flops 2097152 | bytes 6291457 | tf_op jit(solution)/shard_map/convert_element_type | solution.py:217
  162.0 5.4 %all-to-all-start = ((bf16[8,64,1024]{2,1,0:T(8,128)(2,1)}), bf16[8,64,1024]{2,1,0:T(8,128)(2,1)}, u32[]{:S(2)}, u32[]{:S(2)}) async-start(bf16[8,64,1024]{2,1,0:T(8,128)(2,1)} %bitcast.127), calls=%async_computation | async-start | bytes 2097152 | tf_op jit(solution)/shard_map/all_to_all | solution.py:220
  173.5 5.1 %collective-permute-start.24 = (bf16[4,64,704]{2,1,0:T(8,128)(2,1)}, bf16[4,64,704]{2,1,0:T(8,128)(2,1)}, u32[]{:S(2)}, u32[]{:S(2)}) collective-permute-start(bf16[4,64,704]{2,1,0:T(8,128)(2,1)} %get-tuple-element.26), channel_id=1, source_target_pairs={{0,56},{8,0},{16,8},{24,16},{32,24},{40,32},{48,40},{56,48},{1,57}... | collective-permute-start | bytes 1081352 | tf_op jit(solution)/shard_map/ppermute | solution.py:18
  178.7 5.8 %collective-permute-done.20 = bf16[4,64,704]{2,1,0:T(8,128)(2,1)} collective-permute-done((bf16[4,64,704]{2,1,0:T(8,128)(2,1)}, bf16[4,64,704]{2,1,0:T(8,128)(2,1)}, u32[]{:S(2)}, u32[]{:S(2)}) %collective-permute-start.20) | collective-permute-done | bytes 360480 | tf_op jit(solution)/shard_map/ppermute | solution.py:18
  190.3 5.3 %collective-permute-start.25 = (bf16[4,64,704]{2,1,0:T(8,128)(2,1)}, bf16[4,64,704]{2,1,0:T(8,128)(2,1)}, u32[]{:S(2)}, u32[]{:S(2)}) collective-permute-start(bf16[4,64,704]{2,1,0:T(8,128)(2,1)} %get-tuple-element.24), channel_id=1, source_target_pairs={{0,56},{8,0},{16,8},{24,16},{32,24},{40,32},{48,40},{56,48},{1,57}... | collective-permute-start | bytes 1081352 | tf_op jit(solution)/shard_map/ppermute | solution.py:18
  195.5 4.8 %collective-permute-done.21 = bf16[4,64,704]{2,1,0:T(8,128)(2,1)} collective-permute-done((bf16[4,64,704]{2,1,0:T(8,128)(2,1)}, bf16[4,64,704]{2,1,0:T(8,128)(2,1)}, u32[]{:S(2)}, u32[]{:S(2)}) %collective-permute-start.21) | collective-permute-done | bytes 360480 | tf_op jit(solution)/shard_map/ppermute | solution.py:18
  203.5 5.4 %all-to-all-start.2 = ((bf16[4,64,704]{2,1,0:T(8,128)(2,1)}), bf16[4,64,704]{2,1,0:T(8,128)(2,1)S(1)}, u32[]{:S(2)}, u32[]{:S(2)}) async-start(bf16[4,64,704]{2,1,0:T(8,128)(2,1)} %fusion.10), calls=%async_computation.2 | async-start | bytes 786432 | tf_op jit(solution)/shard_map/all_to_all | solution.py:205
  208.9 4.1 %collective-permute-start.13 = (bf16[256,352]{0,1:T(8,128)(2,1)S(1)}, bf16[256,352]{0,1:T(8,128)(2,1)S(1)}, u32[]{:S(2)}, u32[]{:S(2)}) collective-permute-start(bf16[256,352]{0,1:T(8,128)(2,1)S(1)} %get-tuple-element.50), channel_id=1, source_target_pairs={{0,64},{64,0},{1,65},{65,1},{2,66},{66,2},{3,67},{67,3},{4,68},{68... | collective-permute-start | bytes 540680 | tf_op jit(solution)/shard_map/ppermute | solution.py:22
  213.0 6.2 %collective-permute-done.13 = bf16[256,352]{0,1:T(8,128)(2,1)S(1)} collective-permute-done((bf16[256,352]{0,1:T(8,128)(2,1)S(1)}, bf16[256,352]{0,1:T(8,128)(2,1)S(1)}, u32[]{:S(2)}, u32[]{:S(2)}) %collective-permute-start.13) | collective-permute-done | bytes 180256 | tf_op jit(solution)/shard_map/ppermute | solution.py:22
  223.7 4.8 %all-to-all-start.1 = ((bf16[8,64,1024]{2,1,0:T(8,128)(2,1)}), bf16[8,64,1024]{2,1,0:T(8,128)(2,1)S(1)}, u32[]{:S(2)}, u32[]{:S(2)}) async-start(bf16[8,64,1024]{2,1,0:T(8,128)(2,1)} %broadcast_in_dim.4), calls=%async_computation.1 | async-start | bytes 2097152 | tf_op jit(solution)/shard_map/all_to_all | solution.py:225
  231.7 10.7 %all-to-all-done.1 = bf16[8,64,1024]{2,1,0:T(8,128)(2,1)S(1)} async-done(((bf16[8,64,1024]{2,1,0:T(8,128)(2,1)}), bf16[8,64,1024]{2,1,0:T(8,128)(2,1)S(1)}, u32[]{:S(2)}, u32[]{:S(2)}) %all-to-all-start.1) | async-done | bytes 1048608 | tf_op jit(solution)/shard_map/all_to_all | solution.py:225
  (172 shorter events, 112.2 us)
Async XLA Ops:
  1.8 26.6 %collective-permute-start.2 = (bf16[64,704]{1,0:T(8,128)(2,1)S(1)}, bf16[64,704]{1,0:T(8,128)(2,1)S(1)}, u32[]{:S(2)}, u32[]{:S(2)}) collective-permute-start(bf16[64,704]{1,0:T(8,128)(2,1)S(1)} %pad_maximum_fusion.8), channel_id=1, source_target_pairs={{0,448},{64,0},{128,64},{192,128},{256,192},{320,256},{384,320},{4... | collective-permute-start | bytes 270344 | tf_op jit(solution)/shard_map/ppermute | solution.py:18
  12.7 15.7 %collective-permute-start.4 = (bf16[64,704]{1,0:T(8,128)(2,1)S(1)}, bf16[64,704]{1,0:T(8,128)(2,1)S(1)}, u32[]{:S(2)}, u32[]{:S(2)}) collective-permute-start(bf16[64,704]{1,0:T(8,128)(2,1)S(1)} %pad_maximum_fusion.8), channel_id=1, source_target_pairs={{0,64},{64,128},{128,192},{192,256},{256,320},{320,384},{384,448},... | collective-permute-start | bytes 270344 | tf_op jit(solution)/shard_map/ppermute | solution.py:18
  14.8 13.7 %collective-permute-start.3 = (bf16[64,704]{1,0:T(8,128)(2,1)S(1)}, bf16[64,704]{1,0:T(8,128)(2,1)S(1)}, u32[]{:S(2)}, u32[]{:S(2)}) collective-permute-start(bf16[64,704]{1,0:T(8,128)(2,1)S(1)} %pad_maximum_fusion.7), channel_id=1, source_target_pairs={{0,384},{64,448},{128,0},{192,64},{256,128},{320,192},{384,256},{4... | collective-permute-start | bytes 270344 | tf_op jit(solution)/shard_map/ppermute | solution.py:18
  20.7 27.3 %collective-permute-start.15 = (bf16[128,2048]{1,0:T(8,128)(2,1)}, bf16[128,2048]{1,0:T(8,128)(2,1)S(1)}, u32[]{:S(2)}, u32[]{:S(2)}) collective-permute-start(bf16[128,2048]{1,0:T(8,128)(2,1)} %slice_select_fusion), channel_id=1, source_target_pairs={{0,64},{64,0},{1,65},{65,1},{2,66},{66,2},{3,67},{67,3},{4,68},{68... | collective-permute-start | bytes 1572872 | tf_op jit(solution)/shard_map/ppermute | solution.py:22
  26.4 87.6 %collective-permute-start.14 = (bf16[256,352]{0,1:T(8,128)(2,1)S(1)}, bf16[256,352]{0,1:T(8,128)(2,1)S(1)}, u32[]{:S(2)}, u32[]{:S(2)}) collective-permute-start(bf16[256,352]{0,1:T(8,128)(2,1)S(1)} %get-tuple-element.48), channel_id=1, source_target_pairs={{0,64},{64,0},{1,65},{65,1},{2,66},{66,2},{3,67},{67,3},{4,68},{68... | collective-permute-start | bytes 540680 | tf_op jit(solution)/shard_map/ppermute | solution.py:22
  29.5 13.4 %collective-permute-start.5 = (bf16[4,64,704]{2,1,0:T(8,128)(2,1)S(1)}, bf16[4,64,704]{2,1,0:T(8,128)(2,1)S(1)}, u32[]{:S(2)}, u32[]{:S(2)}) collective-permute-start(bf16[4,64,704]{2,1,0:T(8,128)(2,1)S(1)} %get-tuple-element.22), channel_id=1, source_target_pairs={{0,56},{8,0},{16,8},{24,16},{32,24},{40,32},{48,40},{56,48},{1,57}... | collective-permute-start | bytes 1081352 | tf_op jit(solution)/shard_map/ppermute | solution.py:18
  36.9 18.6 %collective-permute-start = (bf16[128,2048]{1,0:T(8,128)(2,1)}, bf16[128,2048]{1,0:T(8,128)(2,1)}, u32[]{:S(2)}, u32[]{:S(2)}) collective-permute-start(bf16[128,2048]{1,0:T(8,128)(2,1)} %slice_select_fusion.1), channel_id=1, source_target_pairs={{0,64},{64,0},{1,65},{65,1},{2,66},{66,2},{3,67},{67,3},{4,68},{68... | collective-permute-start | bytes 1572872 | tf_op jit(solution)/shard_map/ppermute | solution.py:22
  40.8 12.0 %collective-permute-start.8 = (bf16[4,64,704]{2,1,0:T(8,128)(2,1)S(1)}, bf16[4,64,704]{2,1,0:T(8,128)(2,1)S(1)}, u32[]{:S(2)}, u32[]{:S(2)}) collective-permute-start(bf16[4,64,704]{2,1,0:T(8,128)(2,1)S(1)} %get-tuple-element.22), channel_id=1, source_target_pairs={{0,8},{8,16},{16,24},{24,32},{32,40},{40,48},{48,56},{56,0},{1,9},... | collective-permute-start | bytes 1081352 | tf_op jit(solution)/shard_map/ppermute | solution.py:18
  42.9 14.6 %collective-permute-start.6 = (bf16[4,64,704]{2,1,0:T(8,128)(2,1)S(1)}, bf16[4,64,704]{2,1,0:T(8,128)(2,1)S(1)}, u32[]{:S(2)}, u32[]{:S(2)}) collective-permute-start(bf16[4,64,704]{2,1,0:T(8,128)(2,1)S(1)} %collective-permute-done.5), channel_id=1, source_target_pairs={{0,56},{8,0},{16,8},{24,16},{32,24},{40,32},{48,40},{56,48},{1,57}... | collective-permute-start | bytes 1081352 | tf_op jit(solution)/shard_map/ppermute | solution.py:18
  48.0 18.6 %collective-permute-start.16 = (bf16[128,2048]{1,0:T(8,128)(2,1)S(1)}, bf16[128,2048]{1,0:T(8,128)(2,1)}, u32[]{:S(2)}, u32[]{:S(2)}) collective-permute-start(bf16[128,2048]{1,0:T(8,128)(2,1)S(1)} %collective-permute-done.15), channel_id=1, source_target_pairs={{0,1},{1,0},{2,3},{3,2},{4,5},{5,4},{6,7},{7,6},{8,9},{9,8},{10,11... | collective-permute-start | bytes 1572872 | tf_op jit(solution)/shard_map/ppermute | solution.py:22
  55.5 12.2 %collective-permute-start.1 = (bf16[128,2048]{1,0:T(8,128)(2,1)}, bf16[128,2048]{1,0:T(8,128)(2,1)S(1)}, u32[]{:S(2)}, u32[]{:S(2)}) collective-permute-start(bf16[128,2048]{1,0:T(8,128)(2,1)} %collective-permute-done), channel_id=1, source_target_pairs={{0,1},{1,0},{2,3},{3,2},{4,5},{5,4},{6,7},{7,6},{8,9},{9,8},{10,11... | collective-permute-start | bytes 1572872 | tf_op jit(solution)/shard_map/ppermute | solution.py:22
  57.4 22.2 %collective-permute-start.7 = (bf16[4,64,704]{2,1,0:T(8,128)(2,1)S(1)}, bf16[4,64,704]{2,1,0:T(8,128)(2,1)S(1)}, u32[]{:S(2)}, u32[]{:S(2)}) collective-permute-start(bf16[4,64,704]{2,1,0:T(8,128)(2,1)S(1)} %collective-permute-done.6), channel_id=1, source_target_pairs={{0,56},{8,0},{16,8},{24,16},{32,24},{40,32},{48,40},{56,48},{1,57}... | collective-permute-start | bytes 1081352 | tf_op jit(solution)/shard_map/ppermute | solution.py:18
  64.7 13.0 %collective-permute-start.10 = (bf16[4,64,704]{2,1,0:T(8,128)(2,1)S(1)}, bf16[4,64,704]{2,1,0:T(8,128)(2,1)S(1)}, u32[]{:S(2)}, u32[]{:S(2)}) collective-permute-start(bf16[4,64,704]{2,1,0:T(8,128)(2,1)S(1)} %collective-permute-done.9), channel_id=1, source_target_pairs={{0,8},{8,16},{16,24},{24,32},{32,40},{40,48},{48,56},{56,0},{1,9},... | collective-permute-start | bytes 1081352 | tf_op jit(solution)/shard_map/ppermute | solution.py:18
  123.6 34.0 %collective-permute-start.17 = (bf16[512,1024]{1,0:T(8,128)(2,1)}, bf16[512,1024]{1,0:T(8,128)(2,1)}, u32[]{:S(2)}, u32[]{:S(2)}) collective-permute-start(bf16[512,1024]{1,0:T(8,128)(2,1)} %select_convert_fusion), channel_id=1, source_target_pairs={{0,1},{1,0},{2,3},{3,2},{4,5},{5,4},{6,7},{7,6},{8,9},{9,8},{10,11... | collective-permute-start | bytes 3145736 | tf_op jit(solution)/shard_map/ppermute | solution.py:22
  133.0 13.1 %collective-permute-start.18 = (bf16[2,64,704]{2,1,0:T(8,128)(2,1)}, bf16[2,64,704]{2,1,0:T(8,128)(2,1)}, u32[]{:S(2)}, u32[]{:S(2)}) collective-permute-start(bf16[2,64,704]{2,1,0:T(8,128)(2,1)} %get-tuple-element.29), channel_id=1, source_target_pairs={{0,8},{8,16},{16,24},{24,32},{32,40},{40,48},{48,56},{56,0},{1,9},... | collective-permute-start | bytes 540680 | tf_op jit(solution)/shard_map/ppermute | solution.py:18
  141.5 20.5 %all-to-all-start.3 = ((f32[32,1,2112]{2,1,0:T(1,128)}), f32[32,1,2112]{2,1,0:T(1,128)}, u32[]{:S(2)}, u32[]{:S(2)}) async-start(f32[32,1,2112]{2,1,0:T(1,128)} %broadcast_in_dim.5), calls=%async_computation.3 | async-start | bytes 557056 | tf_op jit(solution)/shard_map/all_to_all | solution.py:233
  148.9 18.5 %collective-permute-start.23 = (bf16[4,64,704]{2,1,0:T(8,128)(2,1)}, bf16[4,64,704]{2,1,0:T(8,128)(2,1)}, u32[]{:S(2)}, u32[]{:S(2)}) collective-permute-start(bf16[4,64,704]{2,1,0:T(8,128)(2,1)} %pad_maximum_fusion.5), channel_id=1, source_target_pairs={{0,56},{8,0},{16,8},{24,16},{32,24},{40,32},{48,40},{56,48},{1,57}... | collective-permute-start | bytes 1081352 | tf_op jit(solution)/shard_map/ppermute | solution.py:18
  155.7 13.8 %collective-permute-start.19 = (bf16[4,64,704]{2,1,0:T(8,128)(2,1)}, bf16[4,64,704]{2,1,0:T(8,128)(2,1)}, u32[]{:S(2)}, u32[]{:S(2)}) collective-permute-start(bf16[4,64,704]{2,1,0:T(8,128)(2,1)} %pad_maximum_fusion.4), channel_id=1, source_target_pairs={{0,8},{8,16},{16,24},{24,32},{32,40},{40,48},{48,56},{56,0},{1,9},... | collective-permute-start | bytes 1081352 | tf_op jit(solution)/shard_map/ppermute | solution.py:18
  162.0 41.6 %all-to-all-start = ((bf16[8,64,1024]{2,1,0:T(8,128)(2,1)}), bf16[8,64,1024]{2,1,0:T(8,128)(2,1)}, u32[]{:S(2)}, u32[]{:S(2)}) async-start(bf16[8,64,1024]{2,1,0:T(8,128)(2,1)} %bitcast.127), calls=%async_computation | async-start | bytes 2097152 | tf_op jit(solution)/shard_map/all_to_all | solution.py:220
  171.6 12.9 %collective-permute-start.20 = (bf16[4,64,704]{2,1,0:T(8,128)(2,1)}, bf16[4,64,704]{2,1,0:T(8,128)(2,1)}, u32[]{:S(2)}, u32[]{:S(2)}) collective-permute-start(bf16[4,64,704]{2,1,0:T(8,128)(2,1)} %get-tuple-element.25), channel_id=1, source_target_pairs={{0,8},{8,16},{16,24},{24,32},{32,40},{40,48},{48,56},{56,0},{1,9},... | collective-permute-start | bytes 1081352 | tf_op jit(solution)/shard_map/ppermute | solution.py:18
  173.5 12.2 %collective-permute-start.24 = (bf16[4,64,704]{2,1,0:T(8,128)(2,1)}, bf16[4,64,704]{2,1,0:T(8,128)(2,1)}, u32[]{:S(2)}, u32[]{:S(2)}) collective-permute-start(bf16[4,64,704]{2,1,0:T(8,128)(2,1)} %get-tuple-element.26), channel_id=1, source_target_pairs={{0,56},{8,0},{16,8},{24,16},{32,24},{40,32},{48,40},{56,48},{1,57}... | collective-permute-start | bytes 1081352 | tf_op jit(solution)/shard_map/ppermute | solution.py:18
  187.8 12.5 %collective-permute-start.21 = (bf16[4,64,704]{2,1,0:T(8,128)(2,1)}, bf16[4,64,704]{2,1,0:T(8,128)(2,1)}, u32[]{:S(2)}, u32[]{:S(2)}) collective-permute-start(bf16[4,64,704]{2,1,0:T(8,128)(2,1)} %get-tuple-element.23), channel_id=1, source_target_pairs={{0,8},{8,16},{16,24},{24,32},{32,40},{40,48},{48,56},{56,0},{1,9},... | collective-permute-start | bytes 1081352 | tf_op jit(solution)/shard_map/ppermute | solution.py:18
  203.5 19.1 %all-to-all-start.2 = ((bf16[4,64,704]{2,1,0:T(8,128)(2,1)}), bf16[4,64,704]{2,1,0:T(8,128)(2,1)S(1)}, u32[]{:S(2)}, u32[]{:S(2)}) async-start(bf16[4,64,704]{2,1,0:T(8,128)(2,1)} %fusion.10), calls=%async_computation.2 | async-start | bytes 786432 | tf_op jit(solution)/shard_map/all_to_all | solution.py:205
  223.7 18.6 %all-to-all-start.1 = ((bf16[8,64,1024]{2,1,0:T(8,128)(2,1)}), bf16[8,64,1024]{2,1,0:T(8,128)(2,1)S(1)}, u32[]{:S(2)}, u32[]{:S(2)}) async-start(bf16[8,64,1024]{2,1,0:T(8,128)(2,1)} %broadcast_in_dim.4), calls=%async_computation.1 | async-start | bytes 2097152 | tf_op jit(solution)/shard_map/all_to_all | solution.py:225
  (25 other events, 331.4 us)

commit v2 on v1

--- a/solution.py
+++ b/solution.py
@@ -4,18 +4,13 @@
 from jax.sharding import Mesh
 from jax.sharding import PartitionSpec as P
 
-Z_ALL = ("rep", "zp", "zb")
+Z = ("zp", "zb")
 FS = ("zp", "zb", "y")
 REP_FS = ("rep", "zp", "zb", "y")
 TP = ("x", "c")
 
 contract_last = (((1,), (1,)), ((), ()))
 contract_first = (((0,), (0,)), ((), ()))
-
-
-def shifted(values, axis, by):
-    size = lax.axis_size(axis)
-    return lax.ppermute(values, axis, [(k, (k + by) % size) for k in range(size)])
 
 
 def swapped(values, axis):
@@ -66,47 +61,6 @@
 
 def stored(product):
     return lax.optimization_barrier(product.astype(jnp.bfloat16)).astype(jnp.float32)
-
-
-def rolled(blocks, by):
-    size = blocks.shape[0]
-    twice = jnp.concatenate([blocks, blocks], axis=0)
-    return lax.dynamic_slice_in_dim(twice, (size - by) % size, size, 0)
-
-
-def gathered_ring(block, axis):
-    size = lax.axis_size(axis)
-    half = size // 2
-    cut = block.shape[0] // 2
-    from_below, from_above = [block], [block]
-    for step in range(1, half):
-        from_below.append(shifted(from_below[-1], axis, 1))
-        from_above.append(shifted(from_above[-1], axis, -1))
-    far = jnp.concatenate(
-        [shifted(from_below[-1][:cut], axis, 1), shifted(from_above[-1][cut:], axis, -1)]
-    )
-    return jnp.stack(from_above + [far] + from_below[:0:-1])
-
-
-def summed_ring(block_of, axis):
-    size = lax.axis_size(axis)
-    half = size // 2
-    far = block_of(half)
-    cut = far.shape[0] // 2
-    up = shifted(far[:cut], axis, 1)
-    down = shifted(far[cut:], axis, -1)
-    for step in range(half - 1, 0, -1):
-        above, below = block_of(step), block_of(-step)
-        if step == half - 1:
-            above = jnp.concatenate([above[:cut] + up, above[cut:]])
-            below = jnp.concatenate([below[:cut], below[cut:] + down])
-        else:
-            above = above + up
-            below = below + down
-        up = shifted(above, axis, 1)
-        down = shifted(below, axis, -1)
-    wide = jnp.float32
-    return block_of(0).astype(wide) + up.astype(wide) + down.astype(wide)
 
 
 def per_device(
@@ -129,8 +83,6 @@
     n_y = lax.axis_size("y")
     n_x = lax.axis_size("x")
     zb = lax.axis_index("zb")
-    z = lax.axis_index("zp") * 2 + zb
-    y = lax.axis_index("y")
     first_z = zb == 0
     first_c = lax.axis_index("c") == 0
     rows_scale = (row_count * n_z * n_y) ** (-0.5)
@@ -146,29 +98,35 @@
             jnp.concatenate([other, mine], axis=-1),
         )
 
-    def partner_rows(rows):
+    def own_and_partner(late, early):
         cut = row_count // 2
-        sent = pick(first_c, rows[:cut], rows[cut:])
+        sent = jnp.concatenate(
+            [pick(first_c, rows[:cut], rows[cut:]) for rows in (early, late)]
+        )
         here = swapped(sent, "zb")
         there = swapped(here, "c")
-        return jnp.concatenate([pick(first_c, here, there), pick(first_c, there, here)])
+        low, high = pick(first_c, here, there), pick(first_c, there, here)
+        return (
+            jnp.concatenate([late, low[cut:], high[cut:]]),
+            jnp.concatenate([early, low[:cut], high[:cut]]),
+        )
 
     gate_mine, gate_other = halves(gate_weight)
     up_mine, up_other = halves(up_weight)
     weight_mine = jnp.concatenate([gate_mine, up_mine], axis=1)
     weight_other = jnp.concatenate([gate_other, up_other], axis=1)
-    next_one = shifted(weight_other, Z_ALL, -1)
-    previous_one = shifted(weight_other, Z_ALL, 1)
-    opposite = shifted(weight_mine, Z_ALL, -2)
-    block = rolled(jnp.stack([weight_mine, next_one, opposite, previous_one]), z)
-    early_pair = jnp.concatenate([early_rows, partner_rows(early_rows)])
+    for_z = jnp.stack(
+        [pick(first_z, weight_mine, weight_other), pick(first_z, weight_other, weight_mine)] * 2
+    )
+    block = lax.all_to_all(for_z, Z, 0, 0, tiled=True)
+    late_pair, early_pair = own_and_partner(late_rows, early_rows)
     cot_mine, cot_other = halves(hidden_cot)
     cotangent = jnp.stack([cot_mine, swapped(cot_other, "zb")]).astype(jnp.float32)
-    late_pair = jnp.concatenate([late_rows, partner_rows(late_rows)])
     gate_filter = halves(gate_taps)[0].astype(jnp.float32)
     up_filter = halves(up_taps)[0].astype(jnp.float32)
 
-    weight = rolled(gathered_ring(block, "y"), y)
+    copies = jnp.broadcast_to(block[None], (n_y, *block.shape))
+    weight = lax.all_to_all(copies, "y", 0, 0, tiled=True)
     weight = weight.transpose(1, 0, 2, 3).reshape(depth, 2 * width)
 
     def project(rows):
@@ -197,12 +155,9 @@
     ).astype(jnp.bfloat16)
     terms = terms.reshape(n_z, n_y, shard_rows, 2 * width)
 
-    def terms_for(offset):
-        at = (y + offset + n_y) % n_y
-        return lax.dynamic_index_in_dim(terms, at, 1, keepdims=False)
-
-    reduced = summed_ring(terms_for, "y").astype(jnp.bfloat16)
-    pieces = lax.all_to_all(reduced, ("zp", "zb"), 0, 0, tiled=True)
+    terms = lax.all_to_all(terms.transpose(1, 0, 2, 3), "y", 0, 0, tiled=True)
+    reduced = jnp.sum(terms.astype(jnp.float32), axis=0).astype(jnp.bfloat16)
+    pieces = lax.all_to_all(reduced, Z, 0, 0, tiled=True)
     pieces = pieces.reshape(2, 2, shard_rows, 2 * width).astype(jnp.float32)
     pieces = jnp.sum(pieces, axis=0)
     gate_sum = jnp.concatenate([pieces[0, :, :width], pieces[1, :, :width]], axis=1)

time: 249 us -> 291 us (1.17)
  waiting for transfers between devices: 46 us -> 167 us
  starting transfers between devices: 115 us -> 43.1 us
  blocking collectives: 0 us -> 18.7 us
  other arithmetic: 37.6 us -> 19.7 us
  local copies, waits for them, and re-layouts: 35.2 us -> 28.8 us
    all_to_all x1 -> x3, waiting for transfers between devices: 0.01 us -> 109 us  [the longest x1 70.9 us: per_device(): terms = lax.all_to_all(terms.transpose(1, 0, 2, 3), 'y', 0, 0, tiled=True)]
    ppermute x19 -> x0, starting transfers between devices: 74.5 us -> none  [shifted(): lax.ppermute(values, axis, [(k, (k + by) % size) for k in range(size)])]
    ppermute x19 -> x0, waiting for transfers between devices: 29.1 us -> none  [shifted(): lax.ppermute(values, axis, [(k, (k + by) % size) for k in range(size)])]
    ppermute x7 -> x5, waiting for transfers between devices: 6.21 us -> 32.2 us  [swapped(): return lax.ppermute(values, axis, [(0, 1), (1, 0)])]
    all_to_all x0 -> x1, blocking collectives: none -> 18.7 us  [per_device(): block = lax.all_to_all(for_z, Z, 0, 0, tiled=True)]
    unnamed x62 -> x50, local copies, waits for them, and re-layouts: 18 us -> 7.66 us
    all_to_all x1 -> x3, starting transfers between devices: 5.36 us -> 15.7 us  [the longest x1 7.1 us: per_device(): weight = lax.all_to_all(copies, 'y', 0, 0, tiled=True)]
    all_to_all x1, waiting for transfers between devices: 0.01 us -> 8.88 us  [per_device(): lax.all_to_all(jnp.broadcast_to(taps.reshape(1, -1), (n_fs, taps.size)),...]
  transfers between devices with their start and end apart: 30 -> 11, of which waited for: 12 -> 7; matrix products, arithmetic and copies ran while one was open for 26% -> 13% of each run, Pallas kernels for 0% -> 0%
where the time goes in v2:
time: 291 us; the launch traced here: 288 us
  waiting for transfers between devices  167 us (57%)
  starting transfers between devices  43.1 us (15%)
  local copies, waits for them, and re-layouts  28.8 us (10%)
  other arithmetic  19.7 us (7%)
  blocking collectives  18.7 us (6%)
  matrix products  9.36 us (3%)
    all_to_all x1, waiting for transfers between devices, per_device(): terms = lax.all_to_all(terms.transpose(1, 0, 2, 3), 'y', 0, 0, tiled=True)  70.9 us
    all_to_all x1, waiting for transfers between devices, per_device(): weight = lax.all_to_all(copies, 'y', 0, 0, tiled=True)  38.2 us
    ppermute x5, waiting for transfers between devices, swapped(): return lax.ppermute(values, axis, [(0, 1), (1, 0)])  32.2 us
    all_to_all x1, blocking collectives, per_device(): block = lax.all_to_all(for_z, Z, 0, 0, tiled=True)  18.7 us
    all_to_all x1, waiting for transfers between devices, per_device(): finished = lax.all_to_all(copies, TP, 0, 0, tiled=True)  12.6 us
    ppermute x5, starting transfers between devices, swapped(): return lax.ppermute(values, axis, [(0, 1), (1, 0)])  12 us
    all_to_all x1, waiting for transfers between devices, per_device(): lax.all_to_all(jnp.broadcast_to(taps.reshape(1, -1), (n_fs, taps.size)),...  8.88 us
    unnamed x50, local copies, waits for them, and re-layouts  7.66 us
  transfers between devices with their start and end apart: 11, of which 7 were waited for; matrix products, arithmetic and copies ran while one was open for 13% of the time, Pallas kernels for 0%

profile of v2, /device:TPU:6, one launch (start us, length us, event | category | flops | bytes accessed | tf_op | source)
XLA Modules:
  0.0 287.7 jit_solution(3703482040810851895)
XLA Ops:
  1.8 18.7 %all_to_all.36 = bf16[4,64,704]{2,1,0:T(8,128)(2,1)S(1)} all-to-all(bf16[4,64,704]{2,1,0:T(8,128)(2,1)S(1)} %pad_maximum_fusion.5), channel_id=1, replica_groups=mesh['rep'=2,'zp'=2,'zb'=2,'y'=8,'x'=4,'c'=2] {'zp','zb'}, dimensions={0} | all-to-all | bytes 720896 | tf_op jit(solution)/shard_map/all_to_all | solution.py:121
  22.6 7.1 %all-to-all-start.1 = ((bf16[8,4,64,704]{3,2,1,0:T(8,128)(2,1)}), bf16[8,4,64,704]{3,2,1,0:T(8,128)(2,1)S(1)}, u32[]{:S(2)}, u32[]{:S(2)}) async-start(bf16[8,4,64,704]{3,2,1,0:T(8,128)(2,1)} %broadcast_in_dim.6), calls=%async_computation.1 | async-start | bytes 6291456 | tf_op jit(solution)/shard_map/all_to_all | solution.py:129
  31.5 2.1 collective-permute-start
  33.6 23.3 %collective-permute-done = bf16[256,2048]{1,0:T(8,128)(2,1)S(1)} collective-permute-done((bf16[256,2048]{1,0:T(8,128)(2,1)S(1)}, bf16[256,2048]{1,0:T(8,128)(2,1)S(1)}, u32[]{:S(2)}, u32[]{:S(2)}) %collective-permute-start) | collective-permute-done | bytes 1048608 | tf_op jit(solution)/shard_map/ppermute | solution.py:17
  59.5 2.2 collective-permute-start.3
  64.1 38.2 %all-to-all-done.1 = bf16[8,4,64,704]{3,2,1,0:T(8,128)(2,1)S(1)} async-done(((bf16[8,4,64,704]{3,2,1,0:T(8,128)(2,1)}), bf16[8,4,64,704]{3,2,1,0:T(8,128)(2,1)S(1)}, u32[]{:S(2)}, u32[]{:S(2)}) %all-to-all-start.1) | async-done | bytes 2883616 | tf_op jit(solution)/shard_map/all_to_all | solution.py:129
  110.0 2.6 fusion.6
  112.6 2.9 %reshape.243 = f32[2,256,704]{1,0,2:T(2,128)} reshape(bf16[512,704]{0,1:T(8,128)(2,1)} %fusion.6) | data formatting | bytes 2162688 | tf_op jit(solution)/shard_map/reshape | solution.py:134
  129.0 3.9 %all-to-all-start.6 = ((f32[32,1,2112]{2,1,0:T(1,128)}), f32[32,1,2112]{2,1,0:T(1,128)S(1)}, u32[]{:S(2)}, u32[]{:S(2)}) async-start(f32[32,1,2112]{2,1,0:T(1,128)} %broadcast_in_dim.8), calls=%async_computation.6 | async-start | bytes 557056 | tf_op jit(solution)/shard_map/all_to_all | solution.py:188
  132.9 2.8 add_convert_fusion
  136.9 8.9 %all-to-all-done.6 = f32[32,1,2112]{2,1,0:T(1,128)S(1)} async-done(((f32[32,1,2112]{2,1,0:T(1,128)}), f32[32,1,2112]{2,1,0:T(1,128)S(1)}, u32[]{:S(2)}, u32[]{:S(2)}) %all-to-all-start.6) | async-done | bytes 270368 | tf_op jit(solution)/shard_map/all_to_all | solution.py:188
  145.8 5.0 %all-to-all-start.2 = ((bf16[8,64,1024]{2,1,0:T(8,128)(2,1)}), bf16[8,64,1024]{2,1,0:T(8,128)(2,1)}, u32[]{:S(2)}, u32[]{:S(2)}) async-start(bf16[8,64,1024]{2,1,0:T(8,128)(2,1)} %bitcast.12), calls=%async_computation.2 | async-start | bytes 2097152 | tf_op jit(solution)/shard_map/all_to_all | solution.py:175
  150.8 3.2 %multiply_convert_fusion = bf16[2048,704]{0,1:T(8,128)(2,1)} fusion(bf16[512,704]{0,1:T(8,128)(2,1)S(1)} %bitcast.67, bf16[128,2048]{1,0:T(8,128)(2,1)S(1)} %copy-done.10, bf16[128,2048]{1,0:T(8,128)(2,1)S(1)} %copy-done.12, bf16[256,2048]{1,0:T(8,128)(2,1)S(1)} %copy-done.8), kind=kOutput, calls=%fused_computation | convolution fusion | flops 1485570048 | bytes 5701632 | tf_op jit(solution)/shard_map/dot_general | solution.py:151
  154.0 3.1 %copy.65 = bf16[2048,704]{1,0:T(8,128)(2,1)S(1)} copy(bf16[2048,704]{0,1:T(8,128)(2,1)} %multiply_convert_fusion) | data formatting | bytes 5767168 | tf_op jit(solution)/shard_map/convert_element_type | solution.py:155
  159.0 4.0 %all-to-all-done.2 = bf16[8,64,1024]{2,1,0:T(8,128)(2,1)} async-done(((bf16[8,64,1024]{2,1,0:T(8,128)(2,1)}), bf16[8,64,1024]{2,1,0:T(8,128)(2,1)}, u32[]{:S(2)}, u32[]{:S(2)}) %all-to-all-start.2) | async-done | bytes 1048608 | tf_op jit(solution)/shard_map/all_to_all | solution.py:175
  163.0 5.1 %all-to-all-start.4 = ((bf16[8,4,64,704]{3,2,1,0:T(8,128)(2,1)}), bf16[8,4,64,704]{3,2,1,0:T(8,128)(2,1)S(1)}, u32[]{:S(2)}, u32[]{:S(2)}) async-start(bf16[8,4,64,704]{3,2,1,0:T(8,128)(2,1)} %copy.66), calls=%async_computation.4 | async-start | bytes 6291456 | tf_op jit(solution)/shard_map/all_to_all | solution.py:158
  168.1 2.1 reduce_sum.96
  170.2 70.9 %all-to-all-done.4 = bf16[8,4,64,704]{3,2,1,0:T(8,128)(2,1)S(1)} async-done(((bf16[8,4,64,704]{3,2,1,0:T(8,128)(2,1)}), bf16[8,4,64,704]{3,2,1,0:T(8,128)(2,1)S(1)}, u32[]{:S(2)}, u32[]{:S(2)}) %all-to-all-start.4) | async-done | bytes 2883616 | tf_op jit(solution)/shard_map/all_to_all | solution.py:158
  243.1 6.5 %all-to-all-start.3 = ((bf16[8,64,1024]{2,1,0:T(8,128)(2,1)}), bf16[8,64,1024]{2,1,0:T(8,128)(2,1)}, u32[]{:S(2)}, u32[]{:S(2)}) async-start(bf16[8,64,1024]{2,1,0:T(8,128)(2,1)} %broadcast_in_dim.7), calls=%async_computation.3 | async-start | bytes 2097152 | tf_op jit(solution)/shard_map/all_to_all | solution.py:180
  251.0 12.6 %all-to-all-done.3 = bf16[8,64,1024]{2,1,0:T(8,128)(2,1)} async-done(((bf16[8,64,1024]{2,1,0:T(8,128)(2,1)}), bf16[8,64,1024]{2,1,0:T(8,128)(2,1)}, u32[]{:S(2)}, u32[]{:S(2)}) %all-to-all-start.3) | async-done | bytes 1048608 | tf_op jit(solution)/shard_map/all_to_all | solution.py:180
  263.6 3.5 %all-to-all-start.5 = ((bf16[4,64,704]{2,1,0:T(8,128)(2,1)}), bf16[4,64,704]{2,1,0:T(8,128)(2,1)S(1)}, u32[]{:S(2)}, u32[]{:S(2)}) async-start(bf16[4,64,704]{2,1,0:T(8,128)(2,1)} %reduce_sum.97), calls=%async_computation.5 | async-start | bytes 786432 | tf_op jit(solution)/shard_map/all_to_all | solution.py:160
  267.1 3.9 %collective-permute-start.2 = (bf16[256,352]{0,1:T(8,128)(2,1)S(1)}, bf16[256,352]{0,1:T(8,128)(2,1)S(1)}, u32[]{:S(2)}, u32[]{:S(2)}) collective-permute-start(bf16[256,352]{0,1:T(8,128)(2,1)S(1)} %get-tuple-element.40), channel_id=1, source_target_pairs={{0,64},{64,0},{1,65},{65,1},{2,66},{66,2},{3,67},{67,3},{4,68},{68... | collective-permute-start | bytes 540680 | tf_op jit(solution)/shard_map/ppermute | solution.py:17
  271.0 8.9 %collective-permute-done.2 = bf16[256,352]{0,1:T(8,128)(2,1)S(1)} collective-permute-done((bf16[256,352]{0,1:T(8,128)(2,1)S(1)}, bf16[256,352]{0,1:T(8,128)(2,1)S(1)}, u32[]{:S(2)}, u32[]{:S(2)}) %collective-permute-start.2) | collective-permute-done | bytes 180256 | tf_op jit(solution)/shard_map/ppermute | solution.py:17
  282.4 2.3 copy.64
  (111 shorter events, 42.7 us)
Async XLA Ops:
  22.6 79.8 %all-to-all-start.1 = ((bf16[8,4,64,704]{3,2,1,0:T(8,128)(2,1)}), bf16[8,4,64,704]{3,2,1,0:T(8,128)(2,1)S(1)}, u32[]{:S(2)}, u32[]{:S(2)}) async-start(bf16[8,4,64,704]{3,2,1,0:T(8,128)(2,1)} %broadcast_in_dim.6), calls=%async_computation.1 | async-start | bytes 6291456 | tf_op jit(solution)/shard_map/all_to_all | solution.py:129
  29.7 29.2 %copy-start.15 = (bf16[256,704]{0,1:T(8,128)(2,1)S(1)}, bf16[256,704]{0,1:T(8,128)(2,1)}, u32[]{:S(2)}) copy-start(bf16[256,704]{0,1:T(8,128)(2,1)} %param.13) | copy-start | bytes 1081348
  31.3 30.4 %copy-start.20 = (bf16[3,704]{1,0:T(4,128)(2,1)S(1)}, bf16[3,704]{1,0:T(4,128)(2,1)}, u32[]{:S(2)}) copy-start(bf16[3,704]{1,0:T(4,128)(2,1)} %param.17) | copy-start | bytes 12676
  31.3 30.4 %copy-start.21 = (bf16[3,704]{1,0:T(4,128)(2,1)S(1)}, bf16[3,704]{1,0:T(4,128)(2,1)}, u32[]{:S(2)}) copy-start(bf16[3,704]{1,0:T(4,128)(2,1)} %param.16) | copy-start | bytes 12676
  31.5 25.4 %collective-permute-start = (bf16[256,2048]{1,0:T(8,128)(2,1)S(1)}, bf16[256,2048]{1,0:T(8,128)(2,1)S(1)}, u32[]{:S(2)}, u32[]{:S(2)}) collective-permute-start(bf16[256,2048]{1,0:T(8,128)(2,1)S(1)} %pad_maximum_fusion.1), channel_id=1, source_target_pairs={{0,64},{64,0},{1,65},{65,1},{2,66},{66,2},{3,67},{67,3},{4,68},{68... | collective-permute-start | bytes 3145736 | tf_op jit(solution)/shard_map/ppermute | solution.py:17
  56.9 5.0 %collective-permute-start.1 = (bf16[256,2048]{1,0:T(8,128)(2,1)S(1)}, bf16[256,2048]{1,0:T(8,128)(2,1)S(1)}, u32[]{:S(2)}, u32[]{:S(2)}) collective-permute-start(bf16[256,2048]{1,0:T(8,128)(2,1)S(1)} %collective-permute-done), channel_id=1, source_target_pairs={{0,1},{1,0},{2,3},{3,2},{4,5},{5,4},{6,7},{7,6},{8,9},{9,8},{10,11... | collective-permute-start | bytes 3145736 | tf_op jit(solution)/shard_map/ppermute | solution.py:17
  59.5 57.9 %collective-permute-start.3 = (bf16[256,352]{0,1:T(8,128)(2,1)}, bf16[256,352]{0,1:T(8,128)(2,1)S(1)}, u32[]{:S(2)}, u32[]{:S(2)}) collective-permute-start(bf16[256,352]{0,1:T(8,128)(2,1)} %get-tuple-element.38), channel_id=1, source_target_pairs={{0,64},{64,0},{1,65},{65,1},{2,66},{66,2},{3,67},{67,3},{4,68},{68... | collective-permute-start | bytes 540680 | tf_op jit(solution)/shard_map/ppermute | solution.py:17
  102.4 2.5 copy-start.11
  119.9 2.1 copy-start.3
  126.0 6.9 %collective-permute-start.4 = (bf16[512,1024]{1,0:T(8,128)(2,1)S(1)}, bf16[512,1024]{1,0:T(8,128)(2,1)S(1)}, u32[]{:S(2)}, u32[]{:S(2)}) collective-permute-start(bf16[512,1024]{1,0:T(8,128)(2,1)S(1)} %select_convert_fusion), channel_id=1, source_target_pairs={{0,1},{1,0},{2,3},{3,2},{4,5},{5,4},{6,7},{7,6},{8,9},{9,8},{10,11... | collective-permute-start | bytes 3145736 | tf_op jit(solution)/shard_map/ppermute | solution.py:17
  129.0 16.8 %all-to-all-start.6 = ((f32[32,1,2112]{2,1,0:T(1,128)}), f32[32,1,2112]{2,1,0:T(1,128)S(1)}, u32[]{:S(2)}, u32[]{:S(2)}) async-start(f32[32,1,2112]{2,1,0:T(1,128)} %broadcast_in_dim.8), calls=%async_computation.6 | async-start | bytes 557056 | tf_op jit(solution)/shard_map/all_to_all | solution.py:188
  135.8 15.0 %copy-start.8 = (bf16[256,2048]{1,0:T(8,128)(2,1)S(1)}, bf16[256,2048]{1,0:T(8,128)(2,1)}, u32[]{:S(2)}) copy-start(bf16[256,2048]{1,0:T(8,128)(2,1)} %param.12) | copy-start | bytes 3145732
  135.8 15.0 %copy-start.10 = (bf16[128,2048]{1,0:T(8,128)(2,1)S(1)}, bf16[128,2048]{1,0:T(8,128)(2,1)}, u32[]{:S(2)}) copy-start(bf16[128,2048]{1,0:T(8,128)(2,1)} %get-tuple-element.31) | copy-start | bytes 1572868
  135.8 15.0 %copy-start.12 = (bf16[128,2048]{1,0:T(8,128)(2,1)S(1)}, bf16[128,2048]{1,0:T(8,128)(2,1)}, u32[]{:S(2)}) copy-start(bf16[128,2048]{1,0:T(8,128)(2,1)} %get-tuple-element.29) | copy-start | bytes 1572868
  145.8 5.0 %copy-start.4 = (f32[32,1,2112]{2,1,0:T(1,128)}, f32[32,1,2112]{2,1,0:T(1,128)S(1)}, u32[]{:S(2)}) copy-start(f32[32,1,2112]{2,1,0:T(1,128)S(1)} %all-to-all-done.6) | copy-start | bytes 811012
  145.8 17.2 %all-to-all-start.2 = ((bf16[8,64,1024]{2,1,0:T(8,128)(2,1)}), bf16[8,64,1024]{2,1,0:T(8,128)(2,1)}, u32[]{:S(2)}, u32[]{:S(2)}) async-start(bf16[8,64,1024]{2,1,0:T(8,128)(2,1)} %bitcast.12), calls=%async_computation.2 | async-start | bytes 2097152 | tf_op jit(solution)/shard_map/all_to_all | solution.py:175
  163.0 78.1 %all-to-all-start.4 = ((bf16[8,4,64,704]{3,2,1,0:T(8,128)(2,1)}), bf16[8,4,64,704]{3,2,1,0:T(8,128)(2,1)S(1)}, u32[]{:S(2)}, u32[]{:S(2)}) async-start(bf16[8,4,64,704]{3,2,1,0:T(8,128)(2,1)} %copy.66), calls=%async_computation.4 | async-start | bytes 6291456 | tf_op jit(solution)/shard_map/all_to_all | solution.py:158
  243.1 20.5 %all-to-all-start.3 = ((bf16[8,64,1024]{2,1,0:T(8,128)(2,1)}), bf16[8,64,1024]{2,1,0:T(8,128)(2,1)}, u32[]{:S(2)}, u32[]{:S(2)}) async-start(bf16[8,64,1024]{2,1,0:T(8,128)(2,1)} %broadcast_in_dim.7), calls=%async_computation.3 | async-start | bytes 2097152 | tf_op jit(solution)/shard_map/all_to_all | solution.py:180
  251.0 29.8 %copy-start.5 = (f32[32,1,2112]{2,1,0:T(1,128)S(1)}, f32[32,1,2112]{2,1,0:T(1,128)}, u32[]{:S(2)}) copy-start(f32[32,1,2112]{2,1,0:T(1,128)} %copy-done.4) | copy-start | bytes 811012
  251.0 30.2 %copy-start.18 = (f32[3,704]{1,0:T(4,128)S(1)}, f32[3,704]{1,0:T(4,128)}, u32[]{:S(2)}) copy-start(f32[3,704]{1,0:T(4,128)} %param.20) | copy-start | bytes 25348
  251.0 30.8 %copy-start.19 = (f32[3,704]{1,0:T(4,128)S(1)}, f32[3,704]{1,0:T(4,128)}, u32[]{:S(2)}) copy-start(f32[3,704]{1,0:T(4,128)} %param.21) | copy-start | bytes 25348
  263.6 22.4 %all-to-all-start.5 = ((bf16[4,64,704]{2,1,0:T(8,128)(2,1)}), bf16[4,64,704]{2,1,0:T(8,128)(2,1)S(1)}, u32[]{:S(2)}, u32[]{:S(2)}) async-start(bf16[4,64,704]{2,1,0:T(8,128)(2,1)} %reduce_sum.97), calls=%async_computation.5 | async-start | bytes 786432 | tf_op jit(solution)/shard_map/all_to_all | solution.py:160
  267.1 12.8 %collective-permute-start.2 = (bf16[256,352]{0,1:T(8,128)(2,1)S(1)}, bf16[256,352]{0,1:T(8,128)(2,1)S(1)}, u32[]{:S(2)}, u32[]{:S(2)}) collective-permute-start(bf16[256,352]{0,1:T(8,128)(2,1)S(1)} %get-tuple-element.40), channel_id=1, source_target_pairs={{0,64},{64,0},{1,65},{65,1},{2,66},{66,2},{3,67},{67,3},{4,68},{68... | collective-permute-start | bytes 540680 | tf_op jit(solution)/shard_map/ppermute | solution.py:17
  284.7 2.2 copy-start.17
  (9 other events, 16.4 us)

commit v3 on v2

--- a/solution.py
+++ b/solution.py
@@ -79,6 +79,7 @@
     row_count, depth = late_rows.shape
     shard_rows, width_local = gate_weight.shape
     width = width_local // 2
+    wide = -(-width // 128) * 128
     n_z = lax.axis_size("zp") * lax.axis_size("zb")
     n_y = lax.axis_size("y")
     n_x = lax.axis_size("x")
@@ -87,8 +88,12 @@
     first_c = lax.axis_index("c") == 0
     rows_scale = (row_count * n_z * n_y) ** (-0.5)
 
+    def widened(array):
+        edges = [(0, 0)] * (array.ndim - 1)
+        return jnp.pad(array, edges + [(0, wide - width)])
+
     def halves(array):
-        low, high = array[..., :width], array[..., width:]
+        low, high = widened(array[..., :width]), widened(array[..., width:])
         return pick(first_z, low, high), pick(first_z, high, low)
 
     def columns_joined(mine, other):
@@ -125,14 +130,14 @@
     gate_filter = halves(gate_taps)[0].astype(jnp.float32)
     up_filter = halves(up_taps)[0].astype(jnp.float32)
 
-    copies = jnp.broadcast_to(block[None], (n_y, *block.shape))
-    weight = lax.all_to_all(copies, "y", 0, 0, tiled=True)
-    weight = weight.transpose(1, 0, 2, 3).reshape(depth, 2 * width)
+    block = block.reshape(n_z * shard_rows, 2 * wide)
+    weight = lax.all_gather(block, "y").reshape(n_y, n_z, shard_rows, 2 * wide)
+    weight = weight.transpose(1, 0, 2, 3).reshape(depth, 2 * wide)
 
     def project(rows):
         product = stored(jnp.dot(rows, weight, preferred_element_type=jnp.float32))
-        product = product.reshape(2, row_count, 2 * width)
-        return product[..., :width], product[..., width:]
+        product = product.reshape(2, row_count, 2 * wide)
+        return product[..., :wide], product[..., wide:]
 
     early_gate, early_up = project(early_pair)
     gate_mix = causal_mix(early_gate, gate_filter)
@@ -145,7 +150,7 @@
     d_gate_pre = mix_back(d_gate_mix, gate_filter).astype(jnp.bfloat16)
     d_up_pre = mix_back(d_up_mix, up_filter).astype(jnp.bfloat16)
     both_grads = jnp.concatenate([d_gate_pre, d_up_pre], axis=-1)
-    both_grads = both_grads.reshape(2 * row_count, 2 * width)
+    both_grads = both_grads.reshape(2 * row_count, 2 * wide)
 
     terms = (
         lax.dot_general(
@@ -153,15 +158,16 @@
         )
         * rows_scale
     ).astype(jnp.bfloat16)
-    terms = terms.reshape(n_z, n_y, shard_rows, 2 * width)
-
-    terms = lax.all_to_all(terms.transpose(1, 0, 2, 3), "y", 0, 0, tiled=True)
-    reduced = jnp.sum(terms.astype(jnp.float32), axis=0).astype(jnp.bfloat16)
+    terms = terms.reshape(n_z, n_y, shard_rows, 2 * wide)
+
+    terms = terms.transpose(1, 0, 2, 3).reshape(depth, 2 * wide)
+    reduced = lax.psum_scatter(terms, "y", scatter_dimension=0, tiled=True)
+    reduced = reduced.reshape(n_z, shard_rows, 2 * wide)
     pieces = lax.all_to_all(reduced, Z, 0, 0, tiled=True)
-    pieces = pieces.reshape(2, 2, shard_rows, 2 * width).astype(jnp.float32)
+    pieces = pieces.reshape(2, 2, shard_rows, 2 * wide).astype(jnp.float32)
     pieces = jnp.sum(pieces, axis=0)
     gate_sum = jnp.concatenate([pieces[0, :, :width], pieces[1, :, :width]], axis=1)
-    up_sum = jnp.concatenate([pieces[0, :, width:], pieces[1, :, width:]], axis=1)
+    up_sum = jnp.concatenate([pieces[0, :, wide : wide + width], pieces[1, :, wide : wide + width]], axis=1)
 
     partial = lax.dot_general(
         both_grads, weight, contract_last, preferred_element_type=jnp.float32
@@ -189,14 +195,14 @@
         jnp.broadcast_to(taps.reshape(1, -1), (n_fs, taps.size)), FS, 0, 0, tiled=True
     )
     all_taps = jnp.sum(all_taps.reshape(n_z // 2, 2, n_y, taps.size), axis=(0, 2))
-    all_taps = all_taps.reshape(2, 6, width).transpose(1, 0, 2).reshape(6, width_local)
+    all_taps = all_taps.reshape(2, 6, wide)[..., :width].transpose(1, 0, 2).reshape(6, width_local)
 
     late_gate, late_up = project(late_pair)
     late = (
         jax.nn.gelu(causal_mix(late_gate, gate_filter), approximate=True)
         * causal_mix(late_up, up_filter)
     ).astype(jnp.bfloat16)
-    late_hidden = columns_joined(late[0], swapped(late[1], "zb"))
+    late_hidden = columns_joined(late[0][:, :width], swapped(late[1], "zb")[:, :width])
     return (
         late_hidden,
         early_grad,

time: 291 us -> 195 us (0.67)
  waiting for transfers between devices: 167 us -> 88.3 us
  between operations: 1.16 us -> 14.7 us
  local copies, waits for them, and re-layouts: 28.8 us -> 17.3 us
  starting transfers between devices: 43.1 us -> 32.9 us
  other arithmetic: 19.7 us -> 11.9 us
    all_to_all x2 -> x0, waiting for transfers between devices: 109 us -> none  [the longest x1 70.9 us: per_device(): terms = lax.all_to_all(terms.transpose(1, 0, 2, 3), 'y', 0, 0, tiled=True)]
    all_gather x0 -> x1, waiting for transfers between devices: none -> 15.2 us  [per_device(): weight = lax.all_gather(block, 'y').reshape(n_y, n_z, shard_rows, 2 * wide)]
    all_to_all x2 -> x0, starting transfers between devices: 12.2 us -> none  [the longest x1 7.1 us: per_device(): weight = lax.all_to_all(copies, 'y', 0, 0, tiled=True)]
    all_to_all x1, waiting for transfers between devices: 4 us -> 13.2 us  [per_device(): lax.all_to_all(chip.reshape(2 * n_x, row_count // n_x, cut), ('zb', 'x'),...]
    all_to_all x1, waiting for transfers between devices: 8.88 us -> 16 us  [per_device(): lax.all_to_all(jnp.broadcast_to(taps.reshape(1, -1), (n_fs, taps.size)),...]
    all_to_all x1, waiting for transfers between devices: 0.01 us -> 6.54 us  [per_device(): pieces = lax.all_to_all(reduced, Z, 0, 0, tiled=True)]
    ppermute x5, waiting for transfers between devices: 32.2 us -> 26 us  [swapped(): return lax.ppermute(values, axis, [(0, 1), (1, 0)])]
    all_to_all x1, starting transfers between devices: 3.87 us -> 7.74 us  [per_device(): lax.all_to_all(jnp.broadcast_to(taps.reshape(1, -1), (n_fs, taps.size)),...]
  transfers between devices with their start and end apart: 11 -> 11, of which waited for: 7 -> 7; matrix products, arithmetic and copies ran while one was open for 13% -> 12% of each run, Pallas kernels for 0% -> 0%
where the time goes in v3:
time: 195 us; the launch traced here: 192 us
  waiting for transfers between devices  88.3 us (45%)
  starting transfers between devices  32.9 us (17%)
  blocking collectives  18.8 us (10%)
  local copies, waits for them, and re-layouts  17.3 us (9%)
  between operations  14.7 us (8%)
  other arithmetic  11.9 us (6%)
  matrix products  8.44 us (4%)
    ppermute x5, waiting for transfers between devices, swapped(): return lax.ppermute(values, axis, [(0, 1), (1, 0)])  26 us
    all_to_all x1, blocking collectives, per_device(): block = lax.all_to_all(for_z, Z, 0, 0, tiled=True)  18.8 us
    all_to_all x1, waiting for transfers between devices, per_device(): lax.all_to_all(jnp.broadcast_to(taps.reshape(1, -1), (n_fs, taps.size)),...  16 us
    all_gather x1, waiting for transfers between devices, per_device(): weight = lax.all_gather(block, 'y').reshape(n_y, n_z, shard_rows, 2 * wide)  15.2 us
    all_to_all x1, waiting for transfers between devices, per_device(): lax.all_to_all(chip.reshape(2 * n_x, row_count // n_x, cut), ('zb', 'x'),...  13.2 us
    all_to_all x1, waiting for transfers between devices, per_device(): finished = lax.all_to_all(copies, TP, 0, 0, tiled=True)  11.3 us
    ppermute x5, starting transfers between devices, swapped(): return lax.ppermute(values, axis, [(0, 1), (1, 0)])  10.8 us
    all_to_all x1, starting transfers between devices, per_device(): lax.all_to_all(jnp.broadcast_to(taps.reshape(1, -1), (n_fs, taps.size)),...  7.74 us
  transfers between devices with their start and end apart: 11, of which 7 were waited for; matrix products, arithmetic and copies ran while one was open for 12% of the time, Pallas kernels for 0%

profile of v3, /device:TPU:6, one launch (start us, length us, event | category | flops | bytes accessed | tf_op | source)
XLA Modules:
  0.0 192.4 jit_solution(8071993570860812930)
XLA Ops:
  10.2 18.8 %all_to_all.26 = bf16[4,64,768]{2,1,0:T(8,128)(2,1)} all-to-all(bf16[4,64,768]{2,1,0:T(8,128)(2,1)S(1)} %pad_maximum_fusion.6), channel_id=1, replica_groups=mesh['rep'=2,'zp'=2,'zb'=2,'y'=8,'x'=4,'c'=2] {'zp','zb'}, dimensions={0} | all-to-all | bytes 786432 | tf_op jit(solution)/shard_map/all_to_all | solution.py:126
  29.5 2.1 %collective-permute-start = (bf16[256,2048]{1,0:T(8,128)(2,1)S(1)}, bf16[256,2048]{1,0:T(8,128)(2,1)S(1)}, u32[]{:S(2)}, u32[]{:S(2)}) collective-permute-start(bf16[256,2048]{1,0:T(8,128)(2,1)S(1)} %pad_maximum_fusion.1), channel_id=1, source_target_pairs={{0,64},{64,0},{1,65},{65,1},{2,66},{66,2},{3,67},{67,3},{4,68},{68... | collective-permute-start | bytes 3145736 | tf_op jit(solution)/shard_map/ppermute | solution.py:17
  31.6 23.6 %collective-permute-done = bf16[256,2048]{1,0:T(8,128)(2,1)S(1)} collective-permute-done((bf16[256,2048]{1,0:T(8,128)(2,1)S(1)}, bf16[256,2048]{1,0:T(8,128)(2,1)S(1)}, u32[]{:S(2)}, u32[]{:S(2)}) %collective-permute-start) | collective-permute-done | bytes 1048608 | tf_op jit(solution)/shard_map/ppermute | solution.py:17
  55.2 1.9 collective-permute-start.1
  58.2 2.2 %collective-permute-start.3 = (bf16[256,384]{1,0:T(8,128)(2,1)}, bf16[256,384]{1,0:T(8,128)(2,1)}, u32[]{:S(2)}, u32[]{:S(2)}) collective-permute-start(bf16[256,384]{1,0:T(8,128)(2,1)} %get-tuple-element.79), channel_id=1, source_target_pairs={{0,64},{64,0},{1,65},{65,1},{2,66},{66,2},{3,67},{67,3},{4,68},{68... | collective-permute-start | bytes 589832 | tf_op jit(solution)/shard_map/ppermute | solution.py:17
  63.5 15.2 %all-gather.2.cloned.1.call-done = bf16[8,256,768]{2,1,0:T(8,128)(2,1)} async-done(((bf16[1,256,768]{2,1,0:T(8,128)(2,1)}), bf16[8,256,768]{2,1,0:T(8,128)(2,1)}) %all-gather.2.cloned.1.call-update) | async-done | bytes 3145744 | tf_op jit(solution)/shard_map/all_gather | solution.py:134
  78.6 2.2 %copy.59 = bf16[4,8,64,768]{3,2,1,0:T(8,128)(2,1)S(1)} copy(bf16[4,8,64,768]{3,2,0,1:T(8,128)(2,1)} %bitcast.64) | data formatting | bytes 6291456 | tf_op jit(solution)/shard_map/transpose | solution.py:135
  81.1 1.8 convolution_convert_fusion
  84.4 1.8 fusion.6
  86.9 3.1 %multiply_reduce_fusion = (f32[384]{0:T(512)}, f32[384]{0:T(512)}, f32[384]{0:T(512)}, f32[384]{0:T(512)}, f32[384]{0:T(512)}, /*index=5*/f32[384]{0:T(512)}, f32[2,256,384]{2,1,0:T(8,128)S(1)}, f32[2,256,384]{2,1,0:T(8,128)S(1)}) fusion(f32[2,256,768]{2,1,0:T(8,128)S(1)} %bitcast_convert_fusion, f32[2,256,384]{2,1,0:T(8,128)S(1)} %get-tuple-element.75, ...), kind=kLoop, calls=%fused_computation.38 | loop fusion | flops 9041664 | bytes 5130240 | tf_op jit(solution)/shard_map/reduce_sum | solution.py:56
  91.3 1.9 multiply_convert_fusion
  93.2 2.0 %copy.63 = bf16[4,8,64,768]{3,2,0,1:T(8,128)(2,1)} copy(bf16[4,8,64,768]{3,2,1,0:T(8,128)(2,1)S(1)} %bitcast.68) | data formatting | bytes 6291456 | tf_op jit(solution)/shard_map/reshape | solution.py:161
  95.2 3.0 %fusion.33 = f32[512,2048]{1,0:T(8,128)S(1)} fusion(bf16[512,768]{1,0:T(8,128)(2,1)} %bitcast.77, bf16[2048,768]{1,0:T(8,128)(2,1)S(1)} %bitcast.67), kind=kOutput, calls=%fused_computation.98 | convolution fusion | flops 1610612736 | bytes 8126464 | tf_op jit(solution)/shard_map/dot_general | solution.py:172
  98.4 2.1 %collective-permute-start.4 = (bf16[512,1024]{1,0:T(8,128)(2,1)S(1)}, bf16[512,1024]{1,0:T(8,128)(2,1)S(1)}, u32[]{:S(2)}, u32[]{:S(2)}) collective-permute-start(bf16[512,1024]{1,0:T(8,128)(2,1)S(1)} %select_convert_fusion), channel_id=1, source_target_pairs={{0,1},{1,0},{2,3},{3,2},{4,5},{5,4},{6,7},{7,6},{8,9},{9,8},{10,11... | collective-permute-start | bytes 3145736 | tf_op jit(solution)/shard_map/ppermute | solution.py:17
  100.5 2.4 %collective-permute-done.4 = bf16[512,1024]{1,0:T(8,128)(2,1)S(1)} collective-permute-done((bf16[512,1024]{1,0:T(8,128)(2,1)S(1)}, bf16[512,1024]{1,0:T(8,128)(2,1)S(1)}, u32[]{:S(2)}, u32[]{:S(2)}) %collective-permute-start.4) | collective-permute-done | bytes 1048608 | tf_op jit(solution)/shard_map/ppermute | solution.py:17
  104.8 5.9 %all-to-all-start.1 = ((bf16[8,64,1024]{2,1,0:T(8,128)(2,1)}), bf16[8,64,1024]{2,1,0:T(8,128)(2,1)S(1)}, u32[]{:S(2)}, u32[]{:S(2)}) async-start(bf16[8,64,1024]{2,1,0:T(8,128)(2,1)} %bitcast.19), calls=%async_computation.1 | async-start | bytes 2097152 | tf_op jit(solution)/shard_map/all_to_all | solution.py:181
  110.9 13.2 %all-to-all-done.1 = bf16[8,64,1024]{2,1,0:T(8,128)(2,1)S(1)} async-done(((bf16[8,64,1024]{2,1,0:T(8,128)(2,1)}), bf16[8,64,1024]{2,1,0:T(8,128)(2,1)S(1)}, u32[]{:S(2)}, u32[]{:S(2)}) %all-to-all-start.1) | async-done | bytes 1048608 | tf_op jit(solution)/shard_map/all_to_all | solution.py:181
  124.9 7.7 %all-to-all-start.4 = ((f32[32,1,2304]{2,1,0:T(1,128)}), f32[32,1,2304]{2,1,0:T(1,128)S(1)}, u32[]{:S(2)}, u32[]{:S(2)}) async-start(f32[32,1,2304]{2,1,0:T(1,128)} %broadcast_in_dim.5), calls=%async_computation.5 | async-start | bytes 589824 | tf_op jit(solution)/shard_map/all_to_all | solution.py:194
  132.9 16.0 %all-to-all-done.4 = f32[32,1,2304]{2,1,0:T(1,128)S(1)} async-done(((f32[32,1,2304]{2,1,0:T(1,128)}), f32[32,1,2304]{2,1,0:T(1,128)S(1)}, u32[]{:S(2)}, u32[]{:S(2)}) %all-to-all-start.4) | async-done | bytes 294944 | tf_op jit(solution)/shard_map/all_to_all | solution.py:194
  149.9 5.0 %all-to-all-start.2 = ((bf16[8,64,1024]{2,1,0:T(8,128)(2,1)}), bf16[8,64,1024]{2,1,0:T(8,128)(2,1)S(1)}, u32[]{:S(2)}, u32[]{:S(2)}) async-start(bf16[8,64,1024]{2,1,0:T(8,128)(2,1)} %broadcast_in_dim.4), calls=%async_computation.2 | async-start | bytes 2097152 | tf_op jit(solution)/shard_map/all_to_all | solution.py:186
  155.0 2.5 %collective-permute-start.2 = (bf16[256,384]{1,0:T(8,128)(2,1)S(1)}, bf16[256,384]{1,0:T(8,128)(2,1)S(1)}, u32[]{:S(2)}, u32[]{:S(2)}) collective-permute-start(bf16[256,384]{1,0:T(8,128)(2,1)S(1)} %get-tuple-element.85), channel_id=1, source_target_pairs={{0,64},{64,0},{1,65},{65,1},{2,66},{66,2},{3,67},{67,3},{4,68},{68... | collective-permute-start | bytes 589832 | tf_op jit(solution)/shard_map/ppermute | solution.py:17
  157.5 11.3 %all-to-all-done.2 = bf16[8,64,1024]{2,1,0:T(8,128)(2,1)S(1)} async-done(((bf16[8,64,1024]{2,1,0:T(8,128)(2,1)}), bf16[8,64,1024]{2,1,0:T(8,128)(2,1)S(1)}, u32[]{:S(2)}, u32[]{:S(2)}) %all-to-all-start.2) | async-done | bytes 1048608 | tf_op jit(solution)/shard_map/all_to_all | solution.py:186
  168.8 3.5 %all-to-all-start.3 = ((bf16[4,64,768]{2,1,0:T(8,128)(2,1)}), bf16[4,64,768]{2,1,0:T(8,128)(2,1)S(1)}, u32[]{:S(2)}, u32[]{:S(2)}) async-start(bf16[4,64,768]{2,1,0:T(8,128)(2,1)} %bitcast.79), calls=%async_computation.4 | async-start | bytes 786432 | tf_op jit(solution)/shard_map/all_to_all | solution.py:166
  177.3 6.5 %all-to-all-done.3 = bf16[4,64,768]{2,1,0:T(8,128)(2,1)S(1)} async-done(((bf16[4,64,768]{2,1,0:T(8,128)(2,1)}), bf16[4,64,768]{2,1,0:T(8,128)(2,1)S(1)}, u32[]{:S(2)}, u32[]{:S(2)}) %all-to-all-start.3) | async-done | bytes 393248 | tf_op jit(solution)/shard_map/all_to_all | solution.py:166
  (118 shorter events, 22.0 us)
Async XLA Ops:
  7.2 22.0 %copy-start = (bf16[256,2048]{1,0:T(8,128)(2,1)S(1)}, bf16[256,2048]{1,0:T(8,128)(2,1)}, u32[]{:S(2)}) copy-start(bf16[256,2048]{1,0:T(8,128)(2,1)} %param.11) | copy-start | bytes 3145732
  7.2 22.0 %copy-start.2 = (bf16[256,2048]{1,0:T(8,128)(2,1)S(1)}, bf16[256,2048]{1,0:T(8,128)(2,1)}, u32[]{:S(2)}) copy-start(bf16[256,2048]{1,0:T(8,128)(2,1)} %param.12) | copy-start | bytes 3145732
  7.2 71.4 %all-gather.2.cloned.1.call-start = ((), (), s32[]{:S(2)}) async-start(), calls=%async_computation.6 | async-start | bytes 3538944 | tf_op jit(solution)/shard_map/all_gather | solution.py:134
  29.1 28.0 %slice-start = ((bf16[256,704]{0,1:T(8,128)(2,1)}), bf16[256,384]{0,1:T(8,128)(2,1)S(1)}, s32[]{:S(2)}) async-start(bf16[256,704]{0,1:T(8,128)(2,1)} %param.13), calls=%async_computation.8 | async-start | bytes 393216 | tf_op jit(solution)/shard_map/slice.4
  29.1 139.7 %reduce-scatter.2.cloned.1.call-start = ((), (), s32[]{:S(2)}) async-start(), calls=%async_computation.7 | async-start | bytes 3538944 | tf_op jit(solution)/shard_map/reduce_scatter | solution.py:164
  29.2 28.1 %slice-start.1 = ((bf16[256,704]{0,1:T(8,128)(2,1)}), bf16[256,352]{0,1:T(8,128)(2,1)S(1)}, s32[]{:S(2)}) async-start(bf16[256,704]{0,1:T(8,128)(2,1)} %param.13), calls=%async_computation.9 | async-start | bytes 360448 | tf_op jit(solution)/shard_map/slice | solution.py:96
  29.2 28.2 %copy-start.23 = (pred[384]{0:T(512)(128)(4,1)S(1)}, pred[384]{0:T(512)(128)(4,1)}, u32[]{:S(2)}) copy-start(pred[384]{0:T(512)(128)(4,1)} %constant.27.clone.1) | copy-start | bytes 1156
  29.2 31.2 %copy-start.21 = (bf16[3,704]{1,0:T(4,128)(2,1)S(1)}, bf16[3,704]{1,0:T(4,128)(2,1)}, u32[]{:S(2)}) copy-start(bf16[3,704]{1,0:T(4,128)(2,1)} %param.16) | copy-start | bytes 12676
  29.2 31.3 %copy-start.22 = (bf16[3,704]{1,0:T(4,128)(2,1)S(1)}, bf16[3,704]{1,0:T(4,128)(2,1)}, u32[]{:S(2)}) copy-start(bf16[3,704]{1,0:T(4,128)(2,1)} %param.17) | copy-start | bytes 12676
  29.5 25.7 %collective-permute-start = (bf16[256,2048]{1,0:T(8,128)(2,1)S(1)}, bf16[256,2048]{1,0:T(8,128)(2,1)S(1)}, u32[]{:S(2)}, u32[]{:S(2)}) collective-permute-start(bf16[256,2048]{1,0:T(8,128)(2,1)S(1)} %pad_maximum_fusion.1), channel_id=1, source_target_pairs={{0,64},{64,0},{1,65},{65,1},{2,66},{66,2},{3,67},{67,3},{4,68},{68... | collective-permute-start | bytes 3145736 | tf_op jit(solution)/shard_map/ppermute | solution.py:17
  55.2 6.0 %collective-permute-start.1 = (bf16[256,2048]{1,0:T(8,128)(2,1)S(1)}, bf16[256,2048]{1,0:T(8,128)(2,1)S(1)}, u32[]{:S(2)}, u32[]{:S(2)}) collective-permute-start(bf16[256,2048]{1,0:T(8,128)(2,1)S(1)} %collective-permute-done), channel_id=1, source_target_pairs={{0,1},{1,0},{2,3},{3,2},{4,5},{5,4},{6,7},{7,6},{8,9},{9,8},{10,11... | collective-permute-start | bytes 3145736 | tf_op jit(solution)/shard_map/ppermute | solution.py:17
  58.2 28.2 %collective-permute-start.3 = (bf16[256,384]{1,0:T(8,128)(2,1)}, bf16[256,384]{1,0:T(8,128)(2,1)}, u32[]{:S(2)}, u32[]{:S(2)}) collective-permute-start(bf16[256,384]{1,0:T(8,128)(2,1)} %get-tuple-element.79), channel_id=1, source_target_pairs={{0,64},{64,0},{1,65},{65,1},{2,66},{66,2},{3,67},{67,3},{4,68},{68... | collective-permute-start | bytes 589832 | tf_op jit(solution)/shard_map/ppermute | solution.py:17
  98.4 4.6 %collective-permute-start.4 = (bf16[512,1024]{1,0:T(8,128)(2,1)S(1)}, bf16[512,1024]{1,0:T(8,128)(2,1)S(1)}, u32[]{:S(2)}, u32[]{:S(2)}) collective-permute-start(bf16[512,1024]{1,0:T(8,128)(2,1)S(1)} %select_convert_fusion), channel_id=1, source_target_pairs={{0,1},{1,0},{2,3},{3,2},{4,5},{5,4},{6,7},{7,6},{8,9},{9,8},{10,11... | collective-permute-start | bytes 3145736 | tf_op jit(solution)/shard_map/ppermute | solution.py:17
  103.6 7.1 %copy-start.16 = (f32[384]{0:T(512)S(1)}, f32[384]{0:T(512)}, u32[]{:S(2)}) copy-start(f32[384]{0:T(512)} %get-tuple-element.57) | copy-start | bytes 4612
  103.6 7.1 %copy-start.15 = (f32[384]{0:T(512)S(1)}, f32[384]{0:T(512)}, u32[]{:S(2)}) copy-start(f32[384]{0:T(512)} %get-tuple-element.48) | copy-start | bytes 4612
  104.8 19.3 %all-to-all-start.1 = ((bf16[8,64,1024]{2,1,0:T(8,128)(2,1)}), bf16[8,64,1024]{2,1,0:T(8,128)(2,1)S(1)}, u32[]{:S(2)}, u32[]{:S(2)}) async-start(bf16[8,64,1024]{2,1,0:T(8,128)(2,1)} %bitcast.19), calls=%async_computation.1 | async-start | bytes 2097152 | tf_op jit(solution)/shard_map/all_to_all | solution.py:181
  124.9 23.9 %all-to-all-start.4 = ((f32[32,1,2304]{2,1,0:T(1,128)}), f32[32,1,2304]{2,1,0:T(1,128)S(1)}, u32[]{:S(2)}, u32[]{:S(2)}) async-start(f32[32,1,2304]{2,1,0:T(1,128)} %broadcast_in_dim.5), calls=%async_computation.5 | async-start | bytes 589824 | tf_op jit(solution)/shard_map/all_to_all | solution.py:194
  149.9 23.8 %copy-start.13 = (f32[3,704]{1,0:T(4,128)S(1)}, f32[3,704]{1,0:T(4,128)}, u32[]{:S(2)}) copy-start(f32[3,704]{1,0:T(4,128)} %param.20) | copy-start | bytes 25348
  149.9 24.4 %copy-start.14 = (f32[3,704]{1,0:T(4,128)S(1)}, f32[3,704]{1,0:T(4,128)}, u32[]{:S(2)}) copy-start(f32[3,704]{1,0:T(4,128)} %param.21) | copy-start | bytes 25348
  149.9 18.8 %all-to-all-start.2 = ((bf16[8,64,1024]{2,1,0:T(8,128)(2,1)}), bf16[8,64,1024]{2,1,0:T(8,128)(2,1)S(1)}, u32[]{:S(2)}, u32[]{:S(2)}) async-start(bf16[8,64,1024]{2,1,0:T(8,128)(2,1)} %broadcast_in_dim.4), calls=%async_computation.2 | async-start | bytes 2097152 | tf_op jit(solution)/shard_map/all_to_all | solution.py:186
  155.0 17.3 %collective-permute-start.2 = (bf16[256,384]{1,0:T(8,128)(2,1)S(1)}, bf16[256,384]{1,0:T(8,128)(2,1)S(1)}, u32[]{:S(2)}, u32[]{:S(2)}) collective-permute-start(bf16[256,384]{1,0:T(8,128)(2,1)S(1)} %get-tuple-element.85), channel_id=1, source_target_pairs={{0,64},{64,0},{1,65},{65,1},{2,66},{66,2},{3,67},{67,3},{4,68},{68... | collective-permute-start | bytes 589832 | tf_op jit(solution)/shard_map/ppermute | solution.py:17
  168.8 15.1 %all-to-all-start.3 = ((bf16[4,64,768]{2,1,0:T(8,128)(2,1)}), bf16[4,64,768]{2,1,0:T(8,128)(2,1)S(1)}, u32[]{:S(2)}, u32[]{:S(2)}) async-start(bf16[4,64,768]{2,1,0:T(8,128)(2,1)} %bitcast.79), calls=%async_computation.4 | async-start | bytes 786432 | tf_op jit(solution)/shard_map/all_to_all | solution.py:166
  173.5 10.5 %copy-start.9 = (f32[64,704]{1,0:T(8,128)S(1)}, f32[64,704]{1,0:T(8,128)}, u32[]{:S(2)}) copy-start(f32[64,704]{1,0:T(8,128)} %param.18) | copy-start | bytes 540676
  175.0 9.8 %copy-start.10 = (f32[64,704]{1,0:T(8,128)S(1)}, f32[64,704]{1,0:T(8,128)}, u32[]{:S(2)}) copy-start(f32[64,704]{1,0:T(8,128)} %param.19) | copy-start | bytes 540676
  (13 other events, 42.8 us)
Sparse Core Ops, SparseCore 0:
  29.2 49.3 all-gather.1
  95.4 53.7 reduce-scatter.1

commit v4 on v3

v4 whole, which is shorter than its diff:
```python
import functools
import math

import jax
import jax.numpy as jnp
from jax import lax
from jax.experimental import pallas as pl
from jax.experimental.pallas import tpu as pltpu
from jax.sharding import Mesh
from jax.sharding import PartitionSpec as P

Z = ("zp", "zb")
FS = ("zp", "zb", "y")
REP_FS = ("rep", "zp", "zb", "y")
TP = ("x", "c")

contract_last = (((1,), (1,)), ((), ()))
contract_first = (((0,), (0,)), ((), ()))


def swapped(values, axis):
    return lax.ppermute(values, axis, [(0, 1), (1, 0)])


def pick(flag, first, second):
    return jnp.where(flag, first, second)


def causal_mix(values, filter_taps):
    length = values.shape[-2]
    widths = [(0, 0)] * values.ndim
    widths[-2] = (2, 0)
    padded = jnp.pad(values, widths)
    return (
        filter_taps[0] * padded[..., 0:length, :]
        + filter_taps[1] * padded[..., 1 : length + 1, :]
        + filter_taps[2] * padded[..., 2 : length + 2, :]
    )


def moved(values, by):
    length = values.shape[0]
    at = lax.broadcasted_iota(jnp.int32, values.shape, 0)
    turned = pltpu.roll(values, by % length, 0)
    inside = at >= by if by > 0 else at < length + by
    return jnp.where(inside, turned, 0.0)


def early_kernel(
    scale, gathered, own, other, cotangent, filters, weight, grads, terms, tap_sums
):
    n_y, n_z, shard_rows, columns = gathered.shape
    length, depth = own.shape
    wide = columns // 2
    span = n_y * shard_rows
    for z in range(n_z):
        for y in range(n_y):
            at = z * span + y * shard_rows
            weight[at : at + shard_rows, :] = gathered[y, z]
    first, second, third = filters[0:1, :], filters[1:2, :], filters[2:3, :]
    slope = math.sqrt(2.0 / math.pi)
    sums = [jnp.zeros((1, columns), jnp.float32) for _ in range(3)]
    for part, rows in enumerate((own, other)):
        pre = jnp.dot(rows[...], weight[...], preferred_element_type=jnp.float32)
        pre = pre.astype(jnp.bfloat16).astype(jnp.float32)
        one_back, two_back = moved(pre, 1), moved(pre, 2)
        mixed = first * two_back + second * one_back + third * pre
        gate, up = mixed[:, :wide], mixed[:, wide:]
        square = gate * gate
        bend = jnp.tanh(slope * (gate + 0.044715 * (square * gate)))
        side = 0.5 * (1.0 + bend)
        active = gate * side
        rise = side + 0.5 * gate * (1.0 - bend * bend) * (
            slope * (1.0 + (3 * 0.044715) * square)
        )
        given = cotangent[part].astype(jnp.float32)
        back = jnp.concatenate([given * up * rise, given * active], axis=1)
        for tap, source in enumerate((two_back, one_back, pre)):
            sums[tap] = sums[tap] + jnp.sum(back * source, axis=0, keepdims=True)
        full = third * back + second * moved(back, -1) + first * moved(back, -2)
        grads[part * length : (part + 1) * length, :] = full.astype(jnp.bfloat16)
    tap_sums[...] = jnp.concatenate(
        [scale * value for value in sums]
        + [jnp.zeros((tap_sums.shape[0] - 3, columns), jnp.float32)]
    )
    for z in range(n_z):
        term = sum(
            lax.dot_general(
                rows[:, z * span : (z + 1) * span],
                grads[part * length : (part + 1) * length, :],
                contract_first,
                preferred_element_type=jnp.float32,
            )
            for part, rows in enumerate((own, other))
        )
        term = (term * scale).astype(jnp.bfloat16)
        for y in range(n_y):
            terms[y, z] = term[y * shard_rows : (y + 1) * shard_rows, :]


def early_pass(scale, gathered, own, other, cotangent, filters):
    n_y, n_z, shard_rows, columns = gathered.shape
    length, depth = own.shape
    whole = pl.BlockSpec(memory_space=pltpu.VMEM)
    return pl.pallas_call(
        functools.partial(early_kernel, scale),
        out_shape=(
            jax.ShapeDtypeStruct((depth, columns), jnp.bfloat16),
            jax.ShapeDtypeStruct((2 * length, columns), jnp.bfloat16),
            jax.ShapeDtypeStruct(gathered.shape, jnp.bfloat16),
            jax.ShapeDtypeStruct((8, columns), jnp.float32),
        ),
        in_specs=[whole] * 5,
        out_specs=(whole,) * 4,
        compiler_params=pltpu.CompilerParams(vmem_limit_bytes=48 * 1024 * 1024),
        cost_estimate=pl.CostEstimate(
            flops=8 * length * depth * columns,
            bytes_accessed=6 * depth * columns + 4 * length * depth,
            transcendentals=length * columns,
        ),
        name="early_pass",
    )(gathered, own, other, cotangent, filters)


def stored(product):
    return lax.optimization_barrier(product.astype(jnp.bfloat16)).astype(jnp.float32)


def per_device(
    late_rows,
    early_rows,
    hidden_cot,
    gate_weight,
    up_weight,
    gate_taps,
    up_taps,
    gate_grad_sum,
    up_grad_sum,
    gate_taps_sum,
    up_taps_sum,
):
    row_count, depth = late_rows.shape
    shard_rows, width_local = gate_weight.shape
    width = width_local // 2
    wide = -(-width // 128) * 128
    n_z = lax.axis_size("zp") * lax.axis_size("zb")
    n_y = lax.axis_size("y")
    n_x = lax.axis_size("x")
    zb = lax.axis_index("zb")
    first_z = zb == 0
    first_c = lax.axis_index("c") == 0
    rows_scale = (row_count * n_z * n_y) ** (-0.5)

    def widened(array):
        edges = [(0, 0)] * (array.ndim - 1)
        return jnp.pad(array, edges + [(0, wide - width)])

    def halves(array):
        low, high = widened(array[..., :width]), widened(array[..., width:])
        return pick(first_z, low, high), pick(first_z, high, low)

    def columns_joined(mine, other):
        return pick(
            first_z,
            jnp.concatenate([mine, other], axis=-1),
            jnp.concatenate([other, mine], axis=-1),
        )

    def partners(late, early):
        cut = row_count // 2
        sent = jnp.concatenate(
            [pick(first_c, rows[:cut], rows[cut:]) for rows in (early, late)]
        )
        here = swapped(sent, "zb")
        there = swapped(here, "c")
        low, high = pick(first_c, here, there), pick(first_c, there, here)
        return (
            jnp.concatenate([low[cut:], high[cut:]]),
            jnp.concatenate([low[:cut], high[:cut]]),
        )

    gate_mine, gate_other = halves(gate_weight)
    up_mine, up_other = halves(up_weight)
    weight_mine = jnp.concatenate([gate_mine, up_mine], axis=1)
    weight_other = jnp.concatenate([gate_other, up_other], axis=1)
    for_z = jnp.stack(
        [pick(first_z, weight_mine, weight_other), pick(first_z, weight_other, weight_mine)] * 2
    )
    block = lax.all_to_all(for_z, Z, 0, 0, tiled=True)
    late_other, early_other = partners(late_rows, early_rows)
    cot_mine, cot_other = halves(hidden_cot)
    cotangent = jnp.stack([cot_mine, swapped(cot_other, "zb")])
    filters = jnp.concatenate([halves(gate_taps)[0], halves(up_taps)[0]], axis=1)
    filters = jnp.pad(filters.astype(jnp.float32), [(0, 5), (0, 0)])

    block = block.reshape(n_z * shard_rows, 2 * wide)
    weight = lax.all_gather(block, "y").reshape(n_y, n_z, shard_rows, 2 * wide)
    weight, both_grads, terms, taps = early_pass(
        rows_scale, weight, early_rows, early_other, cotangent, filters
    )
    terms = terms.reshape(depth, 2 * wide)
    reduced = lax.psum_scatter(terms, "y", scatter_dimension=0, tiled=True)
    reduced = reduced.reshape(n_z, shard_rows, 2 * wide)
    partial = lax.dot_general(
        both_grads, weight, contract_last, preferred_element_type=jnp.float32
    )
    cut = depth // 2
    kept = pick(first_c, partial[:, :cut], partial[:, cut:])
    given = pick(first_c, partial[:, cut:], partial[:, :cut]).astype(jnp.bfloat16)
    chip = (kept + swapped(given, "c").astype(jnp.float32)).astype(jnp.bfloat16)
    chip = chip.reshape(2, n_x, row_count // n_x, cut)
    chip = jnp.stack([pick(first_z, chip[0], chip[1]), pick(first_z, chip[1], chip[0])])
    spread = lax.all_to_all(
        chip.reshape(2 * n_x, row_count // n_x, cut), ("zb", "x"), 0, 0, tiled=True
    )
    own = jnp.sum(spread.astype(jnp.float32), axis=0).astype(jnp.bfloat16)
    copies = jnp.broadcast_to(own[None], (2 * n_x, *own.shape))
    finished = lax.all_to_all(copies, TP, 0, 0, tiled=True)
    for step in (1, 2, 4):
        taps = taps + lax.ppermute(taps, "y", [(k, k ^ step) for k in range(n_y)])
    taps = taps + swapped(taps, "zp")
    gate_taps_mine, up_taps_mine = taps[:3, :width], taps[:3, wide : wide + width]
    taps = swapped(taps, "zb")
    gate_tap_sums = columns_joined(gate_taps_mine, taps[:3, :width])
    up_tap_sums = columns_joined(up_taps_mine, taps[:3, wide : wide + width])

    product = [
        stored(jnp.dot(rows, weight, preferred_element_type=jnp.float32))
        for rows in (late_rows, late_other)
    ]
    mixed = [causal_mix(values, filters) for values in product]
    late = [
        (jax.nn.gelu(values[:, :wide], approximate=True) * values[:, wide:]).astype(
            jnp.bfloat16
        )
        for values in mixed
    ]
    late_hidden = columns_joined(late[0][:, :width], swapped(late[1], "zb")[:, :width])

    reduced, finished = lax.optimization_barrier((reduced, finished))
    pieces = lax.all_to_all(reduced, Z, 0, 0, tiled=True)
    pieces = pieces.reshape(2, 2, shard_rows, 2 * wide).astype(jnp.float32)
    pieces = jnp.sum(pieces, axis=0)
    gate_sum = jnp.concatenate([pieces[0, :, :width], pieces[1, :, :width]], axis=1)
    up_sum = jnp.concatenate([pieces[0, :, wide : wide + width], pieces[1, :, wide : wide + width]], axis=1)

    finished = finished.reshape(n_x, 2, row_count // n_x, cut)
    early_grad = finished.transpose(0, 2, 1, 3).reshape(row_count, depth)
    return (
        late_hidden,
        early_grad,
        gate_grad_sum + gate_sum,
        up_grad_sum + up_sum,
        gate_taps_sum + gate_tap_sums,
        up_taps_sum + up_tap_sums,
    )


def solution(mesh):
    split = Mesh(
        mesh.devices.reshape(mesh.shape["rep"], 2, 2, 8, 4, 2),
        ("rep", "zp", "zb", "y", "x", "c"),
    )
    placed = (
        P(REP_FS, None),
        P(REP_FS, None),
        P(REP_FS, TP),
        P(FS, TP),
        P(FS, TP),
        P(None, TP),
        P(None, TP),
        P(REP_FS, TP),
        P(REP_FS, TP),
        P("rep", TP),
        P("rep", TP),
    )
    return jax.shard_map(
        per_device,
        mesh=split,
        in_specs=placed,
        out_specs=(
            P(REP_FS, TP),
            P(REP_FS, None),
            P(REP_FS, TP),
            P(REP_FS, TP),
            P("rep", TP),
            P("rep", TP),
        ),
        check_vma=False,
    )
```

time: 195 us -> 174 us (0.89); the launches traced: 192 us -> 173 us
  waiting for transfers between devices: 88.3 us -> 58.5 us
  starting transfers between devices: 32.9 us -> 47.1 us
  local copies, waits for them, and re-layouts: 17.3 us -> 7.83 us
  Pallas kernels: 0 us -> 9.36 us
  other arithmetic: 11.9 us -> 9.07 us
    all_to_all x1 -> x0, waiting for transfers between devices: 16 us -> none  [per_device(): lax.all_to_all(jnp.broadcast_to(taps.reshape(1, -1), (n_fs, taps.size)),...]
    ppermute x0 -> x3, starting transfers between devices: none -> 12.1 us  [per_device(): taps = taps + lax.ppermute(taps, 'y', [(k, k ^ step) for k in range(n_y)])]
    all_to_all x1, waiting for transfers between devices: 11.3 us -> 0.01 us  [per_device(): finished = lax.all_to_all(copies, TP, 0, 0, tiled=True)]
    pallas_call x0 -> x1, Pallas kernels: none -> 9.36 us  [early_pass(): pl.pallas_call(functools.partial(early_kernel, scale), out_shape=(jax.Sha...]
    ppermute x5 -> x7, starting transfers between devices: 10.8 us -> 19.6 us  [swapped(): return lax.ppermute(values, axis, [(0, 1), (1, 0)])]
    ppermute x5 -> x7, waiting for transfers between devices: 26 us -> 34.8 us  [swapped(): return lax.ppermute(values, axis, [(0, 1), (1, 0)])]
    all_to_all x1 -> x0, starting transfers between devices: 7.74 us -> none  [per_device(): lax.all_to_all(jnp.broadcast_to(taps.reshape(1, -1), (n_fs, taps.size)),...]
    all_to_all x1, waiting for transfers between devices: 13.2 us -> 5.63 us  [per_device(): lax.all_to_all(chip.reshape(2 * n_x, row_count // n_x, cut), ('zb', 'x'),...]
  transfers between devices with their start and end apart: 11 -> 15, of which waited for: 7 -> 9; matrix products, arithmetic and copies ran while one was open for 12% -> 12% of each run, Pallas kernels for 0% -> 0%
where the time goes in v4:
time: 174 us; the launch traced here: 173 us
  waiting for transfers between devices  58.5 us (34%)
  starting transfers between devices  47.1 us (27%)
  blocking collectives  18.8 us (11%)
  between operations  14.6 us (8%)
  Pallas kernels  9.36 us (5%)
  other arithmetic  9.07 us (5%)
  matrix products  8.15 us (5%)
  local copies, waits for them, and re-layouts  7.83 us (4%)
    ppermute x7, waiting for transfers between devices, swapped(): return lax.ppermute(values, axis, [(0, 1), (1, 0)])  34.8 us
    ppermute x7, starting transfers between devices, swapped(): return lax.ppermute(values, axis, [(0, 1), (1, 0)])  19.6 us
    all_to_all x1, blocking collectives, per_device(): block = lax.all_to_all(for_z, Z, 0, 0, tiled=True)  18.8 us
    ppermute x3, starting transfers between devices, per_device(): taps = taps + lax.ppermute(taps, 'y', [(k, k ^ step) for k in range(n_y)])  12.1 us
    pallas_call x1, Pallas kernels, early_pass(): pl.pallas_call(functools.partial(early_kernel, scale), out_shape=(jax.Sha...  9.36 us
    all_gather x1, waiting for transfers between devices, per_device(): weight = lax.all_gather(block, 'y').reshape(n_y, n_z, shard_rows, 2 * wide)  8.58 us
    all_to_all x1, starting transfers between devices, per_device(): lax.all_to_all(chip.reshape(2 * n_x, row_count // n_x, cut), ('zb', 'x'),...  5.88 us
    all_to_all x1, waiting for transfers between devices, per_device(): lax.all_to_all(chip.reshape(2 * n_x, row_count // n_x, cut), ('zb', 'x'),...  5.63 us
  transfers between devices with their start and end apart: 15, of which 9 were waited for; matrix products, arithmetic and copies ran while one was open for 12% of the time, Pallas kernels for 0%

profile of v4, /device:TPU:6, one launch (start us, length us, event | category | flops | bytes accessed | tf_op | source)
XLA Modules:
  0.0 173.5 jit_solution(324105333935805252)
XLA Ops:
  10.2 18.8 %all_to_all.20 = bf16[4,64,768]{2,1,0:T(8,128)(2,1)} all-to-all(bf16[4,64,768]{2,1,0:T(8,128)(2,1)S(1)} %pad_maximum_fusion.3), channel_id=1, replica_groups=mesh['rep'=2,'zp'=2,'zb'=2,'y'=8,'x'=4,'c'=2] {'zp','zb'}, dimensions={0} | all-to-all | bytes 786432 | tf_op jit(solution)/shard_map/all_to_all | solution.py:189
  29.4 2.1 %collective-permute-start = (bf16[256,2048]{1,0:T(8,128)(2,1)S(1)}, bf16[256,2048]{1,0:T(8,128)(2,1)S(1)}, u32[]{:S(2)}, u32[]{:S(2)}) collective-permute-start(bf16[256,2048]{1,0:T(8,128)(2,1)S(1)} %pad_maximum_fusion), channel_id=1, source_target_pairs={{0,64},{64,0},{1,65},{65,1},{2,66},{66,2},{3,67},{67,3},{4,68},{68... | collective-permute-start | bytes 3145736 | tf_op jit(solution)/shard_map/ppermute | solution.py:22
  31.6 23.6 %collective-permute-done = bf16[256,2048]{1,0:T(8,128)(2,1)S(1)} collective-permute-done((bf16[256,2048]{1,0:T(8,128)(2,1)S(1)}, bf16[256,2048]{1,0:T(8,128)(2,1)S(1)}, u32[]{:S(2)}, u32[]{:S(2)}) %collective-permute-start) | collective-permute-done | bytes 1048608 | tf_op jit(solution)/shard_map/ppermute | solution.py:22
  55.2 1.9 %collective-permute-start.1 = (bf16[256,2048]{1,0:T(8,128)(2,1)S(1)}, bf16[256,2048]{1,0:T(8,128)(2,1)}, u32[]{:S(2)}, u32[]{:S(2)}) collective-permute-start(bf16[256,2048]{1,0:T(8,128)(2,1)S(1)} %collective-permute-done), channel_id=1, source_target_pairs={{0,1},{1,0},{2,3},{3,2},{4,5},{5,4},{6,7},{7,6},{8,9},{9,8},{10,11... | collective-permute-start | bytes 3145736 | tf_op jit(solution)/shard_map/ppermute | solution.py:22
  57.5 2.2 %collective-permute-start.2 = (bf16[256,384]{1,0:T(8,128)(2,1)S(1)}, bf16[256,384]{1,0:T(8,128)(2,1)S(1)}, u32[]{:S(2)}, u32[]{:S(2)}) collective-permute-start(bf16[256,384]{1,0:T(8,128)(2,1)S(1)} %get-tuple-element.33), channel_id=1, source_target_pairs={{0,64},{64,0},{1,65},{65,1},{2,66},{66,2},{3,67},{67,3},{4,68},{68... | collective-permute-start | bytes 589832 | tf_op jit(solution)/shard_map/ppermute | solution.py:22
  60.0 6.8 %collective-permute-done.2 = bf16[256,384]{1,0:T(8,128)(2,1)S(1)} collective-permute-done((bf16[256,384]{1,0:T(8,128)(2,1)S(1)}, bf16[256,384]{1,0:T(8,128)(2,1)S(1)}, u32[]{:S(2)}, u32[]{:S(2)}) %collective-permute-start.2) | collective-permute-done | bytes 196640 | tf_op jit(solution)/shard_map/ppermute | solution.py:22
  70.0 8.6 %all-gather.2.cloned.1.call-done = bf16[8,256,768]{2,1,0:T(8,128)(2,1)} async-done(((bf16[1,256,768]{2,1,0:T(8,128)(2,1)}), bf16[8,256,768]{2,1,0:T(8,128)(2,1)}) %all-gather.2.cloned.1.call-update) | async-done | bytes 3145744 | tf_op jit(solution)/shard_map/all_gather | solution.py:197
  78.6 9.4 %early_pass.1 = (bf16[2048,768]{1,0:T(8,128)(2,1)}, bf16[512,768]{1,0:T(8,128)(2,1)S(1)}, bf16[8,4,64,768]{3,2,1,0:T(8,128)(2,1)}, f32[8,768]{1,0:T(8,128)S(1)}) custom-call(bf16[8,4,64,768]{3,2,1,0:T(8,128)(2,1)} %bitcast.51, bf16[256,2048]{1,0:T(8,128)(2,1)S(1)} %copy-done, bf16[256,2048]{1,0:T(8,128)(2,1)S(1)} %pad_maximum_fusion.1.other, ...), custom_call_target="tpu_custom_call" | custom-call | flops 3221225472 | bytes 11534336 | tf_op jit(solution)/shard_map/early_pass/pallas_call | solution.py:105
  88.0 3.7 %fusion.34 = f32[512,2048]{1,0:T(8,128)S(1)} fusion(bf16[512,768]{1,0:T(8,128)(2,1)S(1)} %get-tuple-element.14, bf16[2048,768]{1,0:T(8,128)(2,1)} %get-tuple-element.12), kind=kOutput, calls=%fused_computation.87 | convolution fusion | flops 1610612736 | bytes 8126464 | tf_op jit(solution)/shard_map/dot_general | solution.py:204
  91.9 1.9 %collective-permute-start.4 = (bf16[512,1024]{1,0:T(8,128)(2,1)S(1)}, bf16[512,1024]{1,0:T(8,128)(2,1)S(1)}, u32[]{:S(2)}, u32[]{:S(2)}) collective-permute-start(bf16[512,1024]{1,0:T(8,128)(2,1)S(1)} %select_convert_fusion), channel_id=1, source_target_pairs={{0,1},{1,0},{2,3},{3,2},{4,5},{5,4},{6,7},{7,6},{8,9},{9,8},{10,11... | collective-permute-start | bytes 3145736 | tf_op jit(solution)/shard_map/ppermute | solution.py:22
  93.9 2.6 %collective-permute-done.4 = bf16[512,1024]{1,0:T(8,128)(2,1)S(1)} collective-permute-done((bf16[512,1024]{1,0:T(8,128)(2,1)S(1)}, bf16[512,1024]{1,0:T(8,128)(2,1)S(1)}, u32[]{:S(2)}, u32[]{:S(2)}) %collective-permute-start.4) | collective-permute-done | bytes 1048608 | tf_op jit(solution)/shard_map/ppermute | solution.py:22
  98.3 5.9 %all-to-all-start.1 = ((bf16[8,64,1024]{2,1,0:T(8,128)(2,1)}), bf16[8,64,1024]{2,1,0:T(8,128)(2,1)S(1)}, u32[]{:S(2)}, u32[]{:S(2)}) async-start(bf16[8,64,1024]{2,1,0:T(8,128)(2,1)} %bitcast.13), calls=%async_computation.2 | async-start | bytes 2097152 | tf_op jit(solution)/shard_map/all_to_all | solution.py:213
  104.2 3.4 %convolution_convert_fusion = bf16[256,768]{0,1:T(8,128)(2,1)S(1)} fusion(bf16[2048,768]{1,0:T(8,128)(2,1)} %get-tuple-element.12, bf16[128,2048]{1,0:T(8,128)(2,1)S(1)} %copy-done.4, bf16[128,2048]{1,0:T(8,128)(2,1)S(1)} %copy-done.3), kind=kOutput, calls=%fused_computation.6 | convolution fusion | flops 807600128 | bytes 4587520 | tf_op jit(solution)/shard_map/dot_general | solution.py:228
  107.7 3.1 %collective-permute-start.5 = (f32[8,768]{1,0:T(8,128)S(1)}, f32[8,768]{1,0:T(8,128)S(1)}, u32[]{:S(2)}, u32[]{:S(2)}) collective-permute-start(f32[8,768]{1,0:T(8,128)S(1)} %get-tuple-element.17), channel_id=1, source_target_pairs={{0,8},{8,0},{16,24},{24,16},{32,40},{40,32},{48,56},{56,48},{1,9},... | collective-permute-start | bytes 73736 | tf_op jit(solution)/shard_map/ppermute | solution.py:220
  111.9 5.6 %all-to-all-done.1 = bf16[8,64,1024]{2,1,0:T(8,128)(2,1)S(1)} async-done(((bf16[8,64,1024]{2,1,0:T(8,128)(2,1)}), bf16[8,64,1024]{2,1,0:T(8,128)(2,1)S(1)}, u32[]{:S(2)}, u32[]{:S(2)}) %all-to-all-start.1) | async-done | bytes 1048608 | tf_op jit(solution)/shard_map/all_to_all | solution.py:213
  118.8 5.2 %all-to-all-start.2 = ((bf16[8,64,1024]{2,1,0:T(8,128)(2,1)}), bf16[8,64,1024]{2,1,0:T(8,128)(2,1)S(1)}, u32[]{:S(2)}, u32[]{:S(2)}) async-start(bf16[8,64,1024]{2,1,0:T(8,128)(2,1)} %broadcast_in_dim.2), calls=%async_computation.3 | async-start | bytes 2097152 | tf_op jit(solution)/shard_map/all_to_all | solution.py:218
  125.3 3.8 %collective-permute-start.6 = (f32[8,768]{1,0:T(8,128)S(1)}, f32[8,768]{1,0:T(8,128)S(1)}, u32[]{:S(2)}, u32[]{:S(2)}) collective-permute-start(f32[8,768]{1,0:T(8,128)S(1)} %add.80), channel_id=1, source_target_pairs={{0,16},{8,24},{16,0},{24,8},{32,48},{40,56},{48,32},{56,40},{1,17}... | collective-permute-start | bytes 73736 | tf_op jit(solution)/shard_map/ppermute | solution.py:220
  129.3 3.4 %collective-permute-start.3 = (bf16[256,384]{0,1:T(8,128)(2,1)S(1)}, bf16[256,384]{0,1:T(8,128)(2,1)S(1)}, u32[]{:S(2)}, u32[]{:S(2)}) collective-permute-start(bf16[256,384]{0,1:T(8,128)(2,1)S(1)} %fusion.23), channel_id=1, source_target_pairs={{0,64},{64,0},{1,65},{65,1},{2,66},{66,2},{3,67},{67,3},{4,68},{68... | collective-permute-start | bytes 589832 | tf_op jit(solution)/shard_map/ppermute | solution.py:22
  132.8 5.1 %collective-permute-start.7 = (f32[8,768]{1,0:T(8,128)S(1)}, f32[8,768]{1,0:T(8,128)S(1)}, u32[]{:S(2)}, u32[]{:S(2)}) collective-permute-start(f32[8,768]{1,0:T(8,128)S(1)} %add.81), channel_id=1, source_target_pairs={{0,32},{8,40},{16,48},{24,56},{32,0},{40,8},{48,16},{56,24},{1,33}... | collective-permute-start | bytes 73736 | tf_op jit(solution)/shard_map/ppermute | solution.py:220
  138.1 4.4 %collective-permute-done.7 = f32[8,768]{1,0:T(8,128)S(1)} collective-permute-done((f32[8,768]{1,0:T(8,128)S(1)}, f32[8,768]{1,0:T(8,128)S(1)}, u32[]{:S(2)}, u32[]{:S(2)}) %collective-permute-start.7) | collective-permute-done | bytes 24608 | tf_op jit(solution)/shard_map/ppermute | solution.py:220
  142.5 4.7 %collective-permute-start.8 = (f32[8,768]{1,0:T(8,128)S(1)}, f32[8,768]{1,0:T(8,128)S(1)}, u32[]{:S(2)}, u32[]{:S(2)}) collective-permute-start(f32[8,768]{1,0:T(8,128)S(1)} %add.82), channel_id=1, source_target_pairs={{0,128},{128,0},{1,129},{129,1},{2,130},{130,2},{3,131},{131,3},{4... | collective-permute-start | bytes 73736 | tf_op jit(solution)/shard_map/ppermute | solution.py:22
  149.1 3.4 %collective-permute-start.9 = (f32[8,768]{1,0:T(8,128)S(1)}, f32[8,768]{1,0:T(8,128)S(1)}, u32[]{:S(2)}, u32[]{:S(2)}) collective-permute-start(f32[8,768]{1,0:T(8,128)S(1)} %add.83), channel_id=1, source_target_pairs={{0,64},{64,0},{1,65},{65,1},{2,66},{66,2},{3,67},{67,3},{4,68},{68... | collective-permute-start | bytes 73736 | tf_op jit(solution)/shard_map/ppermute | solution.py:22
  152.5 4.2 %all-to-all-start.3 = ((bf16[4,64,768]{2,1,0:T(8,128)(2,1)}), bf16[4,64,768]{2,1,0:T(8,128)(2,1)S(1)}, u32[]{:S(2)}, u32[]{:S(2)}) async-start(bf16[4,64,768]{2,1,0:T(8,128)(2,1)} %bitcast.49), calls=%async_computation.4 | async-start | bytes 786432 | tf_op jit(solution)/shard_map/all_to_all | solution.py:241
  160.8 4.9 %all-to-all-done.3 = bf16[4,64,768]{2,1,0:T(8,128)(2,1)S(1)} async-done(((bf16[4,64,768]{2,1,0:T(8,128)(2,1)}), bf16[4,64,768]{2,1,0:T(8,128)(2,1)S(1)}, u32[]{:S(2)}, u32[]{:S(2)}) %all-to-all-start.3) | async-done | bytes 393248 | tf_op jit(solution)/shard_map/all_to_all | solution.py:241
  (91 shorter events, 20.1 us)
Async XLA Ops:
  7.2 22.0 %copy-start.1 = (bf16[256,2048]{1,0:T(8,128)(2,1)S(1)}, bf16[256,2048]{1,0:T(8,128)(2,1)}, u32[]{:S(2)}) copy-start(bf16[256,2048]{1,0:T(8,128)(2,1)} %param.11) | copy-start | bytes 3145732
  7.2 22.1 %copy-start = (bf16[256,2048]{1,0:T(8,128)(2,1)S(1)}, bf16[256,2048]{1,0:T(8,128)(2,1)}, u32[]{:S(2)}) copy-start(bf16[256,2048]{1,0:T(8,128)(2,1)} %own.1) | copy-start | bytes 3145732
  7.2 71.4 %all-gather.2.cloned.1.call-start = ((), (), s32[]{:S(2)}) async-start(), calls=%async_computation.5 | async-start | bytes 3538944 | tf_op jit(solution)/shard_map/all_gather | solution.py:197
  29.1 28.0 %slice-start = ((bf16[256,704]{0,1:T(8,128)(2,1)}), bf16[256,352]{0,1:T(8,128)(2,1)S(1)}, s32[]{:S(2)}) async-start(bf16[256,704]{0,1:T(8,128)(2,1)} %param.13), calls=%async_computation.7 | async-start | bytes 360448 | tf_op jit(solution)/shard_map/slice | solution.py:159
  29.1 123.4 %reduce-scatter.2.cloned.1.call-start = ((), (), s32[]{:S(2)}) async-start(), calls=%async_computation.6 | async-start | bytes 3538944 | tf_op jit(solution)/shard_map/reduce_scatter | solution.py:202
  29.2 28.1 %slice-start.1 = ((bf16[256,704]{0,1:T(8,128)(2,1)}), bf16[256,384]{0,1:T(8,128)(2,1)S(1)}, s32[]{:S(2)}) async-start(bf16[256,704]{0,1:T(8,128)(2,1)} %param.13), calls=%async_computation.8 | async-start | bytes 393216 | tf_op jit(solution)/shard_map/slice.5
  29.2 28.2 %copy-start.11 = (pred[384]{0:T(512)(128)(4,1)S(1)}, pred[384]{0:T(512)(128)(4,1)}, u32[]{:S(2)}) copy-start(pred[384]{0:T(512)(128)(4,1)} %constant.23.clone.1) | copy-start | bytes 1156
  29.3 30.5 %copy-start.9 = (bf16[3,704]{1,0:T(4,128)(2,1)S(1)}, bf16[3,704]{1,0:T(4,128)(2,1)}, u32[]{:S(2)}) copy-start(bf16[3,704]{1,0:T(4,128)(2,1)} %param.16) | copy-start | bytes 12676
  29.3 30.5 %copy-start.10 = (bf16[3,704]{1,0:T(4,128)(2,1)S(1)}, bf16[3,704]{1,0:T(4,128)(2,1)}, u32[]{:S(2)}) copy-start(bf16[3,704]{1,0:T(4,128)(2,1)} %param.17) | copy-start | bytes 12676
  29.4 25.7 %collective-permute-start = (bf16[256,2048]{1,0:T(8,128)(2,1)S(1)}, bf16[256,2048]{1,0:T(8,128)(2,1)S(1)}, u32[]{:S(2)}, u32[]{:S(2)}) collective-permute-start(bf16[256,2048]{1,0:T(8,128)(2,1)S(1)} %pad_maximum_fusion), channel_id=1, source_target_pairs={{0,64},{64,0},{1,65},{65,1},{2,66},{66,2},{3,67},{67,3},{4,68},{68... | collective-permute-start | bytes 3145736 | tf_op jit(solution)/shard_map/ppermute | solution.py:22
  55.2 11.6 %collective-permute-start.1 = (bf16[256,2048]{1,0:T(8,128)(2,1)S(1)}, bf16[256,2048]{1,0:T(8,128)(2,1)}, u32[]{:S(2)}, u32[]{:S(2)}) collective-permute-start(bf16[256,2048]{1,0:T(8,128)(2,1)S(1)} %collective-permute-done), channel_id=1, source_target_pairs={{0,1},{1,0},{2,3},{3,2},{4,5},{5,4},{6,7},{7,6},{8,9},{9,8},{10,11... | collective-permute-start | bytes 3145736 | tf_op jit(solution)/shard_map/ppermute | solution.py:22
  57.5 9.2 %collective-permute-start.2 = (bf16[256,384]{1,0:T(8,128)(2,1)S(1)}, bf16[256,384]{1,0:T(8,128)(2,1)S(1)}, u32[]{:S(2)}, u32[]{:S(2)}) collective-permute-start(bf16[256,384]{1,0:T(8,128)(2,1)S(1)} %get-tuple-element.33), channel_id=1, source_target_pairs={{0,64},{64,0},{1,65},{65,1},{2,66},{66,2},{3,67},{67,3},{4,68},{68... | collective-permute-start | bytes 589832 | tf_op jit(solution)/shard_map/ppermute | solution.py:22
  91.9 4.6 %collective-permute-start.4 = (bf16[512,1024]{1,0:T(8,128)(2,1)S(1)}, bf16[512,1024]{1,0:T(8,128)(2,1)S(1)}, u32[]{:S(2)}, u32[]{:S(2)}) collective-permute-start(bf16[512,1024]{1,0:T(8,128)(2,1)S(1)} %select_convert_fusion), channel_id=1, source_target_pairs={{0,1},{1,0},{2,3},{3,2},{4,5},{5,4},{6,7},{7,6},{8,9},{9,8},{10,11... | collective-permute-start | bytes 3145736 | tf_op jit(solution)/shard_map/ppermute | solution.py:22
  98.3 19.3 %all-to-all-start.1 = ((bf16[8,64,1024]{2,1,0:T(8,128)(2,1)}), bf16[8,64,1024]{2,1,0:T(8,128)(2,1)S(1)}, u32[]{:S(2)}, u32[]{:S(2)}) async-start(bf16[8,64,1024]{2,1,0:T(8,128)(2,1)} %bitcast.13), calls=%async_computation.2 | async-start | bytes 2097152 | tf_op jit(solution)/shard_map/all_to_all | solution.py:213
  107.7 17.6 %collective-permute-start.5 = (f32[8,768]{1,0:T(8,128)S(1)}, f32[8,768]{1,0:T(8,128)S(1)}, u32[]{:S(2)}, u32[]{:S(2)}) collective-permute-start(f32[8,768]{1,0:T(8,128)S(1)} %get-tuple-element.17), channel_id=1, source_target_pairs={{0,8},{8,0},{16,24},{24,16},{32,40},{40,32},{48,56},{56,48},{1,9},... | collective-permute-start | bytes 73736 | tf_op jit(solution)/shard_map/ppermute | solution.py:220
  118.8 33.7 %all-to-all-start.2 = ((bf16[8,64,1024]{2,1,0:T(8,128)(2,1)}), bf16[8,64,1024]{2,1,0:T(8,128)(2,1)S(1)}, u32[]{:S(2)}, u32[]{:S(2)}) async-start(bf16[8,64,1024]{2,1,0:T(8,128)(2,1)} %broadcast_in_dim.2), calls=%async_computation.3 | async-start | bytes 2097152 | tf_op jit(solution)/shard_map/all_to_all | solution.py:218
  125.2 31.6 %copy-start.7 = (f32[3,704]{1,0:T(4,128)S(1)}, f32[3,704]{1,0:T(4,128)}, u32[]{:S(2)}) copy-start(f32[3,704]{1,0:T(4,128)} %param.20) | copy-start | bytes 25348
  125.2 31.6 %copy-start.8 = (f32[3,704]{1,0:T(4,128)S(1)}, f32[3,704]{1,0:T(4,128)}, u32[]{:S(2)}) copy-start(f32[3,704]{1,0:T(4,128)} %param.21) | copy-start | bytes 25348
  125.3 7.6 %collective-permute-start.6 = (f32[8,768]{1,0:T(8,128)S(1)}, f32[8,768]{1,0:T(8,128)S(1)}, u32[]{:S(2)}, u32[]{:S(2)}) collective-permute-start(f32[8,768]{1,0:T(8,128)S(1)} %add.80), channel_id=1, source_target_pairs={{0,16},{8,24},{16,0},{24,8},{32,48},{40,56},{48,32},{56,40},{1,17}... | collective-permute-start | bytes 73736 | tf_op jit(solution)/shard_map/ppermute | solution.py:220
  129.3 28.2 %collective-permute-start.3 = (bf16[256,384]{0,1:T(8,128)(2,1)S(1)}, bf16[256,384]{0,1:T(8,128)(2,1)S(1)}, u32[]{:S(2)}, u32[]{:S(2)}) collective-permute-start(bf16[256,384]{0,1:T(8,128)(2,1)S(1)} %fusion.23), channel_id=1, source_target_pairs={{0,64},{64,0},{1,65},{65,1},{2,66},{66,2},{3,67},{67,3},{4,68},{68... | collective-permute-start | bytes 589832 | tf_op jit(solution)/shard_map/ppermute | solution.py:22
  132.8 9.6 %collective-permute-start.7 = (f32[8,768]{1,0:T(8,128)S(1)}, f32[8,768]{1,0:T(8,128)S(1)}, u32[]{:S(2)}, u32[]{:S(2)}) collective-permute-start(f32[8,768]{1,0:T(8,128)S(1)} %add.81), channel_id=1, source_target_pairs={{0,32},{8,40},{16,48},{24,56},{32,0},{40,8},{48,16},{56,24},{1,33}... | collective-permute-start | bytes 73736 | tf_op jit(solution)/shard_map/ppermute | solution.py:220
  142.5 6.6 %collective-permute-start.8 = (f32[8,768]{1,0:T(8,128)S(1)}, f32[8,768]{1,0:T(8,128)S(1)}, u32[]{:S(2)}, u32[]{:S(2)}) collective-permute-start(f32[8,768]{1,0:T(8,128)S(1)} %add.82), channel_id=1, source_target_pairs={{0,128},{128,0},{1,129},{129,1},{2,130},{130,2},{3,131},{131,3},{4... | collective-permute-start | bytes 73736 | tf_op jit(solution)/shard_map/ppermute | solution.py:22
  149.1 7.7 %collective-permute-start.9 = (f32[8,768]{1,0:T(8,128)S(1)}, f32[8,768]{1,0:T(8,128)S(1)}, u32[]{:S(2)}, u32[]{:S(2)}) collective-permute-start(f32[8,768]{1,0:T(8,128)S(1)} %add.83), channel_id=1, source_target_pairs={{0,64},{64,0},{1,65},{65,1},{2,66},{66,2},{3,67},{67,3},{4,68},{68... | collective-permute-start | bytes 73736 | tf_op jit(solution)/shard_map/ppermute | solution.py:22
  152.5 13.1 %all-to-all-start.3 = ((bf16[4,64,768]{2,1,0:T(8,128)(2,1)}), bf16[4,64,768]{2,1,0:T(8,128)(2,1)S(1)}, u32[]{:S(2)}, u32[]{:S(2)}) async-start(bf16[4,64,768]{2,1,0:T(8,128)(2,1)} %bitcast.49), calls=%async_computation.4 | async-start | bytes 786432 | tf_op jit(solution)/shard_map/all_to_all | solution.py:241
  (6 other events, 43.8 us)
Sparse Core Ops, SparseCore 0:
  29.2 49.3 all-gather.1
  88.1 48.4 reduce-scatter.1

commit v5 on v4

--- a/solution.py
+++ b/solution.py
@@ -47,21 +47,45 @@
 
 
 def early_kernel(
-    scale, gathered, own, other, cotangent, filters, weight, grads, terms, tap_sums
+    scale,
+    gathered,
+    own,
+    other,
+    cotangent,
+    filters,
+    weight_out,
+    grads_out,
+    terms_out,
+    tap_sums,
+    weight,
+    grads,
+    terms,
+    in_sems,
+    out_sems,
 ):
     n_y, n_z, shard_rows, columns = gathered.shape
-    length, depth = own.shape
+    length = own.shape[0]
     wide = columns // 2
     span = n_y * shard_rows
-    for z in range(n_z):
-        for y in range(n_y):
-            at = z * span + y * shard_rows
-            weight[at : at + shard_rows, :] = gathered[y, z]
+    fetches = [
+        pltpu.make_async_copy(gathered.at[y], weight.at[:, y], in_sems.at[y])
+        for y in range(n_y)
+    ]
+    for fetch in fetches:
+        fetch.start()
     first, second, third = filters[0:1, :], filters[1:2, :], filters[2:3, :]
     slope = math.sqrt(2.0 / math.pi)
     sums = [jnp.zeros((1, columns), jnp.float32) for _ in range(3)]
+    for fetch in fetches:
+        fetch.wait()
+    stores = [pltpu.make_async_copy(weight, weight_out, out_sems.at[0])]
+    stores[0].start()
     for part, rows in enumerate((own, other)):
-        pre = jnp.dot(rows[...], weight[...], preferred_element_type=jnp.float32)
+        pre = jnp.dot(
+            rows[...],
+            weight[...].reshape(n_z * span, columns),
+            preferred_element_type=jnp.float32,
+        )
         pre = pre.astype(jnp.bfloat16).astype(jnp.float32)
         one_back, two_back = moved(pre, 1), moved(pre, 2)
         mixed = first * two_back + second * one_back + third * pre
@@ -79,6 +103,8 @@
             sums[tap] = sums[tap] + jnp.sum(back * source, axis=0, keepdims=True)
         full = third * back + second * moved(back, -1) + first * moved(back, -2)
         grads[part * length : (part + 1) * length, :] = full.astype(jnp.bfloat16)
+    stores.append(pltpu.make_async_copy(grads, grads_out, out_sems.at[1]))
+    stores[1].start()
     tap_sums[...] = jnp.concatenate(
         [scale * value for value in sums]
         + [jnp.zeros((tap_sums.shape[0] - 3, columns), jnp.float32)]
@@ -94,24 +120,39 @@
             for part, rows in enumerate((own, other))
         )
         term = (term * scale).astype(jnp.bfloat16)
-        for y in range(n_y):
-            terms[y, z] = term[y * shard_rows : (y + 1) * shard_rows, :]
+        terms[z] = term.reshape(n_y, shard_rows, columns)
+        store = pltpu.make_async_copy(
+            terms.at[z], terms_out.at[:, z], out_sems.at[2 + z]
+        )
+        store.start()
+        stores.append(store)
+    for store in stores:
+        store.wait()
 
 
 def early_pass(scale, gathered, own, other, cotangent, filters):
     n_y, n_z, shard_rows, columns = gathered.shape
     length, depth = own.shape
     whole = pl.BlockSpec(memory_space=pltpu.VMEM)
+    apart = pl.BlockSpec(memory_space=pl.ANY)
+    ordered = (n_z, n_y, shard_rows, columns)
     return pl.pallas_call(
         functools.partial(early_kernel, scale),
         out_shape=(
-            jax.ShapeDtypeStruct((depth, columns), jnp.bfloat16),
+            jax.ShapeDtypeStruct(ordered, jnp.bfloat16),
             jax.ShapeDtypeStruct((2 * length, columns), jnp.bfloat16),
             jax.ShapeDtypeStruct(gathered.shape, jnp.bfloat16),
             jax.ShapeDtypeStruct((8, columns), jnp.float32),
         ),
-        in_specs=[whole] * 5,
-        out_specs=(whole,) * 4,
+        in_specs=[apart] + [whole] * 4,
+        out_specs=(apart, apart, apart, whole),
+        scratch_shapes=[
+            pltpu.VMEM(ordered, jnp.bfloat16),
+            pltpu.VMEM((2 * length, columns), jnp.bfloat16),
+            pltpu.VMEM(ordered, jnp.bfloat16),
+            pltpu.SemaphoreType.DMA((n_y,)),
+            pltpu.SemaphoreType.DMA((2 + n_z,)),
+        ],
         compiler_params=pltpu.CompilerParams(vmem_limit_bytes=48 * 1024 * 1024),
         cost_estimate=pl.CostEstimate(
             flops=8 * length * depth * columns,
@@ -179,12 +220,12 @@
             jnp.concatenate([low[:cut], high[:cut]]),
         )
 
-    gate_mine, gate_other = halves(gate_weight)
-    up_mine, up_other = halves(up_weight)
-    weight_mine = jnp.concatenate([gate_mine, up_mine], axis=1)
-    weight_other = jnp.concatenate([gate_other, up_other], axis=1)
     for_z = jnp.stack(
-        [pick(first_z, weight_mine, weight_other), pick(first_z, weight_other, weight_mine)] * 2
+        [
+            jnp.concatenate([widened(gate_weight[:, at]), widened(up_weight[:, at])], axis=1)
+            for at in (slice(0, width), slice(width, 2 * width))
+        ]
+        * (n_z // 2)
     )
     block = lax.all_to_all(for_z, Z, 0, 0, tiled=True)
     late_other, early_other = partners(late_rows, early_rows)
@@ -198,16 +239,18 @@
     weight, both_grads, terms, taps = early_pass(
         rows_scale, weight, early_rows, early_other, cotangent, filters
     )
+    weight = weight.reshape(depth, 2 * wide)
     terms = terms.reshape(depth, 2 * wide)
     reduced = lax.psum_scatter(terms, "y", scatter_dimension=0, tiled=True)
     reduced = reduced.reshape(n_z, shard_rows, 2 * wide)
     partial = lax.dot_general(
         both_grads, weight, contract_last, preferred_element_type=jnp.float32
-    )
+    ).astype(jnp.bfloat16)
     cut = depth // 2
     kept = pick(first_c, partial[:, :cut], partial[:, cut:])
-    given = pick(first_c, partial[:, cut:], partial[:, :cut]).astype(jnp.bfloat16)
-    chip = (kept + swapped(given, "c").astype(jnp.float32)).astype(jnp.bfloat16)
+    given = pick(first_c, partial[:, cut:], partial[:, :cut])
+    chip = kept.astype(jnp.float32) + swapped(given, "c").astype(jnp.float32)
+    chip = chip.astype(jnp.bfloat16)
     chip = chip.reshape(2, n_x, row_count // n_x, cut)
     chip = jnp.stack([pick(first_z, chip[0], chip[1]), pick(first_z, chip[1], chip[0])])
     spread = lax.all_to_all(
@@ -218,11 +261,8 @@
     finished = lax.all_to_all(copies, TP, 0, 0, tiled=True)
     for step in (1, 2, 4):
         taps = taps + lax.ppermute(taps, "y", [(k, k ^ step) for k in range(n_y)])
-    taps = taps + swapped(taps, "zp")
-    gate_taps_mine, up_taps_mine = taps[:3, :width], taps[:3, wide : wide + width]
-    taps = swapped(taps, "zb")
-    gate_tap_sums = columns_joined(gate_taps_mine, taps[:3, :width])
-    up_tap_sums = columns_joined(up_taps_mine, taps[:3, wide : wide + width])
+    high = lax.reduce_precision(taps, 8, 7)
+    taps = jnp.concatenate([high, taps - high]).astype(jnp.bfloat16)
 
     product = [
         stored(jnp.dot(rows, weight, preferred_element_type=jnp.float32))
@@ -238,9 +278,19 @@
     late_hidden = columns_joined(late[0][:, :width], swapped(late[1], "zb")[:, :width])
 
     reduced, finished = lax.optimization_barrier((reduced, finished))
+    reduced = jnp.concatenate(
+        [reduced, jnp.broadcast_to(taps[None], (n_z, *taps.shape))], axis=1
+    )
     pieces = lax.all_to_all(reduced, Z, 0, 0, tiled=True)
-    pieces = pieces.reshape(2, 2, shard_rows, 2 * wide).astype(jnp.float32)
+    pieces = pieces.reshape(2, 2, -1, 2 * wide).astype(jnp.float32)
     pieces = jnp.sum(pieces, axis=0)
+    tap_sums = pieces[:, shard_rows:].reshape(2, 2, -1, 2 * wide)
+    tap_sums = jnp.sum(tap_sums, axis=1)[:, :3]
+    pieces = pieces[:, :shard_rows]
+    gate_tap_sums = jnp.concatenate([tap_sums[0, :, :width], tap_sums[1, :, :width]], axis=1)
+    up_tap_sums = jnp.concatenate(
+        [tap_sums[0, :, wide : wide + width], tap_sums[1, :, wide : wide + width]], axis=1
+    )
     gate_sum = jnp.concatenate([pieces[0, :, :width], pieces[1, :, :width]], axis=1)
     up_sum = jnp.concatenate([pieces[0, :, wide : wide + width], pieces[1, :, wide : wide + width]], axis=1)
 

time: 174 us -> 173 us (level)
  starting transfers between devices: 47.1 us -> 40.3 us
  other arithmetic: 9.07 us -> 12.1 us
  matrix products: 8.15 us -> 9.96 us
    ppermute x7 -> x5, waiting for transfers between devices: 34.8 us -> 43.3 us  [swapped(): return lax.ppermute(values, axis, [(0, 1), (1, 0)])]
    ppermute x7 -> x5, starting transfers between devices: 19.6 us -> 12.2 us  [swapped(): return lax.ppermute(values, axis, [(0, 1), (1, 0)])]
    all_to_all x1, waiting for transfers between devices: 4.9 us -> 0.01 us  [per_device(): pieces = lax.all_to_all(reduced, Z, 0, 0, tiled=True)]
    all_to_all x1, waiting for transfers between devices: 5.63 us -> 2.88 us  [per_device(): lax.all_to_all(chip.reshape(2 * n_x, row_count // n_x, cut), ('zb', 'x'),...]
    slice x6 -> x4, local copies, waits for them, and re-layouts: 2.14 us -> 0.16 us  [halves(): low, high = (widened(array[..., :width]), widened(array[..., width:]))]
    slice x2, local copies, waits for them, and re-layouts: 0.01 us -> 1.99 us  [the longest x1 1.06 us: per_device(): gate_weight[:, at]]
    dot_general x2, matrix products: 4.44 us -> 6.25 us  [per_device(): jnp.dot(rows, weight, preferred_element_type=jnp.float32)]
  transfers between devices with their start and end apart: 15 -> 13, of which waited for: 9 -> 8; matrix products, arithmetic and copies ran while one was open for 12% -> 13% of each run, Pallas kernels for 0% -> 0%
where the time goes in v5:
time: 173 us; the launch traced here: 171 us
  waiting for transfers between devices  59.3 us (34%)
  starting transfers between devices  40.3 us (23%)
  blocking collectives  18.8 us (11%)
  between operations  14.6 us (8%)
  other arithmetic  12.1 us (7%)
  matrix products  9.96 us (6%)
  Pallas kernels  7.92 us (5%)
  local copies, waits for them, and re-layouts  7.83 us (5%)
    ppermute x5, waiting for transfers between devices, swapped(): return lax.ppermute(values, axis, [(0, 1), (1, 0)])  43.3 us
    all_to_all x1, blocking collectives, per_device(): block = lax.all_to_all(for_z, Z, 0, 0, tiled=True)  18.8 us
    ppermute x5, starting transfers between devices, swapped(): return lax.ppermute(values, axis, [(0, 1), (1, 0)])  12.2 us
    ppermute x3, starting transfers between devices, per_device(): taps = taps + lax.ppermute(taps, 'y', [(k, k ^ step) for k in range(n_y)])  12 us
    all_gather x1, waiting for transfers between devices, per_device(): weight = lax.all_gather(block, 'y').reshape(n_y, n_z, shard_rows, 2 * wide)  8.45 us
    pallas_call x1, Pallas kernels, early_pass(): pl.pallas_call(functools.partial(early_kernel, scale), out_shape=(jax.Sha...  7.92 us
    dot_general x2, matrix products, per_device(): jnp.dot(rows, weight, preferred_element_type=jnp.float32)  6.25 us
    all_to_all x1, starting transfers between devices, per_device(): lax.all_to_all(chip.reshape(2 * n_x, row_count // n_x, cut), ('zb', 'x'),...  5.88 us
  transfers between devices with their start and end apart: 13, of which 8 were waited for; matrix products, arithmetic and copies ran while one was open for 13% of the time, Pallas kernels for 0%

profile of v5, /device:TPU:6, one launch (start us, length us, event | category | flops | bytes accessed | tf_op | source)
XLA Modules:
  0.0 170.8 jit_solution(9630398360588605486)
XLA Ops:
  10.2 18.8 %all_to_all.20 = bf16[4,64,768]{2,1,0:T(8,128)(2,1)} all-to-all(bf16[4,64,768]{2,1,0:T(8,128)(2,1)S(1)} %pad_maximum_fusion.4), channel_id=1, replica_groups=mesh['rep'=2,'zp'=2,'zb'=2,'y'=8,'x'=4,'c'=2] {'zp','zb'}, dimensions={0} | all-to-all | bytes 786432 | tf_op jit(solution)/shard_map/all_to_all | solution.py:230
  29.4 2.3 %collective-permute-start = (bf16[256,2048]{1,0:T(8,128)(2,1)S(1)}, bf16[256,2048]{1,0:T(8,128)(2,1)S(1)}, u32[]{:S(2)}, u32[]{:S(2)}) collective-permute-start(bf16[256,2048]{1,0:T(8,128)(2,1)S(1)} %pad_maximum_fusion), channel_id=1, source_target_pairs={{0,64},{64,0},{1,65},{65,1},{2,66},{66,2},{3,67},{67,3},{4,68},{68... | collective-permute-start | bytes 3145736 | tf_op jit(solution)/shard_map/ppermute | solution.py:22
  31.6 23.6 %collective-permute-done = bf16[256,2048]{1,0:T(8,128)(2,1)S(1)} collective-permute-done((bf16[256,2048]{1,0:T(8,128)(2,1)S(1)}, bf16[256,2048]{1,0:T(8,128)(2,1)S(1)}, u32[]{:S(2)}, u32[]{:S(2)}) %collective-permute-start) | collective-permute-done | bytes 1048608 | tf_op jit(solution)/shard_map/ppermute | solution.py:22
  55.2 1.9 %collective-permute-start.1 = (bf16[256,2048]{1,0:T(8,128)(2,1)S(1)}, bf16[256,2048]{1,0:T(8,128)(2,1)}, u32[]{:S(2)}, u32[]{:S(2)}) collective-permute-start(bf16[256,2048]{1,0:T(8,128)(2,1)S(1)} %collective-permute-done), channel_id=1, source_target_pairs={{0,1},{1,0},{2,3},{3,2},{4,5},{5,4},{6,7},{7,6},{8,9},{9,8},{10,11... | collective-permute-start | bytes 3145736 | tf_op jit(solution)/shard_map/ppermute | solution.py:22
  57.6 2.2 %collective-permute-start.2 = (bf16[256,384]{1,0:T(8,128)(2,1)S(1)}, bf16[256,384]{1,0:T(8,128)(2,1)S(1)}, u32[]{:S(2)}, u32[]{:S(2)}) collective-permute-start(bf16[256,384]{1,0:T(8,128)(2,1)S(1)} %get-tuple-element.37), channel_id=1, source_target_pairs={{0,64},{64,0},{1,65},{65,1},{2,66},{66,2},{3,67},{67,3},{4,68},{68... | collective-permute-start | bytes 589832 | tf_op jit(solution)/shard_map/ppermute | solution.py:22
  60.0 6.8 %collective-permute-done.2 = bf16[256,384]{1,0:T(8,128)(2,1)S(1)} collective-permute-done((bf16[256,384]{1,0:T(8,128)(2,1)S(1)}, bf16[256,384]{1,0:T(8,128)(2,1)S(1)}, u32[]{:S(2)}, u32[]{:S(2)}) %collective-permute-start.2) | collective-permute-done | bytes 196640 | tf_op jit(solution)/shard_map/ppermute | solution.py:22
  70.1 8.5 %all-gather.2.cloned.1.call-done = bf16[8,256,768]{2,1,0:T(8,128)(2,1)} async-done(((bf16[1,256,768]{2,1,0:T(8,128)(2,1)}), bf16[8,256,768]{2,1,0:T(8,128)(2,1)}) %all-gather.2.cloned.1.call-update) | async-done | bytes 3145744 | tf_op jit(solution)/shard_map/all_gather | solution.py:238
  78.6 7.9 %early_pass.1 = (bf16[4,8,64,768]{3,2,1,0:T(8,128)(2,1)}, bf16[512,768]{1,0:T(8,128)(2,1)S(1)}, bf16[8,4,64,768]{3,2,1,0:T(8,128)(2,1)}, f32[8,768]{1,0:T(8,128)S(1)}) custom-call(bf16[8,4,64,768]{3,2,1,0:T(8,128)(2,1)} %bitcast.60, bf16[256,2048]{1,0:T(8,128)(2,1)S(1)} %copy-done, bf16[256,2048]{1,0:T(8,128)(2,1)S(1)} %pad_maximum_fusion.1.other, ...), custom_call_target="tpu_custom_call" | custom-call | flops 3221225472 | bytes 11534336 | tf_op jit(solution)/shard_map/early_pass/pallas_call | solution.py:139
  86.5 3.7 %convolution_convert_fusion = bf16[512,2048]{1,0:T(8,128)(2,1)S(1)} fusion(bf16[512,768]{1,0:T(8,128)(2,1)S(1)} %get-tuple-element.14, bf16[2048,768]{1,0:T(8,128)(2,1)} %bitcast.61), kind=kOutput, calls=%fused_computation | convolution fusion | flops 1611661312 | bytes 6029312 | tf_op jit(solution)/shard_map/dot_general | solution.py:246
  90.4 1.9 %collective-permute-start.4 = (bf16[512,1024]{1,0:T(8,128)(2,1)S(1)}, bf16[512,1024]{1,0:T(8,128)(2,1)S(1)}, u32[]{:S(2)}, u32[]{:S(2)}) collective-permute-start(bf16[512,1024]{1,0:T(8,128)(2,1)S(1)} %broadcast_select_fusion), channel_id=1, source_target_pairs={{0,1},{1,0},{2,3},{3,2},{4,5},{5,4},{6,7},{7,6},{8,9},{9,8},{10,11... | collective-permute-start | bytes 3145736 | tf_op jit(solution)/shard_map/ppermute | solution.py:22
  92.3 2.6 %collective-permute-done.4 = bf16[512,1024]{1,0:T(8,128)(2,1)S(1)} collective-permute-done((bf16[512,1024]{1,0:T(8,128)(2,1)S(1)}, bf16[512,1024]{1,0:T(8,128)(2,1)S(1)}, u32[]{:S(2)}, u32[]{:S(2)}) %collective-permute-start.4) | collective-permute-done | bytes 1048608 | tf_op jit(solution)/shard_map/ppermute | solution.py:22
  96.7 5.9 %all-to-all-start.1 = ((bf16[8,64,1024]{2,1,0:T(8,128)(2,1)}), bf16[8,64,1024]{2,1,0:T(8,128)(2,1)S(1)}, u32[]{:S(2)}, u32[]{:S(2)}) async-start(bf16[8,64,1024]{2,1,0:T(8,128)(2,1)} %bitcast.12), calls=%async_computation.2 | async-start | bytes 2097152 | tf_op jit(solution)/shard_map/all_to_all | solution.py:256
  102.6 3.0 %collective-permute-start.5 = (f32[8,768]{1,0:T(8,128)S(1)}, f32[8,768]{1,0:T(8,128)S(1)}, u32[]{:S(2)}, u32[]{:S(2)}) collective-permute-start(f32[8,768]{1,0:T(8,128)S(1)} %get-tuple-element.17), channel_id=1, source_target_pairs={{0,8},{8,0},{16,24},{24,16},{32,40},{40,32},{48,56},{56,48},{1,9},... | collective-permute-start | bytes 73736 | tf_op jit(solution)/shard_map/ppermute | solution.py:263
  105.6 3.0 %fusion = bf16[256,768]{0,1:T(8,128)(2,1)S(1)} fusion(bf16[2048,768]{1,0:T(8,128)(2,1)} %bitcast.62, bf16[256,2048]{1,0:T(8,128)(2,1)S(1)} %copy-done.2), kind=kOutput, calls=%fused_computation.8 | convolution fusion | flops 805502976 | bytes 4587520 | tf_op jit(solution)/shard_map/dot_general | solution.py:268
  109.0 4.1 %collective-permute-start.6 = (f32[8,768]{1,0:T(8,128)S(1)}, f32[8,768]{1,0:T(8,128)S(1)}, u32[]{:S(2)}, u32[]{:S(2)}) collective-permute-start(f32[8,768]{1,0:T(8,128)S(1)} %add.75), channel_id=1, source_target_pairs={{0,16},{8,24},{16,0},{24,8},{32,48},{40,56},{48,32},{56,40},{1,17}... | collective-permute-start | bytes 73736 | tf_op jit(solution)/shard_map/ppermute | solution.py:263
  113.1 2.9 %all-to-all-done.1 = bf16[8,64,1024]{2,1,0:T(8,128)(2,1)S(1)} async-done(((bf16[8,64,1024]{2,1,0:T(8,128)(2,1)}), bf16[8,64,1024]{2,1,0:T(8,128)(2,1)S(1)}, u32[]{:S(2)}, u32[]{:S(2)}) %all-to-all-start.1) | async-done | bytes 1048608 | tf_op jit(solution)/shard_map/all_to_all | solution.py:256
  117.2 5.2 %all-to-all-start.2 = ((bf16[8,64,1024]{2,1,0:T(8,128)(2,1)}), bf16[8,64,1024]{2,1,0:T(8,128)(2,1)S(1)}, u32[]{:S(2)}, u32[]{:S(2)}) async-start(bf16[8,64,1024]{2,1,0:T(8,128)(2,1)} %broadcast_in_dim.4), calls=%async_computation.3 | async-start | bytes 2097152 | tf_op jit(solution)/shard_map/all_to_all | solution.py:261
  122.5 3.3 %convolution_convert_fusion.1 = bf16[256,768]{0,1:T(8,128)(2,1)S(1)} fusion(bf16[2048,768]{1,0:T(8,128)(2,1)} %bitcast.63, bf16[128,2048]{1,0:T(8,128)(2,1)S(1)} %copy-done.4, bf16[128,2048]{1,0:T(8,128)(2,1)S(1)} %copy-done.3), kind=kOutput, calls=%fused_computation.6 | convolution fusion | flops 807600128 | bytes 4587520 | tf_op jit(solution)/shard_map/dot_general | solution.py:268
  125.9 5.0 %collective-permute-start.7 = (f32[8,768]{1,0:T(8,128)S(1)}, f32[8,768]{1,0:T(8,128)S(1)}, u32[]{:S(2)}, u32[]{:S(2)}) collective-permute-start(f32[8,768]{1,0:T(8,128)S(1)} %add.76), channel_id=1, source_target_pairs={{0,32},{8,40},{16,48},{24,56},{32,0},{40,8},{48,16},{56,24},{1,33}... | collective-permute-start | bytes 73736 | tf_op jit(solution)/shard_map/ppermute | solution.py:263
  132.1 4.2 %collective-permute-done.7 = f32[8,768]{1,0:T(8,128)S(1)} collective-permute-done((f32[8,768]{1,0:T(8,128)S(1)}, f32[8,768]{1,0:T(8,128)S(1)}, u32[]{:S(2)}, u32[]{:S(2)}) %collective-permute-start.7) | collective-permute-done | bytes 24608 | tf_op jit(solution)/shard_map/ppermute | solution.py:263
  136.3 1.8 %pad_maximum_fusion.3 = bf16[4,80,768]{2,1,0:T(8,128)(2,1)} fusion(bf16[4,16,768]{2,1,0:T(8,128)(2,1)S(1)} %broadcast_in_dim.5, bf16[4,64,768]{2,1,0:T(8,128)(2,1)} %bitcast.58), kind=kLoop, calls=%fused_computation.33 | loop fusion | flops 983040 | bytes 983040 | tf_op jit(solution)/shard_map/concatenate | solution.py:281
  138.2 4.9 %all-to-all-start.3 = ((bf16[4,80,768]{2,1,0:T(8,128)(2,1)}), bf16[4,80,768]{2,1,0:T(8,128)(2,1)S(1)}, u32[]{:S(2)}, u32[]{:S(2)}) async-start(bf16[4,80,768]{2,1,0:T(8,128)(2,1)} %pad_maximum_fusion.3), calls=%async_computation.4 | async-start | bytes 983040 | tf_op jit(solution)/shard_map/all_to_all | solution.py:284
  143.2 3.9 %collective-permute-start.3 = (bf16[256,384]{0,1:T(8,128)(2,1)S(1)}, bf16[256,384]{0,1:T(8,128)(2,1)S(1)}, u32[]{:S(2)}, u32[]{:S(2)}) collective-permute-start(bf16[256,384]{0,1:T(8,128)(2,1)S(1)} %fusion.23), channel_id=1, source_target_pairs={{0,64},{64,0},{1,65},{65,1},{2,66},{66,2},{3,67},{67,3},{4,68},{68... | collective-permute-start | bytes 589832 | tf_op jit(solution)/shard_map/ppermute | solution.py:22
  147.3 10.3 %collective-permute-done.3 = bf16[256,384]{0,1:T(8,128)(2,1)S(1)} collective-permute-done((bf16[256,384]{0,1:T(8,128)(2,1)S(1)}, bf16[256,384]{0,1:T(8,128)(2,1)S(1)}, u32[]{:S(2)}, u32[]{:S(2)}) %collective-permute-start.3) | collective-permute-done | bytes 196640 | tf_op jit(solution)/shard_map/ppermute | solution.py:22
  (88 shorter events, 18.7 us)
Async XLA Ops:
  7.2 21.9 %copy-start = (bf16[256,2048]{1,0:T(8,128)(2,1)S(1)}, bf16[256,2048]{1,0:T(8,128)(2,1)}, u32[]{:S(2)}) copy-start(bf16[256,2048]{1,0:T(8,128)(2,1)} %own.1) | copy-start | bytes 3145732
  7.2 21.9 %copy-start.1 = (bf16[256,2048]{1,0:T(8,128)(2,1)S(1)}, bf16[256,2048]{1,0:T(8,128)(2,1)}, u32[]{:S(2)}) copy-start(bf16[256,2048]{1,0:T(8,128)(2,1)} %param.11) | copy-start | bytes 3145732
  7.2 71.4 %all-gather.2.cloned.1.call-start = ((), (), s32[]{:S(2)}) async-start(), calls=%async_computation.5 | async-start | bytes 3538944 | tf_op jit(solution)/shard_map/all_gather | solution.py:238
  29.0 107.3 %reduce-scatter.2.cloned.1.call-start = ((), (), s32[]{:S(2)}) async-start(), calls=%async_computation.6 | async-start | bytes 3538944 | tf_op jit(solution)/shard_map/reduce_scatter | solution.py:244
  29.2 27.9 %slice-start = ((bf16[256,704]{0,1:T(8,128)(2,1)}), bf16[256,352]{0,1:T(8,128)(2,1)S(1)}, s32[]{:S(2)}) async-start(bf16[256,704]{0,1:T(8,128)(2,1)} %param.13), calls=%async_computation.7 | async-start | bytes 360448 | tf_op jit(solution)/shard_map/slice | solution.py:200
  29.2 28.1 %slice-start.1 = ((bf16[256,704]{0,1:T(8,128)(2,1)}), bf16[256,384]{0,1:T(8,128)(2,1)S(1)}, s32[]{:S(2)}) async-start(bf16[256,704]{0,1:T(8,128)(2,1)} %param.13), calls=%async_computation.8 | async-start | bytes 393216 | tf_op jit(solution)/shard_map/slice.5
  29.3 28.2 %copy-start.11 = (pred[384]{0:T(512)(128)(4,1)S(1)}, pred[384]{0:T(512)(128)(4,1)}, u32[]{:S(2)}) copy-start(pred[384]{0:T(512)(128)(4,1)} %constant.23.clone.1) | copy-start | bytes 1156
  29.3 30.5 %copy-start.9 = (bf16[3,704]{1,0:T(4,128)(2,1)S(1)}, bf16[3,704]{1,0:T(4,128)(2,1)}, u32[]{:S(2)}) copy-start(bf16[3,704]{1,0:T(4,128)(2,1)} %param.16) | copy-start | bytes 12676
  29.3 30.6 %copy-start.10 = (bf16[3,704]{1,0:T(4,128)(2,1)S(1)}, bf16[3,704]{1,0:T(4,128)(2,1)}, u32[]{:S(2)}) copy-start(bf16[3,704]{1,0:T(4,128)(2,1)} %param.17) | copy-start | bytes 12676
  29.4 25.8 %collective-permute-start = (bf16[256,2048]{1,0:T(8,128)(2,1)S(1)}, bf16[256,2048]{1,0:T(8,128)(2,1)S(1)}, u32[]{:S(2)}, u32[]{:S(2)}) collective-permute-start(bf16[256,2048]{1,0:T(8,128)(2,1)S(1)} %pad_maximum_fusion), channel_id=1, source_target_pairs={{0,64},{64,0},{1,65},{65,1},{2,66},{66,2},{3,67},{67,3},{4,68},{68... | collective-permute-start | bytes 3145736 | tf_op jit(solution)/shard_map/ppermute | solution.py:22
  55.2 11.6 %collective-permute-start.1 = (bf16[256,2048]{1,0:T(8,128)(2,1)S(1)}, bf16[256,2048]{1,0:T(8,128)(2,1)}, u32[]{:S(2)}, u32[]{:S(2)}) collective-permute-start(bf16[256,2048]{1,0:T(8,128)(2,1)S(1)} %collective-permute-done), channel_id=1, source_target_pairs={{0,1},{1,0},{2,3},{3,2},{4,5},{5,4},{6,7},{7,6},{8,9},{9,8},{10,11... | collective-permute-start | bytes 3145736 | tf_op jit(solution)/shard_map/ppermute | solution.py:22
  57.6 9.2 %collective-permute-start.2 = (bf16[256,384]{1,0:T(8,128)(2,1)S(1)}, bf16[256,384]{1,0:T(8,128)(2,1)S(1)}, u32[]{:S(2)}, u32[]{:S(2)}) collective-permute-start(bf16[256,384]{1,0:T(8,128)(2,1)S(1)} %get-tuple-element.37), channel_id=1, source_target_pairs={{0,64},{64,0},{1,65},{65,1},{2,66},{66,2},{3,67},{67,3},{4,68},{68... | collective-permute-start | bytes 589832 | tf_op jit(solution)/shard_map/ppermute | solution.py:22
  90.4 4.6 %collective-permute-start.4 = (bf16[512,1024]{1,0:T(8,128)(2,1)S(1)}, bf16[512,1024]{1,0:T(8,128)(2,1)S(1)}, u32[]{:S(2)}, u32[]{:S(2)}) collective-permute-start(bf16[512,1024]{1,0:T(8,128)(2,1)S(1)} %broadcast_select_fusion), channel_id=1, source_target_pairs={{0,1},{1,0},{2,3},{3,2},{4,5},{5,4},{6,7},{7,6},{8,9},{9,8},{10,11... | collective-permute-start | bytes 3145736 | tf_op jit(solution)/shard_map/ppermute | solution.py:22
  95.6 10.0 %copy-start.2 = (bf16[256,2048]{1,0:T(8,128)(2,1)S(1)}, bf16[256,2048]{1,0:T(8,128)(2,1)}, u32[]{:S(2)}) copy-start(bf16[256,2048]{1,0:T(8,128)(2,1)} %param.11) | copy-start | bytes 3145732
  96.7 19.3 %all-to-all-start.1 = ((bf16[8,64,1024]{2,1,0:T(8,128)(2,1)}), bf16[8,64,1024]{2,1,0:T(8,128)(2,1)S(1)}, u32[]{:S(2)}, u32[]{:S(2)}) async-start(bf16[8,64,1024]{2,1,0:T(8,128)(2,1)} %bitcast.12), calls=%async_computation.2 | async-start | bytes 2097152 | tf_op jit(solution)/shard_map/all_to_all | solution.py:256
  102.6 6.4 %collective-permute-start.5 = (f32[8,768]{1,0:T(8,128)S(1)}, f32[8,768]{1,0:T(8,128)S(1)}, u32[]{:S(2)}, u32[]{:S(2)}) collective-permute-start(f32[8,768]{1,0:T(8,128)S(1)} %get-tuple-element.17), channel_id=1, source_target_pairs={{0,8},{8,0},{16,24},{24,16},{32,40},{40,32},{48,56},{56,48},{1,9},... | collective-permute-start | bytes 73736 | tf_op jit(solution)/shard_map/ppermute | solution.py:263
  109.0 13.5 %copy-start.3 = (bf16[128,2048]{1,0:T(8,128)(2,1)S(1)}, bf16[128,2048]{1,0:T(8,128)(2,1)}, u32[]{:S(2)}) copy-start(bf16[128,2048]{1,0:T(8,128)(2,1)} %get-tuple-element.25) | copy-start | bytes 1572868
  109.0 13.5 %copy-start.4 = (bf16[128,2048]{1,0:T(8,128)(2,1)S(1)}, bf16[128,2048]{1,0:T(8,128)(2,1)}, u32[]{:S(2)}) copy-start(bf16[128,2048]{1,0:T(8,128)(2,1)} %get-tuple-element.27) | copy-start | bytes 1572868
  109.0 16.9 %collective-permute-start.6 = (f32[8,768]{1,0:T(8,128)S(1)}, f32[8,768]{1,0:T(8,128)S(1)}, u32[]{:S(2)}, u32[]{:S(2)}) collective-permute-start(f32[8,768]{1,0:T(8,128)S(1)} %add.75), channel_id=1, source_target_pairs={{0,16},{8,24},{16,0},{24,8},{32,48},{40,56},{48,32},{56,40},{1,17}... | collective-permute-start | bytes 73736 | tf_op jit(solution)/shard_map/ppermute | solution.py:263
  117.2 19.1 %all-to-all-start.2 = ((bf16[8,64,1024]{2,1,0:T(8,128)(2,1)}), bf16[8,64,1024]{2,1,0:T(8,128)(2,1)S(1)}, u32[]{:S(2)}, u32[]{:S(2)}) async-start(bf16[8,64,1024]{2,1,0:T(8,128)(2,1)} %broadcast_in_dim.4), calls=%async_computation.3 | async-start | bytes 2097152 | tf_op jit(solution)/shard_map/all_to_all | solution.py:261
  125.9 10.4 %collective-permute-start.7 = (f32[8,768]{1,0:T(8,128)S(1)}, f32[8,768]{1,0:T(8,128)S(1)}, u32[]{:S(2)}, u32[]{:S(2)}) collective-permute-start(f32[8,768]{1,0:T(8,128)S(1)} %add.76), channel_id=1, source_target_pairs={{0,32},{8,40},{16,48},{24,56},{32,0},{40,8},{48,16},{56,24},{1,33}... | collective-permute-start | bytes 73736 | tf_op jit(solution)/shard_map/ppermute | solution.py:263
  138.2 22.7 %all-to-all-start.3 = ((bf16[4,80,768]{2,1,0:T(8,128)(2,1)}), bf16[4,80,768]{2,1,0:T(8,128)(2,1)S(1)}, u32[]{:S(2)}, u32[]{:S(2)}) async-start(bf16[4,80,768]{2,1,0:T(8,128)(2,1)} %pad_maximum_fusion.3), calls=%async_computation.4 | async-start | bytes 983040 | tf_op jit(solution)/shard_map/all_to_all | solution.py:284
  143.2 14.4 %collective-permute-start.3 = (bf16[256,384]{0,1:T(8,128)(2,1)S(1)}, bf16[256,384]{0,1:T(8,128)(2,1)S(1)}, u32[]{:S(2)}, u32[]{:S(2)}) collective-permute-start(bf16[256,384]{0,1:T(8,128)(2,1)S(1)} %fusion.23), channel_id=1, source_target_pairs={{0,64},{64,0},{1,65},{65,1},{2,66},{66,2},{3,67},{67,3},{4,68},{68... | collective-permute-start | bytes 589832 | tf_op jit(solution)/shard_map/ppermute | solution.py:22
  159.6 3.6 %copy-start.6 = (f32[64,704]{1,0:T(8,128)S(1)}, f32[64,704]{1,0:T(8,128)}, u32[]{:S(2)}) copy-start(f32[64,704]{1,0:T(8,128)} %param.18) | copy-start | bytes 540676
  (3 other events, 6.5 us)
Sparse Core Ops, SparseCore 0:
  29.2 49.3 all-gather.1
  86.6 48.7 reduce-scatter.1

commit v6 on v5

--- a/solution.py
+++ b/solution.py
@@ -26,18 +26,6 @@
     return jnp.where(flag, first, second)
 
 
-def causal_mix(values, filter_taps):
-    length = values.shape[-2]
-    widths = [(0, 0)] * values.ndim
-    widths[-2] = (2, 0)
-    padded = jnp.pad(values, widths)
-    return (
-        filter_taps[0] * padded[..., 0:length, :]
-        + filter_taps[1] * padded[..., 1 : length + 1, :]
-        + filter_taps[2] * padded[..., 2 : length + 2, :]
-    )
-
-
 def moved(values, by):
     length = values.shape[0]
     at = lax.broadcasted_iota(jnp.int32, values.shape, 0)
@@ -52,14 +40,16 @@
     own,
     other,
     cotangent,
-    filters,
+    filters_in,
     weight_out,
     grads_out,
     terms_out,
-    tap_sums,
+    sums_out,
     weight,
     grads,
     terms,
+    filters,
+    tap_sums,
     in_sems,
     out_sems,
 ):
@@ -71,13 +61,14 @@
         pltpu.make_async_copy(gathered.at[y], weight.at[:, y], in_sems.at[y])
         for y in range(n_y)
     ]
+    fetches.append(pltpu.make_async_copy(filters_in, filters, in_sems.at[n_y]))
     for fetch in fetches:
         fetch.start()
+    for fetch in fetches:
+        fetch.wait()
     first, second, third = filters[0:1, :], filters[1:2, :], filters[2:3, :]
     slope = math.sqrt(2.0 / math.pi)
     sums = [jnp.zeros((1, columns), jnp.float32) for _ in range(3)]
-    for fetch in fetches:
-        fetch.wait()
     stores = [pltpu.make_async_copy(weight, weight_out, out_sems.at[0])]
     stores[0].start()
     for part, rows in enumerate((own, other)):
@@ -109,6 +100,8 @@
         [scale * value for value in sums]
         + [jnp.zeros((tap_sums.shape[0] - 3, columns), jnp.float32)]
     )
+    stores.append(pltpu.make_async_copy(tap_sums, sums_out, out_sems.at[2]))
+    stores[2].start()
     for z in range(n_z):
         term = sum(
             lax.dot_general(
@@ -122,7 +115,7 @@
         term = (term * scale).astype(jnp.bfloat16)
         terms[z] = term.reshape(n_y, shard_rows, columns)
         store = pltpu.make_async_copy(
-            terms.at[z], terms_out.at[:, z], out_sems.at[2 + z]
+            terms.at[z], terms_out.at[:, z], out_sems.at[3 + z]
         )
         store.start()
         stores.append(store)
@@ -134,7 +127,7 @@
     n_y, n_z, shard_rows, columns = gathered.shape
     length, depth = own.shape
     whole = pl.BlockSpec(memory_space=pltpu.VMEM)
-    apart = pl.BlockSpec(memory_space=pl.ANY)
+    apart = pl.BlockSpec(memory_space=pltpu.HBM)
     ordered = (n_z, n_y, shard_rows, columns)
     return pl.pallas_call(
         functools.partial(early_kernel, scale),
@@ -144,16 +137,18 @@
             jax.ShapeDtypeStruct(gathered.shape, jnp.bfloat16),
             jax.ShapeDtypeStruct((8, columns), jnp.float32),
         ),
-        in_specs=[apart] + [whole] * 4,
-        out_specs=(apart, apart, apart, whole),
+        in_specs=[apart] + [whole] * 3 + [apart],
+        out_specs=(apart,) * 4,
         scratch_shapes=[
             pltpu.VMEM(ordered, jnp.bfloat16),
             pltpu.VMEM((2 * length, columns), jnp.bfloat16),
             pltpu.VMEM(ordered, jnp.bfloat16),
-            pltpu.SemaphoreType.DMA((n_y,)),
-            pltpu.SemaphoreType.DMA((2 + n_z,)),
+            pltpu.VMEM((8, columns), jnp.float32),
+            pltpu.VMEM((8, columns), jnp.float32),
+            pltpu.SemaphoreType.DMA((n_y + 1,)),
+            pltpu.SemaphoreType.DMA((3 + n_z,)),
         ],
-        compiler_params=pltpu.CompilerParams(vmem_limit_bytes=48 * 1024 * 1024),
+        compiler_params=pltpu.CompilerParams(vmem_limit_bytes=57 * 1024 * 1024),
         cost_estimate=pl.CostEstimate(
             flops=8 * length * depth * columns,
             bytes_accessed=6 * depth * columns + 4 * length * depth,
@@ -163,8 +158,50 @@
     )(gathered, own, other, cotangent, filters)
 
 
-def stored(product):
-    return lax.optimization_barrier(product.astype(jnp.bfloat16)).astype(jnp.float32)
+def late_kernel(weight_in, own, other, filters_in, hidden, weight, filters, in_sems):
+    wide = hidden.shape[2]
+    fetches = [
+        pltpu.make_async_copy(weight_in, weight, in_sems.at[0]),
+        pltpu.make_async_copy(filters_in, filters, in_sems.at[1]),
+    ]
+    for fetch in fetches:
+        fetch.start()
+    for fetch in fetches:
+        fetch.wait()
+    first, second, third = filters[0:1, :], filters[1:2, :], filters[2:3, :]
+    slope = math.sqrt(2.0 / math.pi)
+    for part, rows in enumerate((own, other)):
+        pre = jnp.dot(rows[...], weight[...], preferred_element_type=jnp.float32)
+        pre = pre.astype(jnp.bfloat16).astype(jnp.float32)
+        mixed = first * moved(pre, 2) + second * moved(pre, 1) + third * pre
+        gate, up = mixed[:, :wide], mixed[:, wide:]
+        bend = jnp.tanh(slope * (gate + 0.044715 * (gate * gate * gate)))
+        hidden[part] = (0.5 * gate * (1.0 + bend) * up).astype(jnp.bfloat16)
+
+
+def late_pass(weight, own, other, filters):
+    depth, columns = weight.shape
+    length = own.shape[0]
+    whole = pl.BlockSpec(memory_space=pltpu.VMEM)
+    apart = pl.BlockSpec(memory_space=pltpu.HBM)
+    return pl.pallas_call(
+        late_kernel,
+        out_shape=jax.ShapeDtypeStruct((2, length, columns // 2), jnp.bfloat16),
+        in_specs=[apart, whole, whole, apart],
+        out_specs=whole,
+        scratch_shapes=[
+            pltpu.VMEM(weight.shape, jnp.bfloat16),
+            pltpu.VMEM(filters.shape, jnp.float32),
+            pltpu.SemaphoreType.DMA((2,)),
+        ],
+        compiler_params=pltpu.CompilerParams(vmem_limit_bytes=58 * 1024 * 1024),
+        cost_estimate=pl.CostEstimate(
+            flops=4 * length * depth * columns,
+            bytes_accessed=2 * depth * columns + 4 * length * depth,
+            transcendentals=length * columns,
+        ),
+        name="late_pass",
+    )(weight, own, other, filters)
 
 
 def per_device(
@@ -182,8 +219,8 @@
 ):
     row_count, depth = late_rows.shape
     shard_rows, width_local = gate_weight.shape
-    width = width_local // 2
-    wide = -(-width // 128) * 128
+    wide = -(-width_local // 256) * 128
+    rest = width_local - wide
     n_z = lax.axis_size("zp") * lax.axis_size("zb")
     n_y = lax.axis_size("y")
     n_x = lax.axis_size("x")
@@ -192,20 +229,16 @@
     first_c = lax.axis_index("c") == 0
     rows_scale = (row_count * n_z * n_y) ** (-0.5)
 
-    def widened(array):
+    def low_high(array):
         edges = [(0, 0)] * (array.ndim - 1)
-        return jnp.pad(array, edges + [(0, wide - width)])
+        return array[..., :wide], jnp.pad(array[..., wide:], edges + [(0, wide - rest)])
 
     def halves(array):
-        low, high = widened(array[..., :width]), widened(array[..., width:])
+        low, high = low_high(array)
         return pick(first_z, low, high), pick(first_z, high, low)
 
-    def columns_joined(mine, other):
-        return pick(
-            first_z,
-            jnp.concatenate([mine, other], axis=-1),
-            jnp.concatenate([other, mine], axis=-1),
-        )
+    def joined(low, high):
+        return jnp.concatenate([low, high[..., :rest]], axis=-1)
 
     def partners(late, early):
         cut = row_count // 2
@@ -220,13 +253,11 @@
             jnp.concatenate([low[:cut], high[:cut]]),
         )
 
-    for_z = jnp.stack(
-        [
-            jnp.concatenate([widened(gate_weight[:, at]), widened(up_weight[:, at])], axis=1)
-            for at in (slice(0, width), slice(width, 2 * width))
-        ]
-        * (n_z // 2)
-    )
+    sides = [
+        jnp.concatenate(pair, axis=1)
+        for pair in zip(low_high(gate_weight), low_high(up_weight))
+    ]
+    for_z = jnp.stack(sides * (n_z // 2))
     block = lax.all_to_all(for_z, Z, 0, 0, tiled=True)
     late_other, early_other = partners(late_rows, early_rows)
     cot_mine, cot_other = halves(hidden_cot)
@@ -257,52 +288,44 @@
         chip.reshape(2 * n_x, row_count // n_x, cut), ("zb", "x"), 0, 0, tiled=True
     )
     own = jnp.sum(spread.astype(jnp.float32), axis=0).astype(jnp.bfloat16)
-    copies = jnp.broadcast_to(own[None], (2 * n_x, *own.shape))
-    finished = lax.all_to_all(copies, TP, 0, 0, tiled=True)
+    copies = jnp.broadcast_to(own[None], (n_x, *own.shape))
+    finished = lax.all_to_all(copies, "x", 0, 0, tiled=True).reshape(row_count, cut)
     for step in (1, 2, 4):
         taps = taps + lax.ppermute(taps, "y", [(k, k ^ step) for k in range(n_y)])
     high = lax.reduce_precision(taps, 8, 7)
     taps = jnp.concatenate([high, taps - high]).astype(jnp.bfloat16)
 
-    product = [
-        stored(jnp.dot(rows, weight, preferred_element_type=jnp.float32))
-        for rows in (late_rows, late_other)
-    ]
-    mixed = [causal_mix(values, filters) for values in product]
-    late = [
-        (jax.nn.gelu(values[:, :wide], approximate=True) * values[:, wide:]).astype(
-            jnp.bfloat16
-        )
-        for values in mixed
-    ]
-    late_hidden = columns_joined(late[0][:, :width], swapped(late[1], "zb")[:, :width])
-
-    reduced, finished = lax.optimization_barrier((reduced, finished))
-    reduced = jnp.concatenate(
-        [reduced, jnp.broadcast_to(taps[None], (n_z, *taps.shape))], axis=1
-    )
+    late = late_pass(weight, late_rows, late_other, filters)
+    late_there = swapped(late[1], "zb")
+
+    start = jnp.broadcast_to(taps[None], (n_z, *taps.shape))
+    start = jnp.pad(start, [(0, 0), (shard_rows, 0), (0, 0)])
+    reduced, finished, late_there, start = lax.optimization_barrier(
+        (reduced, finished, late_there, start)
+    )
+    reduced = lax.dynamic_update_slice(start, reduced, (0, 0, 0))
     pieces = lax.all_to_all(reduced, Z, 0, 0, tiled=True)
     pieces = pieces.reshape(2, 2, -1, 2 * wide).astype(jnp.float32)
     pieces = jnp.sum(pieces, axis=0)
     tap_sums = pieces[:, shard_rows:].reshape(2, 2, -1, 2 * wide)
     tap_sums = jnp.sum(tap_sums, axis=1)[:, :3]
     pieces = pieces[:, :shard_rows]
-    gate_tap_sums = jnp.concatenate([tap_sums[0, :, :width], tap_sums[1, :, :width]], axis=1)
-    up_tap_sums = jnp.concatenate(
-        [tap_sums[0, :, wide : wide + width], tap_sums[1, :, wide : wide + width]], axis=1
-    )
-    gate_sum = jnp.concatenate([pieces[0, :, :width], pieces[1, :, :width]], axis=1)
-    up_sum = jnp.concatenate([pieces[0, :, wide : wide + width], pieces[1, :, wide : wide + width]], axis=1)
-
-    finished = finished.reshape(n_x, 2, row_count // n_x, cut)
-    early_grad = finished.transpose(0, 2, 1, 3).reshape(row_count, depth)
+    beside = swapped(finished, "c")
+    early_grad = pick(
+        first_c,
+        jnp.concatenate([finished, beside], axis=1),
+        jnp.concatenate([beside, finished], axis=1),
+    )
+    late_hidden = joined(
+        pick(first_z, late[0], late_there), pick(first_z, late_there, late[0])
+    )
     return (
         late_hidden,
         early_grad,
-        gate_grad_sum + gate_sum,
-        up_grad_sum + up_sum,
-        gate_taps_sum + gate_tap_sums,
-        up_taps_sum + up_tap_sums,
+        gate_grad_sum + joined(pieces[0, :, :wide], pieces[1, :, :wide]),
+        up_grad_sum + joined(pieces[0, :, wide:], pieces[1, :, wide:]),
+        gate_taps_sum + joined(tap_sums[0, :, :wide], tap_sums[1, :, :wide]),
+        up_taps_sum + joined(tap_sums[0, :, wide:], tap_sums[1, :, wide:]),
     )
 
 

time: 173 us -> 169 us (0.977)
  Pallas kernels: 7.92 us -> 16.1 us
  matrix products: 9.96 us -> 3.71 us
  waiting for transfers between devices: 59.3 us -> 54.2 us
  other arithmetic: 12.1 us -> 10.3 us
    pallas_call x0 -> x1, Pallas kernels: none -> 6.59 us  [late_pass(): pl.pallas_call(late_kernel, out_shape=jax.ShapeDtypeStruct((2, length, co...]
    ppermute x5 -> x6, waiting for transfers between devices: 43.3 us -> 36.7 us  [swapped(): return lax.ppermute(values, axis, [(0, 1), (1, 0)])]
    dot_general x2 -> x0, matrix products: 6.25 us -> none  [per_device(): jnp.dot(rows, weight, preferred_element_type=jnp.float32)]
    all_to_all x1, waiting for transfers between devices: 0.01 us -> 5.51 us  [per_device(): pieces = lax.all_to_all(reduced, Z, 0, 0, tiled=True)]
    all_to_all x1, waiting for transfers between devices: 2.88 us -> 0.01 us  [per_device(): lax.all_to_all(chip.reshape(2 * n_x, row_count // n_x, cut), ('zb', 'x'),...]
    ppermute x3, waiting for transfers between devices: 4.61 us -> 2.43 us  [per_device(): taps = taps + lax.ppermute(taps, 'y', [(k, k ^ step) for k in range(n_y)])]
    dynamic_update_slice x0 -> x1, local copies, waits for them, and re-layouts: none -> 1.77 us  [per_device(): reduced = lax.dynamic_update_slice(start, reduced, (0, 0, 0))]
    add x5 -> x4, other arithmetic: 4.1 us -> 2.62 us  [the longest x1 0.71 us: per_device(): gate_grad_sum + joined(pieces[0, :, :wide], pieces[1, :, :wide])]
  transfers between devices with their start and end apart: 13 -> 14, of which waited for: 8 -> 8; matrix products, arithmetic and copies ran while one was open for 13% -> 9% of each run, Pallas kernels for 0% -> 4%
where the time goes in v6:
time: 169 us; the launch traced here: 168 us
  waiting for transfers between devices  54.2 us (32%)
  starting transfers between devices  40.4 us (24%)
  blocking collectives  18.8 us (11%)
  Pallas kernels  16.1 us (10%)
  between operations  14.5 us (9%)
  other arithmetic  10.3 us (6%)
  local copies, waits for them, and re-layouts  9.43 us (6%)
  matrix products  3.71 us (2%)
    ppermute x6, waiting for transfers between devices, swapped(): return lax.ppermute(values, axis, [(0, 1), (1, 0)])  36.7 us
    all_to_all x1, blocking collectives, per_device(): block = lax.all_to_all(for_z, Z, 0, 0, tiled=True)  18.8 us
    ppermute x6, starting transfers between devices, swapped(): return lax.ppermute(values, axis, [(0, 1), (1, 0)])  13.6 us
    ppermute x3, starting transfers between devices, per_device(): taps = taps + lax.ppermute(taps, 'y', [(k, k ^ step) for k in range(n_y)])  11.2 us
    all_gather x1, waiting for transfers between devices, per_device(): weight = lax.all_gather(block, 'y').reshape(n_y, n_z, shard_rows, 2 * wide)  9.55 us
    pallas_call x1, Pallas kernels, early_pass(): pl.pallas_call(functools.partial(early_kernel, scale), out_shape=(jax.Sha...  9.54 us
    pallas_call x1, Pallas kernels, late_pass(): pl.pallas_call(late_kernel, out_shape=jax.ShapeDtypeStruct((2, length, co...  6.59 us
    all_to_all x1, starting transfers between devices, per_device(): lax.all_to_all(chip.reshape(2 * n_x, row_count // n_x, cut), ('zb', 'x'),...  5.88 us
  transfers between devices with their start and end apart: 14, of which 8 were waited for; matrix products, arithmetic and copies ran while one was open for 9% of the time, Pallas kernels for 4%

profile of v6, /device:TPU:6, one launch (start us, length us, event | category | flops | bytes accessed | tf_op | source)
XLA Modules:
  0.0 167.6 jit_solution(5949217197996055038)
XLA Ops:
  10.7 18.8 %all_to_all.20 = bf16[4,64,768]{2,1,0:T(8,128)(2,1)} all-to-all(bf16[4,64,768]{2,1,0:T(8,128)(2,1)S(1)} %pad_maximum_fusion.4), channel_id=1, replica_groups=mesh['rep'=2,'zp'=2,'zb'=2,'y'=8,'x'=4,'c'=2] {'zp','zb'}, dimensions={0} | all-to-all | bytes 786432 | tf_op jit(solution)/shard_map/all_to_all | solution.py:261
  29.9 2.3 %collective-permute-start = (bf16[256,2048]{1,0:T(8,128)(2,1)S(1)}, bf16[256,2048]{1,0:T(8,128)(2,1)S(1)}, u32[]{:S(2)}, u32[]{:S(2)}) collective-permute-start(bf16[256,2048]{1,0:T(8,128)(2,1)S(1)} %pad_maximum_fusion), channel_id=1, source_target_pairs={{0,64},{64,0},{1,65},{65,1},{2,66},{66,2},{3,67},{67,3},{4,68},{68... | collective-permute-start | bytes 3145736 | tf_op jit(solution)/shard_map/ppermute | solution.py:22
  32.2 23.6 %collective-permute-done = bf16[256,2048]{1,0:T(8,128)(2,1)S(1)} collective-permute-done((bf16[256,2048]{1,0:T(8,128)(2,1)S(1)}, bf16[256,2048]{1,0:T(8,128)(2,1)S(1)}, u32[]{:S(2)}, u32[]{:S(2)}) %collective-permute-start) | collective-permute-done | bytes 1048608 | tf_op jit(solution)/shard_map/ppermute | solution.py:22
  55.8 1.9 %collective-permute-start.1 = (bf16[256,2048]{1,0:T(8,128)(2,1)S(1)}, bf16[256,2048]{1,0:T(8,128)(2,1)S(1)}, u32[]{:S(2)}, u32[]{:S(2)}) collective-permute-start(bf16[256,2048]{1,0:T(8,128)(2,1)S(1)} %collective-permute-done), channel_id=1, source_target_pairs={{0,1},{1,0},{2,3},{3,2},{4,5},{5,4},{6,7},{7,6},{8,9},{9,8},{10,11... | collective-permute-start | bytes 3145736 | tf_op jit(solution)/shard_map/ppermute | solution.py:22
  58.1 2.2 %collective-permute-start.2 = (bf16[256,384]{1,0:T(8,128)(2,1)S(1)}, bf16[256,384]{1,0:T(8,128)(2,1)S(1)}, u32[]{:S(2)}, u32[]{:S(2)}) collective-permute-start(bf16[256,384]{1,0:T(8,128)(2,1)S(1)} %get-tuple-element.49), channel_id=1, source_target_pairs={{0,64},{64,0},{1,65},{65,1},{2,66},{66,2},{3,67},{67,3},{4,68},{68... | collective-permute-start | bytes 589832 | tf_op jit(solution)/shard_map/ppermute | solution.py:22
  61.0 6.3 %collective-permute-done.2 = bf16[256,384]{1,0:T(8,128)(2,1)S(1)} collective-permute-done((bf16[256,384]{1,0:T(8,128)(2,1)S(1)}, bf16[256,384]{1,0:T(8,128)(2,1)S(1)}, u32[]{:S(2)}, u32[]{:S(2)}) %collective-permute-start.2) | collective-permute-done | bytes 196640 | tf_op jit(solution)/shard_map/ppermute | solution.py:22
  69.5 9.5 %all-gather.2.cloned.1.call-done = bf16[8,256,768]{2,1,0:T(8,128)(2,1)} async-done(((bf16[1,256,768]{2,1,0:T(8,128)(2,1)}), bf16[8,256,768]{2,1,0:T(8,128)(2,1)}) %all-gather.2.cloned.1.call-update) | async-done | bytes 3145744 | tf_op jit(solution)/shard_map/all_gather | solution.py:269
  79.1 9.5 %early_pass.1 = (bf16[4,8,64,768]{3,2,1,0:T(8,128)(2,1)}, bf16[512,768]{1,0:T(8,128)(2,1)}, bf16[8,4,64,768]{3,2,1,0:T(8,128)(2,1)}, f32[8,768]{1,0:T(8,128)}) custom-call(bf16[8,4,64,768]{3,2,1,0:T(8,128)(2,1)} %bitcast.63, bf16[256,2048]{1,0:T(8,128)(2,1)} %own.2, bf16[256,2048]{1,0:T(8,128)(2,1)} %pad_maximum_fusion.1.other, ...), custom_call_target="tpu_custom_call" | custom-call | flops 3221225472 | bytes 11534336 | tf_op jit(solution)/shard_map/early_pass/pallas_call | solution.py:132
  89.7 3.7 %convolution_convert_fusion = bf16[512,2048]{1,0:T(8,128)(2,1)S(1)} fusion(bf16[512,768]{1,0:T(8,128)(2,1)S(1)} %copy-done.10, bf16[2048,768]{1,0:T(8,128)(2,1)} %bitcast.64), kind=kOutput, calls=%fused_computation | convolution fusion | flops 1611661312 | bytes 6029312 | tf_op jit(solution)/shard_map/dot_general | solution.py:277
  93.6 1.9 %collective-permute-start.3 = (bf16[512,1024]{1,0:T(8,128)(2,1)S(1)}, bf16[512,1024]{1,0:T(8,128)(2,1)S(1)}, u32[]{:S(2)}, u32[]{:S(2)}) collective-permute-start(bf16[512,1024]{1,0:T(8,128)(2,1)S(1)} %broadcast_select_fusion), channel_id=1, source_target_pairs={{0,1},{1,0},{2,3},{3,2},{4,5},{5,4},{6,7},{7,6},{8,9},{9,8},{10,11... | collective-permute-start | bytes 3145736 | tf_op jit(solution)/shard_map/ppermute | solution.py:22
  95.5 2.6 %collective-permute-done.3 = bf16[512,1024]{1,0:T(8,128)(2,1)S(1)} collective-permute-done((bf16[512,1024]{1,0:T(8,128)(2,1)S(1)}, bf16[512,1024]{1,0:T(8,128)(2,1)S(1)}, u32[]{:S(2)}, u32[]{:S(2)}) %collective-permute-start.3) | collective-permute-done | bytes 1048608 | tf_op jit(solution)/shard_map/ppermute | solution.py:22
  99.9 5.9 %all-to-all-start.1 = ((bf16[8,64,1024]{2,1,0:T(8,128)(2,1)}), bf16[8,64,1024]{2,1,0:T(8,128)(2,1)S(1)}, u32[]{:S(2)}, u32[]{:S(2)}) async-start(bf16[8,64,1024]{2,1,0:T(8,128)(2,1)} %bitcast.12), calls=%async_computation.2 | async-start | bytes 2097152 | tf_op jit(solution)/shard_map/all_to_all | solution.py:287
  105.8 2.9 %collective-permute-start.5 = (f32[8,768]{1,0:T(8,128)S(1)}, f32[8,768]{1,0:T(8,128)S(1)}, u32[]{:S(2)}, u32[]{:S(2)}) collective-permute-start(f32[8,768]{1,0:T(8,128)S(1)} %copy-done.5), channel_id=1, source_target_pairs={{0,8},{8,0},{16,24},{24,16},{32,40},{40,32},{48,56},{56,48},{1,9},... | collective-permute-start | bytes 73736 | tf_op jit(solution)/shard_map/ppermute | solution.py:294
  109.7 2.4 %collective-permute-done.5 = f32[8,768]{1,0:T(8,128)S(1)} collective-permute-done((f32[8,768]{1,0:T(8,128)S(1)}, f32[8,768]{1,0:T(8,128)S(1)}, u32[]{:S(2)}, u32[]{:S(2)}) %collective-permute-start.5) | collective-permute-done | bytes 24608 | tf_op jit(solution)/shard_map/ppermute | solution.py:294
  112.2 3.6 %collective-permute-start.6 = (f32[8,768]{1,0:T(8,128)S(1)}, f32[8,768]{1,0:T(8,128)S(1)}, u32[]{:S(2)}, u32[]{:S(2)}) collective-permute-start(f32[8,768]{1,0:T(8,128)S(1)} %add.41), channel_id=1, source_target_pairs={{0,16},{8,24},{16,0},{24,8},{32,48},{40,56},{48,32},{56,40},{1,17}... | collective-permute-start | bytes 73736 | tf_op jit(solution)/shard_map/ppermute | solution.py:294
  115.8 6.6 %late_pass.1 = bf16[2,256,384]{2,1,0:T(8,128)(2,1)} custom-call(bf16[2048,768]{1,0:T(8,128)(2,1)} %bitcast.65, bf16[256,2048]{1,0:T(8,128)(2,1)} %own.3, bf16[256,2048]{1,0:T(8,128)(2,1)} %pad_maximum_fusion.2.other, f32[8,768]{1,0:T(8,128)} %fusion.9.filters_in), custom_call_target="tpu_custom_call" | custom-call | flops 1610612736 | bytes 5242880 | tf_op jit(solution)/shard_map/late_pass/pallas_call | solution.py:187
  122.4 4.7 %collective-permute-start.7 = (f32[8,768]{1,0:T(8,128)S(1)}, f32[8,768]{1,0:T(8,128)S(1)}, u32[]{:S(2)}, u32[]{:S(2)}) collective-permute-start(f32[8,768]{1,0:T(8,128)S(1)} %add.42), channel_id=1, source_target_pairs={{0,32},{8,40},{16,48},{24,56},{32,0},{40,8},{48,16},{56,24},{1,33}... | collective-permute-start | bytes 73736 | tf_op jit(solution)/shard_map/ppermute | solution.py:294
  128.2 4.8 %all-to-all-start.2 = ((bf16[4,64,1024]{2,1,0:T(8,128)(2,1)}), bf16[4,64,1024]{2,1,0:T(8,128)(2,1)S(1)}, u32[]{:S(2)}, u32[]{:S(2)}) async-start(bf16[4,64,1024]{2,1,0:T(8,128)(2,1)} %broadcast_in_dim.4), calls=%async_computation.3 | async-start | bytes 1048576 | tf_op jit(solution)/shard_map/all_to_all | solution.py:292
  133.0 3.4 %collective-permute-start.4 = (bf16[256,384]{1,0:T(8,128)(2,1)S(1)}, bf16[256,384]{1,0:T(8,128)(2,1)S(1)}, u32[]{:S(2)}, u32[]{:S(2)}) collective-permute-start(bf16[256,384]{1,0:T(8,128)(2,1)S(1)} %get-tuple-element.46), channel_id=1, source_target_pairs={{0,64},{64,0},{1,65},{65,1},{2,66},{66,2},{3,67},{67,3},{4,68},{68... | collective-permute-start | bytes 589832 | tf_op jit(solution)/shard_map/ppermute | solution.py:22
  137.3 3.3 %collective-permute-done.4 = bf16[256,384]{1,0:T(8,128)(2,1)S(1)} collective-permute-done((bf16[256,384]{1,0:T(8,128)(2,1)S(1)}, bf16[256,384]{1,0:T(8,128)(2,1)S(1)}, u32[]{:S(2)}, u32[]{:S(2)}) %collective-permute-start.4) | collective-permute-done | bytes 196640 | tf_op jit(solution)/shard_map/ppermute | solution.py:22
  140.6 1.8 %constant_dynamic-update-slice_fusion = bf16[4,80,768]{2,1,0:T(8,128)(2,1)} fusion(bf16[4,80,768]{2,1,0:T(8,128)(2,1)} %pad.35, bf16[4,64,768]{2,1,0:T(8,128)(2,1)} %bitcast.59), kind=kLoop, calls=%fused_computation.56 | loop fusion | bytes 786432 | tf_op jit(solution)/shard_map/dynamic_update_slice | solution.py:306
  142.4 4.9 %all-to-all-start.3 = ((bf16[4,80,768]{2,1,0:T(8,128)(2,1)}), bf16[4,80,768]{2,1,0:T(8,128)(2,1)S(1)}, u32[]{:S(2)}, u32[]{:S(2)}) async-start(bf16[4,80,768]{2,1,0:T(8,128)(2,1)} %constant_dynamic-update-slice_fusion), calls=%async_computation.4 | async-start | bytes 983040 | tf_op jit(solution)/shard_map/all_to_all | solution.py:307
  147.3 1.9 %collective-permute-start.8 = (bf16[256,1024]{1,0:T(8,128)(2,1)S(1)}, bf16[256,1024]{1,0:T(8,128)(2,1)S(1)}, u32[]{:S(2)}, u32[]{:S(2)}) collective-permute-start(bf16[256,1024]{1,0:T(8,128)(2,1)S(1)} %bitcast.51), channel_id=1, source_target_pairs={{0,1},{1,0},{2,3},{3,2},{4,5},{5,4},{6,7},{7,6},{8,9},{9,8},{10,11... | collective-permute-start | bytes 1572872 | tf_op jit(solution)/shard_map/ppermute | solution.py:22
  152.4 5.5 %all-to-all-done.3 = bf16[4,80,768]{2,1,0:T(8,128)(2,1)S(1)} async-done(((bf16[4,80,768]{2,1,0:T(8,128)(2,1)}), bf16[4,80,768]{2,1,0:T(8,128)(2,1)S(1)}, u32[]{:S(2)}, u32[]{:S(2)}) %all-to-all-start.3) | async-done | bytes 491552 | tf_op jit(solution)/shard_map/all_to_all | solution.py:307
  (86 shorter events, 18.9 us)
Async XLA Ops:
  7.2 22.4 %copy-start = (bf16[256,2048]{1,0:T(8,128)(2,1)S(1)}, bf16[256,2048]{1,0:T(8,128)(2,1)}, u32[]{:S(2)}) copy-start(bf16[256,2048]{1,0:T(8,128)(2,1)} %own.2) | copy-start | bytes 3145732
  7.2 22.4 %copy-start.1 = (bf16[256,2048]{1,0:T(8,128)(2,1)S(1)}, bf16[256,2048]{1,0:T(8,128)(2,1)}, u32[]{:S(2)}) copy-start(bf16[256,2048]{1,0:T(8,128)(2,1)} %own.3) | copy-start | bytes 3145732
  7.2 71.9 %all-gather.2.cloned.1.call-start = ((), (), s32[]{:S(2)}) async-start(), calls=%async_computation.5 | async-start | bytes 3538944 | tf_op jit(solution)/shard_map/all_gather | solution.py:269
  29.5 111.1 %reduce-scatter.2.cloned.1.call-start = ((), (), s32[]{:S(2)}) async-start(), calls=%async_computation.6 | async-start | bytes 3538944 | tf_op jit(solution)/shard_map/reduce_scatter | solution.py:275
  29.7 27.9 %slice-start = ((bf16[256,704]{0,1:T(8,128)(2,1)}), bf16[256,320]{0,1:T(8,128)(2,1)S(1)}, s32[]{:S(2)}) async-start(bf16[256,704]{0,1:T(8,128)(2,1)} %param.13), calls=%async_computation.7 | async-start | bytes 327680 | tf_op jit(solution)/shard_map/slice | solution.py:234
  29.7 28.1 %slice-start.1 = ((bf16[256,704]{0,1:T(8,128)(2,1)}), bf16[256,384]{0,1:T(8,128)(2,1)S(1)}, s32[]{:S(2)}) async-start(bf16[256,704]{0,1:T(8,128)(2,1)} %param.13), calls=%async_computation.8 | async-start | bytes 393216 | tf_op jit(solution)/shard_map/slice | solution.py:234
  29.8 30.6 %copy-start.6 = (bf16[3,704]{1,0:T(4,128)(2,1)S(1)}, bf16[3,704]{1,0:T(4,128)(2,1)}, u32[]{:S(2)}) copy-start(bf16[3,704]{1,0:T(4,128)(2,1)} %param.16) | copy-start | bytes 12676
  29.8 30.6 %slice-start.2 = ((bf16[3,704]{1,0:T(4,128)(2,1)}), bf16[3,320]{1,0:T(4,128)(2,1)S(1)}, s32[]{:S(2)}) async-start(bf16[3,704]{1,0:T(4,128)(2,1)} %param.16), calls=%async_computation.9 | async-start | bytes 6144 | tf_op jit(solution)/shard_map/slice | solution.py:234
  29.8 30.6 %copy-start.7 = (bf16[3,704]{1,0:T(4,128)(2,1)S(1)}, bf16[3,704]{1,0:T(4,128)(2,1)}, u32[]{:S(2)}) copy-start(bf16[3,704]{1,0:T(4,128)(2,1)} %param.17) | copy-start | bytes 12676
  29.8 30.6 %slice-start.3 = ((bf16[3,704]{1,0:T(4,128)(2,1)}), bf16[3,320]{1,0:T(4,128)(2,1)S(1)}, s32[]{:S(2)}) async-start(bf16[3,704]{1,0:T(4,128)(2,1)} %param.17), calls=%async_computation.10 | async-start | bytes 6144 | tf_op jit(solution)/shard_map/slice | solution.py:234
  29.9 25.8 %collective-permute-start = (bf16[256,2048]{1,0:T(8,128)(2,1)S(1)}, bf16[256,2048]{1,0:T(8,128)(2,1)S(1)}, u32[]{:S(2)}, u32[]{:S(2)}) collective-permute-start(bf16[256,2048]{1,0:T(8,128)(2,1)S(1)} %pad_maximum_fusion), channel_id=1, source_target_pairs={{0,64},{64,0},{1,65},{65,1},{2,66},{66,2},{3,67},{67,3},{4,68},{68... | collective-permute-start | bytes 3145736 | tf_op jit(solution)/shard_map/ppermute | solution.py:22
  55.8 12.4 %collective-permute-start.1 = (bf16[256,2048]{1,0:T(8,128)(2,1)S(1)}, bf16[256,2048]{1,0:T(8,128)(2,1)S(1)}, u32[]{:S(2)}, u32[]{:S(2)}) collective-permute-start(bf16[256,2048]{1,0:T(8,128)(2,1)S(1)} %collective-permute-done), channel_id=1, source_target_pairs={{0,1},{1,0},{2,3},{3,2},{4,5},{5,4},{6,7},{7,6},{8,9},{9,8},{10,11... | collective-permute-start | bytes 3145736 | tf_op jit(solution)/shard_map/ppermute | solution.py:22
  58.1 9.2 %collective-permute-start.2 = (bf16[256,384]{1,0:T(8,128)(2,1)S(1)}, bf16[256,384]{1,0:T(8,128)(2,1)S(1)}, u32[]{:S(2)}, u32[]{:S(2)}) collective-permute-start(bf16[256,384]{1,0:T(8,128)(2,1)S(1)} %get-tuple-element.49), channel_id=1, source_target_pairs={{0,64},{64,0},{1,65},{65,1},{2,66},{66,2},{3,67},{67,3},{4,68},{68... | collective-permute-start | bytes 589832 | tf_op jit(solution)/shard_map/ppermute | solution.py:22
  93.6 4.6 %collective-permute-start.3 = (bf16[512,1024]{1,0:T(8,128)(2,1)S(1)}, bf16[512,1024]{1,0:T(8,128)(2,1)S(1)}, u32[]{:S(2)}, u32[]{:S(2)}) collective-permute-start(bf16[512,1024]{1,0:T(8,128)(2,1)S(1)} %broadcast_select_fusion), channel_id=1, source_target_pairs={{0,1},{1,0},{2,3},{3,2},{4,5},{5,4},{6,7},{7,6},{8,9},{9,8},{10,11... | collective-permute-start | bytes 3145736 | tf_op jit(solution)/shard_map/ppermute | solution.py:22
  99.9 27.2 %all-to-all-start.1 = ((bf16[8,64,1024]{2,1,0:T(8,128)(2,1)}), bf16[8,64,1024]{2,1,0:T(8,128)(2,1)S(1)}, u32[]{:S(2)}, u32[]{:S(2)}) async-start(bf16[8,64,1024]{2,1,0:T(8,128)(2,1)} %bitcast.12), calls=%async_computation.2 | async-start | bytes 2097152 | tf_op jit(solution)/shard_map/all_to_all | solution.py:287
  105.8 6.4 %collective-permute-start.5 = (f32[8,768]{1,0:T(8,128)S(1)}, f32[8,768]{1,0:T(8,128)S(1)}, u32[]{:S(2)}, u32[]{:S(2)}) collective-permute-start(f32[8,768]{1,0:T(8,128)S(1)} %copy-done.5), channel_id=1, source_target_pairs={{0,8},{8,0},{16,24},{24,16},{32,40},{40,32},{48,56},{56,48},{1,9},... | collective-permute-start | bytes 73736 | tf_op jit(solution)/shard_map/ppermute | solution.py:294
  112.2 10.2 %collective-permute-start.6 = (f32[8,768]{1,0:T(8,128)S(1)}, f32[8,768]{1,0:T(8,128)S(1)}, u32[]{:S(2)}, u32[]{:S(2)}) collective-permute-start(f32[8,768]{1,0:T(8,128)S(1)} %add.41), channel_id=1, source_target_pairs={{0,16},{8,24},{16,0},{24,8},{32,48},{40,56},{48,32},{56,40},{1,17}... | collective-permute-start | bytes 73736 | tf_op jit(solution)/shard_map/ppermute | solution.py:294
  122.4 10.6 %copy-start.2 = (bf16[2,256,384]{2,1,0:T(8,128)(2,1)S(1)}, bf16[2,256,384]{2,1,0:T(8,128)(2,1)}, u32[]{:S(2)}) copy-start(bf16[2,256,384]{2,1,0:T(8,128)(2,1)} %late_pass.1) | copy-start | bytes 1179652
  122.4 14.0 %collective-permute-start.7 = (f32[8,768]{1,0:T(8,128)S(1)}, f32[8,768]{1,0:T(8,128)S(1)}, u32[]{:S(2)}, u32[]{:S(2)}) collective-permute-start(f32[8,768]{1,0:T(8,128)S(1)} %add.42), channel_id=1, source_target_pairs={{0,32},{8,40},{16,48},{24,56},{32,0},{40,8},{48,16},{56,24},{1,33}... | collective-permute-start | bytes 73736 | tf_op jit(solution)/shard_map/ppermute | solution.py:294
  128.2 12.4 %all-to-all-start.2 = ((bf16[4,64,1024]{2,1,0:T(8,128)(2,1)}), bf16[4,64,1024]{2,1,0:T(8,128)(2,1)S(1)}, u32[]{:S(2)}, u32[]{:S(2)}) async-start(bf16[4,64,1024]{2,1,0:T(8,128)(2,1)} %broadcast_in_dim.4), calls=%async_computation.3 | async-start | bytes 1048576 | tf_op jit(solution)/shard_map/all_to_all | solution.py:292
  133.0 7.6 %collective-permute-start.4 = (bf16[256,384]{1,0:T(8,128)(2,1)S(1)}, bf16[256,384]{1,0:T(8,128)(2,1)S(1)}, u32[]{:S(2)}, u32[]{:S(2)}) collective-permute-start(bf16[256,384]{1,0:T(8,128)(2,1)S(1)} %get-tuple-element.46), channel_id=1, source_target_pairs={{0,64},{64,0},{1,65},{65,1},{2,66},{66,2},{3,67},{67,3},{4,68},{68... | collective-permute-start | bytes 589832 | tf_op jit(solution)/shard_map/ppermute | solution.py:22
  142.4 15.6 %all-to-all-start.3 = ((bf16[4,80,768]{2,1,0:T(8,128)(2,1)}), bf16[4,80,768]{2,1,0:T(8,128)(2,1)S(1)}, u32[]{:S(2)}, u32[]{:S(2)}) async-start(bf16[4,80,768]{2,1,0:T(8,128)(2,1)} %constant_dynamic-update-slice_fusion), calls=%async_computation.4 | async-start | bytes 983040 | tf_op jit(solution)/shard_map/all_to_all | solution.py:307
  147.3 3.8 %collective-permute-start.8 = (bf16[256,1024]{1,0:T(8,128)(2,1)S(1)}, bf16[256,1024]{1,0:T(8,128)(2,1)S(1)}, u32[]{:S(2)}, u32[]{:S(2)}) collective-permute-start(bf16[256,1024]{1,0:T(8,128)(2,1)S(1)} %bitcast.51), channel_id=1, source_target_pairs={{0,1},{1,0},{2,3},{3,2},{4,5},{5,4},{6,7},{7,6},{8,9},{9,8},{10,11... | collective-permute-start | bytes 1572872 | tf_op jit(solution)/shard_map/ppermute | solution.py:22
  150.2 9.8 %copy-start.4 = (f32[64,704]{1,0:T(8,128)S(1)}, f32[64,704]{1,0:T(8,128)}, u32[]{:S(2)}) copy-start(f32[64,704]{1,0:T(8,128)} %param.18) | copy-start | bytes 540676
  (5 other events, 33.6 us)
Sparse Core Ops, SparseCore 0:
  29.7 49.3 all-gather.1
  88.8 49.2 reduce-scatter.1

commit v7 on v6

--- a/solution.py
+++ b/solution.py
@@ -37,9 +37,10 @@
 def early_kernel(
     scale,
     gathered,
-    own,
-    other,
-    cotangent,
+    own_in,
+    low_in,
+    high_in,
+    cotangent_in,
     filters_in,
     weight_out,
     grads_out,
@@ -48,6 +49,9 @@
     weight,
     grads,
     terms,
+    own,
+    other,
+    cotangent,
     filters,
     tap_sums,
     in_sems,
@@ -55,13 +59,24 @@
 ):
     n_y, n_z, shard_rows, columns = gathered.shape
     length = own.shape[0]
+    cut = length // 2
     wide = columns // 2
     span = n_y * shard_rows
     fetches = [
         pltpu.make_async_copy(gathered.at[y], weight.at[:, y], in_sems.at[y])
         for y in range(n_y)
     ]
-    fetches.append(pltpu.make_async_copy(filters_in, filters, in_sems.at[n_y]))
+    pairs = (
+        (own_in, own),
+        (filters_in, filters),
+        (cotangent_in, cotangent),
+        (low_in.at[:cut], other.at[:cut]),
+        (high_in.at[:cut], other.at[cut:]),
+    )
+    fetches += [
+        pltpu.make_async_copy(source, target, in_sems.at[n_y + at])
+        for at, (source, target) in enumerate(pairs)
+    ]
     for fetch in fetches:
         fetch.start()
     for fetch in fetches:
@@ -123,10 +138,9 @@
         store.wait()
 
 
-def early_pass(scale, gathered, own, other, cotangent, filters):
+def early_pass(scale, gathered, own, low, high, cotangent, filters):
     n_y, n_z, shard_rows, columns = gathered.shape
     length, depth = own.shape
-    whole = pl.BlockSpec(memory_space=pltpu.VMEM)
     apart = pl.BlockSpec(memory_space=pltpu.HBM)
     ordered = (n_z, n_y, shard_rows, columns)
     return pl.pallas_call(
@@ -137,15 +151,18 @@
             jax.ShapeDtypeStruct(gathered.shape, jnp.bfloat16),
             jax.ShapeDtypeStruct((8, columns), jnp.float32),
         ),
-        in_specs=[apart] + [whole] * 3 + [apart],
+        in_specs=[apart] * 6,
         out_specs=(apart,) * 4,
         scratch_shapes=[
             pltpu.VMEM(ordered, jnp.bfloat16),
             pltpu.VMEM((2 * length, columns), jnp.bfloat16),
             pltpu.VMEM(ordered, jnp.bfloat16),
+            pltpu.VMEM(own.shape, jnp.bfloat16),
+            pltpu.VMEM(own.shape, jnp.bfloat16),
+            pltpu.VMEM(cotangent.shape, jnp.bfloat16),
             pltpu.VMEM((8, columns), jnp.float32),
             pltpu.VMEM((8, columns), jnp.float32),
-            pltpu.SemaphoreType.DMA((n_y + 1,)),
+            pltpu.SemaphoreType.DMA((n_y + 5,)),
             pltpu.SemaphoreType.DMA((3 + n_z,)),
         ],
         compiler_params=pltpu.CompilerParams(vmem_limit_bytes=57 * 1024 * 1024),
@@ -155,14 +172,35 @@
             transcendentals=length * columns,
         ),
         name="early_pass",
-    )(gathered, own, other, cotangent, filters)
-
-
-def late_kernel(weight_in, own, other, filters_in, hidden, weight, filters, in_sems):
-    wide = hidden.shape[2]
+    )(gathered, own, low, high, cotangent, filters)
+
+
+def late_kernel(
+    weight_in,
+    own_in,
+    low_in,
+    high_in,
+    filters_in,
+    mine,
+    theirs,
+    weight,
+    own,
+    other,
+    filters,
+    in_sems,
+):
+    length, wide = mine.shape
+    cut = length // 2
+    pairs = (
+        (own_in, own),
+        (weight_in, weight),
+        (filters_in, filters),
+        (low_in.at[cut:], other.at[:cut]),
+        (high_in.at[cut:], other.at[cut:]),
+    )
     fetches = [
-        pltpu.make_async_copy(weight_in, weight, in_sems.at[0]),
-        pltpu.make_async_copy(filters_in, filters, in_sems.at[1]),
+        pltpu.make_async_copy(source, target, in_sems.at[at])
+        for at, (source, target) in enumerate(pairs)
     ]
     for fetch in fetches:
         fetch.start()
@@ -170,29 +208,32 @@
         fetch.wait()
     first, second, third = filters[0:1, :], filters[1:2, :], filters[2:3, :]
     slope = math.sqrt(2.0 / math.pi)
-    for part, rows in enumerate((own, other)):
+    for rows, hidden in ((other, theirs), (own, mine)):
         pre = jnp.dot(rows[...], weight[...], preferred_element_type=jnp.float32)
         pre = pre.astype(jnp.bfloat16).astype(jnp.float32)
         mixed = first * moved(pre, 2) + second * moved(pre, 1) + third * pre
         gate, up = mixed[:, :wide], mixed[:, wide:]
         bend = jnp.tanh(slope * (gate + 0.044715 * (gate * gate * gate)))
-        hidden[part] = (0.5 * gate * (1.0 + bend) * up).astype(jnp.bfloat16)
-
-
-def late_pass(weight, own, other, filters):
+        hidden[...] = (0.5 * gate * (1.0 + bend) * up).astype(jnp.bfloat16)
+
+
+def late_pass(weight, own, low, high, filters):
     depth, columns = weight.shape
     length = own.shape[0]
     whole = pl.BlockSpec(memory_space=pltpu.VMEM)
     apart = pl.BlockSpec(memory_space=pltpu.HBM)
+    part = jax.ShapeDtypeStruct((length, columns // 2), jnp.bfloat16)
     return pl.pallas_call(
         late_kernel,
-        out_shape=jax.ShapeDtypeStruct((2, length, columns // 2), jnp.bfloat16),
-        in_specs=[apart, whole, whole, apart],
-        out_specs=whole,
+        out_shape=(part, part),
+        in_specs=[apart] * 5,
+        out_specs=(whole, whole),
         scratch_shapes=[
             pltpu.VMEM(weight.shape, jnp.bfloat16),
+            pltpu.VMEM(own.shape, jnp.bfloat16),
+            pltpu.VMEM(own.shape, jnp.bfloat16),
             pltpu.VMEM(filters.shape, jnp.float32),
-            pltpu.SemaphoreType.DMA((2,)),
+            pltpu.SemaphoreType.DMA((5,)),
         ],
         compiler_params=pltpu.CompilerParams(vmem_limit_bytes=58 * 1024 * 1024),
         cost_estimate=pl.CostEstimate(
@@ -201,7 +242,29 @@
             transcendentals=length * columns,
         ),
         name="late_pass",
-    )(weight, own, other, filters)
+    )(weight, own, low, high, filters)
+
+
+def pack_kernel(gate, up, packed):
+    wide = packed.shape[2] // 2
+    rows, width = gate.shape
+    blank = jnp.zeros((rows, 2 * wide - width), packed.dtype)
+    for at, source in ((0, gate), (wide, up)):
+        low = source[:, :wide]
+        high = jnp.concatenate([source[:, wide:], blank], axis=1)
+        for z in range(packed.shape[0]):
+            packed[z, :, at : at + wide] = high if z % 2 else low
+
+
+def packed_halves(gate, up, wide, count):
+    whole = pl.BlockSpec(memory_space=pltpu.VMEM)
+    return pl.pallas_call(
+        pack_kernel,
+        out_shape=jax.ShapeDtypeStruct((count, gate.shape[0], 2 * wide), gate.dtype),
+        in_specs=[whole] * 2,
+        out_specs=whole,
+        name="pack_halves",
+    )(gate, up)
 
 
 def per_device(
@@ -240,26 +303,15 @@
     def joined(low, high):
         return jnp.concatenate([low, high[..., :rest]], axis=-1)
 
-    def partners(late, early):
-        cut = row_count // 2
-        sent = jnp.concatenate(
-            [pick(first_c, rows[:cut], rows[cut:]) for rows in (early, late)]
-        )
-        here = swapped(sent, "zb")
-        there = swapped(here, "c")
-        low, high = pick(first_c, here, there), pick(first_c, there, here)
-        return (
-            jnp.concatenate([low[cut:], high[cut:]]),
-            jnp.concatenate([low[:cut], high[:cut]]),
-        )
-
-    sides = [
-        jnp.concatenate(pair, axis=1)
-        for pair in zip(low_high(gate_weight), low_high(up_weight))
-    ]
-    for_z = jnp.stack(sides * (n_z // 2))
+    for_z = packed_halves(gate_weight, up_weight, wide, n_z)
     block = lax.all_to_all(for_z, Z, 0, 0, tiled=True)
-    late_other, early_other = partners(late_rows, early_rows)
+    half = row_count // 2
+    sent = jnp.concatenate(
+        [pick(first_c, rows[:half], rows[half:]) for rows in (early_rows, late_rows)]
+    )
+    here = swapped(sent, "zb")
+    there = swapped(here, "c")
+    low, high = pick(first_c, here, there), pick(first_c, there, here)
     cot_mine, cot_other = halves(hidden_cot)
     cotangent = jnp.stack([cot_mine, swapped(cot_other, "zb")])
     filters = jnp.concatenate([halves(gate_taps)[0], halves(up_taps)[0]], axis=1)
@@ -268,64 +320,66 @@
     block = block.reshape(n_z * shard_rows, 2 * wide)
     weight = lax.all_gather(block, "y").reshape(n_y, n_z, shard_rows, 2 * wide)
     weight, both_grads, terms, taps = early_pass(
-        rows_scale, weight, early_rows, early_other, cotangent, filters
+        rows_scale, weight, early_rows, low, high, cotangent, filters
     )
     weight = weight.reshape(depth, 2 * wide)
     terms = terms.reshape(depth, 2 * wide)
     reduced = lax.psum_scatter(terms, "y", scatter_dimension=0, tiled=True)
     reduced = reduced.reshape(n_z, shard_rows, 2 * wide)
+    def taps_over(values, step):
+        return values + lax.ppermute(values, "y", [(k, k ^ step) for k in range(n_y)])
+
     partial = lax.dot_general(
         both_grads, weight, contract_last, preferred_element_type=jnp.float32
     ).astype(jnp.bfloat16)
     cut = depth // 2
     kept = pick(first_c, partial[:, :cut], partial[:, cut:])
     given = pick(first_c, partial[:, cut:], partial[:, :cut])
-    chip = kept.astype(jnp.float32) + swapped(given, "c").astype(jnp.float32)
+    taken, taps = lax.optimization_barrier((swapped(given, "c"), taps_over(taps, 1)))
+    chip = kept.astype(jnp.float32) + taken.astype(jnp.float32)
     chip = chip.astype(jnp.bfloat16)
     chip = chip.reshape(2, n_x, row_count // n_x, cut)
     chip = jnp.stack([pick(first_z, chip[0], chip[1]), pick(first_z, chip[1], chip[0])])
     spread = lax.all_to_all(
         chip.reshape(2 * n_x, row_count // n_x, cut), ("zb", "x"), 0, 0, tiled=True
     )
+    late_here, late_sent = late_pass(weight, late_rows, low, high, filters)
+    taps = taps_over(taps_over(taps, 2), 4)
+    spread, late_here, late_sent, taps = lax.optimization_barrier(
+        (spread, late_here, late_sent, taps)
+    )
     own = jnp.sum(spread.astype(jnp.float32), axis=0).astype(jnp.bfloat16)
     copies = jnp.broadcast_to(own[None], (n_x, *own.shape))
     finished = lax.all_to_all(copies, "x", 0, 0, tiled=True).reshape(row_count, cut)
-    for step in (1, 2, 4):
-        taps = taps + lax.ppermute(taps, "y", [(k, k ^ step) for k in range(n_y)])
-    high = lax.reduce_precision(taps, 8, 7)
-    taps = jnp.concatenate([high, taps - high]).astype(jnp.bfloat16)
-
-    late = late_pass(weight, late_rows, late_other, filters)
-    late_there = swapped(late[1], "zb")
-
-    start = jnp.broadcast_to(taps[None], (n_z, *taps.shape))
-    start = jnp.pad(start, [(0, 0), (shard_rows, 0), (0, 0)])
-    reduced, finished, late_there, start = lax.optimization_barrier(
-        (reduced, finished, late_there, start)
-    )
-    reduced = lax.dynamic_update_slice(start, reduced, (0, 0, 0))
+    taps = taps + swapped(taps, "zp")
+    taps_there = swapped(taps, "zb")
+
+    late_there = swapped(late_sent, "zb")
+
+    reduced, finished, late_there, taps_there = lax.optimization_barrier(
+        (reduced, finished, late_there, taps_there)
+    )
     pieces = lax.all_to_all(reduced, Z, 0, 0, tiled=True)
-    pieces = pieces.reshape(2, 2, -1, 2 * wide).astype(jnp.float32)
+    pieces = pieces.reshape(2, 2, shard_rows, 2 * wide).astype(jnp.float32)
     pieces = jnp.sum(pieces, axis=0)
-    tap_sums = pieces[:, shard_rows:].reshape(2, 2, -1, 2 * wide)
-    tap_sums = jnp.sum(tap_sums, axis=1)[:, :3]
-    pieces = pieces[:, :shard_rows]
+
+    def both(mine, other):
+        return joined(pick(first_z, mine, other), pick(first_z, other, mine))
+
     beside = swapped(finished, "c")
     early_grad = pick(
         first_c,
         jnp.concatenate([finished, beside], axis=1),
         jnp.concatenate([beside, finished], axis=1),
     )
-    late_hidden = joined(
-        pick(first_z, late[0], late_there), pick(first_z, late_there, late[0])
-    )
+    late_hidden = both(late_here, late_there)
     return (
         late_hidden,
         early_grad,
         gate_grad_sum + joined(pieces[0, :, :wide], pieces[1, :, :wide]),
         up_grad_sum + joined(pieces[0, :, wide:], pieces[1, :, wide:]),
-        gate_taps_sum + joined(tap_sums[0, :, :wide], tap_sums[1, :, :wide]),
-        up_taps_sum + joined(tap_sums[0, :, wide:], tap_sums[1, :, wide:]),
+        gate_taps_sum + both(taps[:3, :wide], taps_there[:3, :wide]),
+        up_taps_sum + both(taps[:3, wide:], taps_there[:3, wide:]),
     )
 
 

time: 169 us -> 169 us (level)
  starting transfers between devices: 40.4 us -> 47.1 us
  local copies, waits for them, and re-layouts: 9.43 us -> 4.05 us
    ppermute x6 -> x8, starting transfers between devices: 13.6 us -> 20.6 us  [swapped(): return lax.ppermute(values, axis, [(0, 1), (1, 0)])]
    ppermute x3, waiting for transfers between devices: 2.43 us -> 6.02 us  [taps_over(): lax.ppermute(values, 'y', [(k, k ^ step) for k in range(n_y)])]
    select_n x8 -> x11, other arithmetic: 1.86 us -> 4.41 us  [pick(): return jnp.where(flag, first, second)]
    all_to_all x1, waiting for transfers between devices: 5.51 us -> 3.36 us  [per_device(): pieces = lax.all_to_all(reduced, Z, 0, 0, tiled=True)]
    concatenate x4 -> x1, other arithmetic: 2.22 us -> 0.1 us  [per_device(): jnp.concatenate([pick(first_c, rows[:half], rows[half:]) for rows in (ear...]
    dynamic_update_slice x1 -> x0, local copies, waits for them, and re-layouts: 1.77 us -> none  [per_device(): reduced = lax.dynamic_update_slice(start, reduced, (0, 0, 0))]
    slice x8 -> x6, local copies, waits for them, and re-layouts: 1.76 us -> 0.02 us  [low_high(): array[..., wide:]]
    ppermute x6 -> x8, waiting for transfers between devices: 36.7 us -> 35.6 us  [swapped(): return lax.ppermute(values, axis, [(0, 1), (1, 0)])]
  transfers between devices with their start and end apart: 14 -> 16, of which waited for: 8 -> 8; matrix products, arithmetic and copies ran while one was open for 9% -> 8% of each run, Pallas kernels for 4% -> 3%
where the time goes in v7:
time: 169 us; the launch traced here: 168 us
  waiting for transfers between devices  53.3 us (32%)
  starting transfers between devices  47.1 us (28%)
  blocking collectives  19 us (11%)
  Pallas kernels  16 us (9%)
  between operations  14.5 us (9%)
  other arithmetic  10.6 us (6%)
  local copies, waits for them, and re-layouts  4.05 us (2%)
  matrix products  2.96 us (2%)
    ppermute x8, waiting for transfers between devices, swapped(): return lax.ppermute(values, axis, [(0, 1), (1, 0)])  35.6 us
    ppermute x8, starting transfers between devices, swapped(): return lax.ppermute(values, axis, [(0, 1), (1, 0)])  20.6 us
    all_to_all x1, blocking collectives, per_device(): block = lax.all_to_all(for_z, Z, 0, 0, tiled=True)  19 us
    ppermute x3, starting transfers between devices, taps_over(): lax.ppermute(values, 'y', [(k, k ^ step) for k in range(n_y)])  11.9 us
    pallas_call x1, Pallas kernels, early_pass(): pl.pallas_call(functools.partial(early_kernel, scale), out_shape=(jax.Sha...  8.69 us
    all_gather x1, waiting for transfers between devices, per_device(): weight = lax.all_gather(block, 'y').reshape(n_y, n_z, shard_rows, 2 * wide)  8.3 us
    ppermute x3, waiting for transfers between devices, taps_over(): lax.ppermute(values, 'y', [(k, k ^ step) for k in range(n_y)])  6.02 us
    all_to_all x1, starting transfers between devices, per_device(): lax.all_to_all(chip.reshape(2 * n_x, row_count // n_x, cut), ('zb', 'x'),...  5.88 us
  transfers between devices with their start and end apart: 16, of which 8 were waited for; matrix products, arithmetic and copies ran while one was open for 8% of the time, Pallas kernels for 3%

profile of v7, /device:TPU:6, one launch (start us, length us, event | category | flops | bytes accessed | tf_op | source)
XLA Modules:
  0.0 167.6 jit_solution(844103972404697741)
XLA Ops:
  9.0 19.0 %all_to_all.20 = bf16[4,64,768]{2,1,0:T(8,128)(2,1)} all-to-all(bf16[4,64,768]{2,1,0:T(8,128)(2,1)} %pack_halves.1), channel_id=1, replica_groups=mesh['rep'=2,'zp'=2,'zb'=2,'y'=8,'x'=4,'c'=2] {'zp','zb'}, dimensions={0} | all-to-all | bytes 786432 | tf_op jit(solution)/shard_map/all_to_all | solution.py:307
  29.6 2.3 %collective-permute-start = (bf16[256,2048]{1,0:T(8,128)(2,1)S(1)}, bf16[256,2048]{1,0:T(8,128)(2,1)S(1)}, u32[]{:S(2)}, u32[]{:S(2)}) collective-permute-start(bf16[256,2048]{1,0:T(8,128)(2,1)S(1)} %pad_maximum_fusion), channel_id=1, source_target_pairs={{0,64},{64,0},{1,65},{65,1},{2,66},{66,2},{3,67},{67,3},{4,68},{68... | collective-permute-start | bytes 3145736 | tf_op jit(solution)/shard_map/ppermute | solution.py:22
  31.9 23.6 %collective-permute-done = bf16[256,2048]{1,0:T(8,128)(2,1)S(1)} collective-permute-done((bf16[256,2048]{1,0:T(8,128)(2,1)S(1)}, bf16[256,2048]{1,0:T(8,128)(2,1)S(1)}, u32[]{:S(2)}, u32[]{:S(2)}) %collective-permute-start) | collective-permute-done | bytes 1048608 | tf_op jit(solution)/shard_map/ppermute | solution.py:22
  57.9 2.2 %collective-permute-start.2 = (bf16[256,384]{1,0:T(8,128)(2,1)S(1)}, bf16[256,384]{1,0:T(8,128)(2,1)S(1)}, u32[]{:S(2)}, u32[]{:S(2)}) collective-permute-start(bf16[256,384]{1,0:T(8,128)(2,1)S(1)} %get-tuple-element.59), channel_id=1, source_target_pairs={{0,64},{64,0},{1,65},{65,1},{2,66},{66,2},{3,67},{67,3},{4,68},{68... | collective-permute-start | bytes 589832 | tf_op jit(solution)/shard_map/ppermute | solution.py:22
  60.7 6.3 %collective-permute-done.2 = bf16[256,384]{1,0:T(8,128)(2,1)S(1)} collective-permute-done((bf16[256,384]{1,0:T(8,128)(2,1)S(1)}, bf16[256,384]{1,0:T(8,128)(2,1)S(1)}, u32[]{:S(2)}, u32[]{:S(2)}) %collective-permute-start.2) | collective-permute-done | bytes 196640 | tf_op jit(solution)/shard_map/ppermute | solution.py:22
  69.3 8.3 %all-gather.2.cloned.1.call-done = bf16[8,256,768]{2,1,0:T(8,128)(2,1)} async-done(((bf16[1,256,768]{2,1,0:T(8,128)(2,1)}), bf16[8,256,768]{2,1,0:T(8,128)(2,1)}) %all-gather.2.cloned.1.call-update) | async-done | bytes 3145744 | tf_op jit(solution)/shard_map/all_gather | solution.py:321
  77.6 8.7 %early_pass.1 = (bf16[4,8,64,768]{3,2,1,0:T(8,128)(2,1)}, bf16[512,768]{1,0:T(8,128)(2,1)}, bf16[8,4,64,768]{3,2,1,0:T(8,128)(2,1)}, f32[8,768]{1,0:T(8,128)}) custom-call(bf16[8,4,64,768]{3,2,1,0:T(8,128)(2,1)} %bitcast.39, bf16[256,2048]{1,0:T(8,128)(2,1)} %own_in.2, bf16[256,2048]{1,0:T(8,128)(2,1)} %get-tuple-element.51.low_in, ...), custom_call_target="tpu_custom_call" | custom-call | flops 3221225472 | bytes 11534336 | tf_op jit(solution)/shard_map/early_pass/pallas_call | solution.py:146
  88.2 3.0 %convolution_convert_fusion = bf16[512,2048]{1,0:T(8,128)(2,1)S(1)} fusion(bf16[512,768]{1,0:T(8,128)(2,1)} %get-tuple-element.22, bf16[2048,768]{1,0:T(8,128)(2,1)S(1)} %bitcast.28), kind=kOutput, calls=%fused_computation | convolution fusion | flops 1611661312 | bytes 6029312 | tf_op jit(solution)/shard_map/dot_general | solution.py:332
  91.3 1.9 %collective-permute-start.3 = (bf16[512,1024]{1,0:T(8,128)(2,1)S(1)}, bf16[512,1024]{1,0:T(8,128)(2,1)S(1)}, u32[]{:S(2)}, u32[]{:S(2)}) collective-permute-start(bf16[512,1024]{1,0:T(8,128)(2,1)S(1)} %broadcast_select_fusion.2), channel_id=1, source_target_pairs={{0,1},{1,0},{2,3},{3,2},{4,5},{5,4},{6,7},{7,6},{8,9},{9,8},{10,11... | collective-permute-start | bytes 3145736 | tf_op jit(solution)/shard_map/ppermute | solution.py:22
  93.2 2.9 %collective-permute-start.4 = (f32[8,768]{1,0:T(8,128)S(1)}, f32[8,768]{1,0:T(8,128)S(1)}, u32[]{:S(2)}, u32[]{:S(2)}) collective-permute-start(f32[8,768]{1,0:T(8,128)S(1)} %copy-done.5), channel_id=1, source_target_pairs={{0,8},{8,0},{16,24},{24,16},{32,40},{40,32},{48,56},{56,48},{1,9},... | collective-permute-start | bytes 73736 | tf_op jit(solution)/shard_map/ppermute | solution.py:330
  96.1 2.8 %collective-permute-done.4 = f32[8,768]{1,0:T(8,128)S(1)} collective-permute-done((f32[8,768]{1,0:T(8,128)S(1)}, f32[8,768]{1,0:T(8,128)S(1)}, u32[]{:S(2)}, u32[]{:S(2)}) %collective-permute-start.4) | collective-permute-done | bytes 24608 | tf_op jit(solution)/shard_map/ppermute | solution.py:330
  100.8 5.9 %all-to-all-start.1 = ((bf16[8,64,1024]{2,1,0:T(8,128)(2,1)}), bf16[8,64,1024]{2,1,0:T(8,128)(2,1)S(1)}, u32[]{:S(2)}, u32[]{:S(2)}) async-start(bf16[8,64,1024]{2,1,0:T(8,128)(2,1)} %bitcast.7), calls=%async_computation.1 | async-start | bytes 2097152 | tf_op jit(solution)/shard_map/all_to_all | solution.py:343
  106.6 3.8 %collective-permute-start.5 = (f32[8,768]{1,0:T(8,128)S(1)}, f32[8,768]{1,0:T(8,128)S(1)}, u32[]{:S(2)}, u32[]{:S(2)}) collective-permute-start(f32[8,768]{1,0:T(8,128)S(1)} %add.37), channel_id=1, source_target_pairs={{0,16},{8,24},{16,0},{24,8},{32,48},{40,56},{48,32},{56,40},{1,17}... | collective-permute-start | bytes 73736 | tf_op jit(solution)/shard_map/ppermute | solution.py:330
  110.5 3.2 %collective-permute-done.5 = f32[8,768]{1,0:T(8,128)S(1)} collective-permute-done((f32[8,768]{1,0:T(8,128)S(1)}, f32[8,768]{1,0:T(8,128)S(1)}, u32[]{:S(2)}, u32[]{:S(2)}) %collective-permute-start.5) | collective-permute-done | bytes 24608 | tf_op jit(solution)/shard_map/ppermute | solution.py:330
  113.7 5.2 %collective-permute-start.6 = (f32[8,768]{1,0:T(8,128)S(1)}, f32[8,768]{1,0:T(8,128)S(1)}, u32[]{:S(2)}, u32[]{:S(2)}) collective-permute-start(f32[8,768]{1,0:T(8,128)S(1)} %add.39), channel_id=1, source_target_pairs={{0,32},{8,40},{16,48},{24,56},{32,0},{40,8},{48,16},{56,24},{1,33}... | collective-permute-start | bytes 73736 | tf_op jit(solution)/shard_map/ppermute | solution.py:330
  118.9 5.5 %late_pass.1 = (bf16[256,384]{1,0:T(8,128)(2,1)}, bf16[256,384]{1,0:T(8,128)(2,1)}) custom-call(bf16[2048,768]{1,0:T(8,128)(2,1)} %bitcast.27, bf16[256,2048]{1,0:T(8,128)(2,1)} %own_in.3, bf16[256,2048]{1,0:T(8,128)(2,1)} %get-tuple-element.51.low_in, bf16[256,2048]{1,0:T(8,128)(2,1)} %get-tuple-element.50.high_in, f32[8,768]{1,0:T(8,128)} %fusion.3.filters_in), custom_call_target="tpu_custom_call" | custom-call | flops 1610612736 | bytes 5242880 | tf_op jit(solution)/shard_map/late_pass/pallas_call | solution.py:226
  125.6 4.8 %all-to-all-start.2 = ((bf16[4,64,1024]{2,1,0:T(8,128)(2,1)}), bf16[4,64,1024]{2,1,0:T(8,128)(2,1)S(1)}, u32[]{:S(2)}, u32[]{:S(2)}) async-start(bf16[4,64,1024]{2,1,0:T(8,128)(2,1)} %broadcast_in_dim.2), calls=%async_computation.3 | async-start | bytes 1048576 | tf_op jit(solution)/shard_map/all_to_all | solution.py:353
  130.4 3.5 %collective-permute-start.7 = (bf16[256,384]{1,0:T(8,128)(2,1)S(1)}, bf16[256,384]{1,0:T(8,128)(2,1)S(1)}, u32[]{:S(2)}, u32[]{:S(2)}) collective-permute-start(bf16[256,384]{1,0:T(8,128)(2,1)S(1)} %copy-done.10), channel_id=1, source_target_pairs={{0,64},{64,0},{1,65},{65,1},{2,66},{66,2},{3,67},{67,3},{4,68},{68... | collective-permute-start | bytes 589832 | tf_op jit(solution)/shard_map/ppermute | solution.py:22
  133.8 4.6 %collective-permute-start.8 = (f32[8,768]{1,0:T(8,128)S(1)}, f32[8,768]{1,0:T(8,128)S(1)}, u32[]{:S(2)}, u32[]{:S(2)}) collective-permute-start(f32[8,768]{1,0:T(8,128)S(1)} %add.40), channel_id=1, source_target_pairs={{0,128},{128,0},{1,129},{129,1},{2,130},{130,2},{3,131},{131,3},{4... | collective-permute-start | bytes 73736 | tf_op jit(solution)/shard_map/ppermute | solution.py:22
  138.5 2.3 %collective-permute-done.8 = f32[8,768]{1,0:T(8,128)S(1)} collective-permute-done((f32[8,768]{1,0:T(8,128)S(1)}, f32[8,768]{1,0:T(8,128)S(1)}, u32[]{:S(2)}, u32[]{:S(2)}) %collective-permute-start.8) | collective-permute-done | bytes 24608 | tf_op jit(solution)/shard_map/ppermute | solution.py:22
  140.7 2.3 %collective-permute-start.9 = (f32[8,768]{1,0:T(8,128)S(1)}, f32[8,768]{1,0:T(8,128)S(1)}, u32[]{:S(2)}, u32[]{:S(2)}) collective-permute-start(f32[8,768]{1,0:T(8,128)S(1)} %add.41), channel_id=1, source_target_pairs={{0,64},{64,0},{1,65},{65,1},{2,66},{66,2},{3,67},{67,3},{4,68},{68... | collective-permute-start | bytes 73736 | tf_op jit(solution)/shard_map/ppermute | solution.py:22
  143.0 3.4 %collective-permute-done.9 = f32[8,768]{1,0:T(8,128)S(1)} collective-permute-done((f32[8,768]{1,0:T(8,128)S(1)}, f32[8,768]{1,0:T(8,128)S(1)}, u32[]{:S(2)}, u32[]{:S(2)}) %collective-permute-start.9) | collective-permute-done | bytes 24608 | tf_op jit(solution)/shard_map/ppermute | solution.py:22
  146.5 3.8 %all-to-all-start.3 = ((bf16[4,64,768]{2,1,0:T(8,128)(2,1)}), bf16[4,64,768]{2,1,0:T(8,128)(2,1)S(1)}, u32[]{:S(2)}, u32[]{:S(2)}) async-start(bf16[4,64,768]{2,1,0:T(8,128)(2,1)} %bitcast.37), calls=%async_computation.4 | async-start | bytes 786432 | tf_op jit(solution)/shard_map/all_to_all | solution.py:362
  155.9 3.4 %all-to-all-done.3 = bf16[4,64,768]{2,1,0:T(8,128)(2,1)S(1)} async-done(((bf16[4,64,768]{2,1,0:T(8,128)(2,1)}), bf16[4,64,768]{2,1,0:T(8,128)(2,1)S(1)}, u32[]{:S(2)}, u32[]{:S(2)}) %all-to-all-start.3) | async-done | bytes 393248 | tf_op jit(solution)/shard_map/all_to_all | solution.py:362
  (78 shorter events, 20.4 us)
Async XLA Ops:
  7.2 70.4 %all-gather.2.cloned.1.call-start = ((), (), s32[]{:S(2)}) async-start(), calls=%async_computation.5 | async-start | bytes 3538944 | tf_op jit(solution)/shard_map/all_gather | solution.py:321
  28.1 118.4 %reduce-scatter.2.cloned.1.call-start = ((), (), s32[]{:S(2)}) async-start(), calls=%async_computation.6 | async-start | bytes 3538944 | tf_op jit(solution)/shard_map/reduce_scatter | solution.py:327
  29.5 27.9 %slice-start = ((bf16[256,704]{0,1:T(8,128)(2,1)}), bf16[256,320]{0,1:T(8,128)(2,1)S(1)}, s32[]{:S(2)}) async-start(bf16[256,704]{0,1:T(8,128)(2,1)} %param.13), calls=%async_computation.7 | async-start | bytes 327680 | tf_op jit(solution)/shard_map/slice | solution.py:297
  29.5 28.1 %slice-start.1 = ((bf16[256,704]{0,1:T(8,128)(2,1)}), bf16[256,384]{0,1:T(8,128)(2,1)S(1)}, s32[]{:S(2)}) async-start(bf16[256,704]{0,1:T(8,128)(2,1)} %param.13), calls=%async_computation.8 | async-start | bytes 393216 | tf_op jit(solution)/shard_map/slice | solution.py:297
  29.5 30.6 %copy-start.6 = (bf16[3,704]{1,0:T(4,128)(2,1)S(1)}, bf16[3,704]{1,0:T(4,128)(2,1)}, u32[]{:S(2)}) copy-start(bf16[3,704]{1,0:T(4,128)(2,1)} %param.16) | copy-start | bytes 12676
  29.5 30.6 %slice-start.2 = ((bf16[3,704]{1,0:T(4,128)(2,1)}), bf16[3,320]{1,0:T(4,128)(2,1)S(1)}, s32[]{:S(2)}) async-start(bf16[3,704]{1,0:T(4,128)(2,1)} %param.16), calls=%async_computation.9 | async-start | bytes 6144 | tf_op jit(solution)/shard_map/slice | solution.py:297
  29.5 30.6 %copy-start.7 = (bf16[3,704]{1,0:T(4,128)(2,1)S(1)}, bf16[3,704]{1,0:T(4,128)(2,1)}, u32[]{:S(2)}) copy-start(bf16[3,704]{1,0:T(4,128)(2,1)} %param.17) | copy-start | bytes 12676
  29.5 30.6 %slice-start.3 = ((bf16[3,704]{1,0:T(4,128)(2,1)}), bf16[3,320]{1,0:T(4,128)(2,1)S(1)}, s32[]{:S(2)}) async-start(bf16[3,704]{1,0:T(4,128)(2,1)} %param.17), calls=%async_computation.10 | async-start | bytes 6144 | tf_op jit(solution)/shard_map/slice | solution.py:297
  29.6 25.8 %collective-permute-start = (bf16[256,2048]{1,0:T(8,128)(2,1)S(1)}, bf16[256,2048]{1,0:T(8,128)(2,1)S(1)}, u32[]{:S(2)}, u32[]{:S(2)}) collective-permute-start(bf16[256,2048]{1,0:T(8,128)(2,1)S(1)} %pad_maximum_fusion), channel_id=1, source_target_pairs={{0,64},{64,0},{1,65},{65,1},{2,66},{66,2},{3,67},{67,3},{4,68},{68... | collective-permute-start | bytes 3145736 | tf_op jit(solution)/shard_map/ppermute | solution.py:22
  55.5 12.4 %collective-permute-start.1 = (bf16[256,2048]{1,0:T(8,128)(2,1)S(1)}, bf16[256,2048]{1,0:T(8,128)(2,1)S(1)}, u32[]{:S(2)}, u32[]{:S(2)}) collective-permute-start(bf16[256,2048]{1,0:T(8,128)(2,1)S(1)} %collective-permute-done), channel_id=1, source_target_pairs={{0,1},{1,0},{2,3},{3,2},{4,5},{5,4},{6,7},{7,6},{8,9},{9,8},{10,11... | collective-permute-start | bytes 3145736 | tf_op jit(solution)/shard_map/ppermute | solution.py:22
  57.9 9.2 %collective-permute-start.2 = (bf16[256,384]{1,0:T(8,128)(2,1)S(1)}, bf16[256,384]{1,0:T(8,128)(2,1)S(1)}, u32[]{:S(2)}, u32[]{:S(2)}) collective-permute-start(bf16[256,384]{1,0:T(8,128)(2,1)S(1)} %get-tuple-element.59), channel_id=1, source_target_pairs={{0,64},{64,0},{1,65},{65,1},{2,66},{66,2},{3,67},{67,3},{4,68},{68... | collective-permute-start | bytes 589832 | tf_op jit(solution)/shard_map/ppermute | solution.py:22
  91.3 7.7 %collective-permute-start.3 = (bf16[512,1024]{1,0:T(8,128)(2,1)S(1)}, bf16[512,1024]{1,0:T(8,128)(2,1)S(1)}, u32[]{:S(2)}, u32[]{:S(2)}) collective-permute-start(bf16[512,1024]{1,0:T(8,128)(2,1)S(1)} %broadcast_select_fusion.2), channel_id=1, source_target_pairs={{0,1},{1,0},{2,3},{3,2},{4,5},{5,4},{6,7},{7,6},{8,9},{9,8},{10,11... | collective-permute-start | bytes 3145736 | tf_op jit(solution)/shard_map/ppermute | solution.py:22
  93.2 5.7 %collective-permute-start.4 = (f32[8,768]{1,0:T(8,128)S(1)}, f32[8,768]{1,0:T(8,128)S(1)}, u32[]{:S(2)}, u32[]{:S(2)}) collective-permute-start(f32[8,768]{1,0:T(8,128)S(1)} %copy-done.5), channel_id=1, source_target_pairs={{0,8},{8,0},{16,24},{24,16},{32,40},{40,32},{48,56},{56,48},{1,9},... | collective-permute-start | bytes 73736 | tf_op jit(solution)/shard_map/ppermute | solution.py:330
  100.8 23.7 %all-to-all-start.1 = ((bf16[8,64,1024]{2,1,0:T(8,128)(2,1)}), bf16[8,64,1024]{2,1,0:T(8,128)(2,1)S(1)}, u32[]{:S(2)}, u32[]{:S(2)}) async-start(bf16[8,64,1024]{2,1,0:T(8,128)(2,1)} %bitcast.7), calls=%async_computation.1 | async-start | bytes 2097152 | tf_op jit(solution)/shard_map/all_to_all | solution.py:343
  106.6 7.0 %collective-permute-start.5 = (f32[8,768]{1,0:T(8,128)S(1)}, f32[8,768]{1,0:T(8,128)S(1)}, u32[]{:S(2)}, u32[]{:S(2)}) collective-permute-start(f32[8,768]{1,0:T(8,128)S(1)} %add.37), channel_id=1, source_target_pairs={{0,16},{8,24},{16,0},{24,8},{32,48},{40,56},{48,32},{56,40},{1,17}... | collective-permute-start | bytes 73736 | tf_op jit(solution)/shard_map/ppermute | solution.py:330
  113.7 10.8 %collective-permute-start.6 = (f32[8,768]{1,0:T(8,128)S(1)}, f32[8,768]{1,0:T(8,128)S(1)}, u32[]{:S(2)}, u32[]{:S(2)}) collective-permute-start(f32[8,768]{1,0:T(8,128)S(1)} %add.39), channel_id=1, source_target_pairs={{0,32},{8,40},{16,48},{24,56},{32,0},{40,8},{48,16},{56,24},{1,33}... | collective-permute-start | bytes 73736 | tf_op jit(solution)/shard_map/ppermute | solution.py:330
  124.7 27.6 %copy-start.8 = (f32[3,704]{1,0:T(4,128)S(1)}, f32[3,704]{1,0:T(4,128)}, u32[]{:S(2)}) copy-start(f32[3,704]{1,0:T(4,128)} %param.21) | copy-start | bytes 25348
  125.6 20.9 %all-to-all-start.2 = ((bf16[4,64,1024]{2,1,0:T(8,128)(2,1)}), bf16[4,64,1024]{2,1,0:T(8,128)(2,1)S(1)}, u32[]{:S(2)}, u32[]{:S(2)}) async-start(bf16[4,64,1024]{2,1,0:T(8,128)(2,1)} %broadcast_in_dim.2), calls=%async_computation.3 | async-start | bytes 1048576 | tf_op jit(solution)/shard_map/all_to_all | solution.py:353
  130.4 23.5 %copy-start.9 = (f32[3,704]{1,0:T(4,128)S(1)}, f32[3,704]{1,0:T(4,128)}, u32[]{:S(2)}) copy-start(f32[3,704]{1,0:T(4,128)} %param.20) | copy-start | bytes 25348
  130.4 16.1 %collective-permute-start.7 = (bf16[256,384]{1,0:T(8,128)(2,1)S(1)}, bf16[256,384]{1,0:T(8,128)(2,1)S(1)}, u32[]{:S(2)}, u32[]{:S(2)}) collective-permute-start(bf16[256,384]{1,0:T(8,128)(2,1)S(1)} %copy-done.10), channel_id=1, source_target_pairs={{0,64},{64,0},{1,65},{65,1},{2,66},{66,2},{3,67},{67,3},{4,68},{68... | collective-permute-start | bytes 589832 | tf_op jit(solution)/shard_map/ppermute | solution.py:22
  133.8 6.9 %collective-permute-start.8 = (f32[8,768]{1,0:T(8,128)S(1)}, f32[8,768]{1,0:T(8,128)S(1)}, u32[]{:S(2)}, u32[]{:S(2)}) collective-permute-start(f32[8,768]{1,0:T(8,128)S(1)} %add.40), channel_id=1, source_target_pairs={{0,128},{128,0},{1,129},{129,1},{2,130},{130,2},{3,131},{131,3},{4... | collective-permute-start | bytes 73736 | tf_op jit(solution)/shard_map/ppermute | solution.py:22
  140.7 5.7 %collective-permute-start.9 = (f32[8,768]{1,0:T(8,128)S(1)}, f32[8,768]{1,0:T(8,128)S(1)}, u32[]{:S(2)}, u32[]{:S(2)}) collective-permute-start(f32[8,768]{1,0:T(8,128)S(1)} %add.41), channel_id=1, source_target_pairs={{0,64},{64,0},{1,65},{65,1},{2,66},{66,2},{3,67},{67,3},{4,68},{68... | collective-permute-start | bytes 73736 | tf_op jit(solution)/shard_map/ppermute | solution.py:22
  146.5 12.7 %all-to-all-start.3 = ((bf16[4,64,768]{2,1,0:T(8,128)(2,1)}), bf16[4,64,768]{2,1,0:T(8,128)(2,1)S(1)}, u32[]{:S(2)}, u32[]{:S(2)}) async-start(bf16[4,64,768]{2,1,0:T(8,128)(2,1)} %bitcast.37), calls=%async_computation.4 | async-start | bytes 786432 | tf_op jit(solution)/shard_map/all_to_all | solution.py:362
  150.4 4.1 %collective-permute-start.10 = (bf16[256,1024]{1,0:T(8,128)(2,1)S(1)}, bf16[256,1024]{1,0:T(8,128)(2,1)S(1)}, u32[]{:S(2)}, u32[]{:S(2)}) collective-permute-start(bf16[256,1024]{1,0:T(8,128)(2,1)S(1)} %bitcast.29), channel_id=1, source_target_pairs={{0,1},{1,0},{2,3},{3,2},{4,5},{5,4},{6,7},{7,6},{8,9},{9,8},{10,11... | collective-permute-start | bytes 1572872 | tf_op jit(solution)/shard_map/ppermute | solution.py:22
  (7 other events, 64.8 us)
Sparse Core Ops, SparseCore 0:
  28.2 49.3 all-gather.1
  86.5 49.0 reduce-scatter.1

commit v8 on v7

--- a/solution.py
+++ b/solution.py
@@ -13,6 +13,7 @@
 FS = ("zp", "zb", "y")
 REP_FS = ("rep", "zp", "zb", "y")
 TP = ("x", "c")
+EXTRA = 8
 
 contract_last = (((1,), (1,)), ((), ()))
 contract_first = (((0,), (0,)), ((), ()))
@@ -45,7 +46,6 @@
     weight_out,
     grads_out,
     terms_out,
-    sums_out,
     weight,
     grads,
     terms,
@@ -53,7 +53,6 @@
     other,
     cotangent,
     filters,
-    tap_sums,
     in_sems,
     out_sems,
 ):
@@ -111,12 +110,11 @@
         grads[part * length : (part + 1) * length, :] = full.astype(jnp.bfloat16)
     stores.append(pltpu.make_async_copy(grads, grads_out, out_sems.at[1]))
     stores[1].start()
-    tap_sums[...] = jnp.concatenate(
-        [scale * value for value in sums]
-        + [jnp.zeros((tap_sums.shape[0] - 3, columns), jnp.float32)]
-    )
-    stores.append(pltpu.make_async_copy(tap_sums, sums_out, out_sems.at[2]))
-    stores[2].start()
+    taps = [scale * value for value in sums]
+    high = [value.astype(jnp.bfloat16).astype(jnp.float32) for value in taps]
+    blank = jnp.zeros((terms.shape[2] - shard_rows - 6, columns), jnp.float32)
+    extra = high + [value - top for value, top in zip(taps, high)] + [blank]
+    extra = jnp.concatenate(extra).astype(jnp.bfloat16)
     for z in range(n_z):
         term = sum(
             lax.dot_general(
@@ -128,9 +126,11 @@
             for part, rows in enumerate((own, other))
         )
         term = (term * scale).astype(jnp.bfloat16)
-        terms[z] = term.reshape(n_y, shard_rows, columns)
+        for y in range(n_y):
+            terms[z, y, :shard_rows] = term[y * shard_rows : (y + 1) * shard_rows]
+            terms[z, y, shard_rows:] = extra
         store = pltpu.make_async_copy(
-            terms.at[z], terms_out.at[:, z], out_sems.at[3 + z]
+            terms.at[z], terms_out.at[:, z], out_sems.at[2 + z]
         )
         store.start()
         stores.append(store)
@@ -148,22 +148,20 @@
         out_shape=(
             jax.ShapeDtypeStruct(ordered, jnp.bfloat16),
             jax.ShapeDtypeStruct((2 * length, columns), jnp.bfloat16),
-            jax.ShapeDtypeStruct(gathered.shape, jnp.bfloat16),
-            jax.ShapeDtypeStruct((8, columns), jnp.float32),
+            jax.ShapeDtypeStruct((n_y, n_z, shard_rows + EXTRA, columns), jnp.bfloat16),
         ),
         in_specs=[apart] * 6,
-        out_specs=(apart,) * 4,
+        out_specs=(apart,) * 3,
         scratch_shapes=[
             pltpu.VMEM(ordered, jnp.bfloat16),
             pltpu.VMEM((2 * length, columns), jnp.bfloat16),
-            pltpu.VMEM(ordered, jnp.bfloat16),
+            pltpu.VMEM((n_z, n_y, shard_rows + EXTRA, columns), jnp.bfloat16),
             pltpu.VMEM(own.shape, jnp.bfloat16),
             pltpu.VMEM(own.shape, jnp.bfloat16),
             pltpu.VMEM(cotangent.shape, jnp.bfloat16),
             pltpu.VMEM((8, columns), jnp.float32),
-            pltpu.VMEM((8, columns), jnp.float32),
             pltpu.SemaphoreType.DMA((n_y + 5,)),
-            pltpu.SemaphoreType.DMA((3 + n_z,)),
+            pltpu.SemaphoreType.DMA((2 + n_z,)),
         ],
         compiler_params=pltpu.CompilerParams(vmem_limit_bytes=57 * 1024 * 1024),
         cost_estimate=pl.CostEstimate(
@@ -319,24 +317,20 @@
 
     block = block.reshape(n_z * shard_rows, 2 * wide)
     weight = lax.all_gather(block, "y").reshape(n_y, n_z, shard_rows, 2 * wide)
-    weight, both_grads, terms, taps = early_pass(
+    weight, both_grads, terms = early_pass(
         rows_scale, weight, early_rows, low, high, cotangent, filters
     )
     weight = weight.reshape(depth, 2 * wide)
-    terms = terms.reshape(depth, 2 * wide)
+    terms = terms.reshape(-1, 2 * wide)
     reduced = lax.psum_scatter(terms, "y", scatter_dimension=0, tiled=True)
-    reduced = reduced.reshape(n_z, shard_rows, 2 * wide)
-    def taps_over(values, step):
-        return values + lax.ppermute(values, "y", [(k, k ^ step) for k in range(n_y)])
-
+    reduced = reduced.reshape(n_z, shard_rows + EXTRA, 2 * wide)
     partial = lax.dot_general(
         both_grads, weight, contract_last, preferred_element_type=jnp.float32
     ).astype(jnp.bfloat16)
     cut = depth // 2
     kept = pick(first_c, partial[:, :cut], partial[:, cut:])
     given = pick(first_c, partial[:, cut:], partial[:, :cut])
-    taken, taps = lax.optimization_barrier((swapped(given, "c"), taps_over(taps, 1)))
-    chip = kept.astype(jnp.float32) + taken.astype(jnp.float32)
+    chip = kept.astype(jnp.float32) + swapped(given, "c").astype(jnp.float32)
     chip = chip.astype(jnp.bfloat16)
     chip = chip.reshape(2, n_x, row_count // n_x, cut)
     chip = jnp.stack([pick(first_z, chip[0], chip[1]), pick(first_z, chip[1], chip[0])])
@@ -344,24 +338,22 @@
         chip.reshape(2 * n_x, row_count // n_x, cut), ("zb", "x"), 0, 0, tiled=True
     )
     late_here, late_sent = late_pass(weight, late_rows, low, high, filters)
-    taps = taps_over(taps_over(taps, 2), 4)
-    spread, late_here, late_sent, taps = lax.optimization_barrier(
-        (spread, late_here, late_sent, taps)
+    spread, late_here, late_sent = lax.optimization_barrier(
+        (spread, late_here, late_sent)
     )
     own = jnp.sum(spread.astype(jnp.float32), axis=0).astype(jnp.bfloat16)
     copies = jnp.broadcast_to(own[None], (n_x, *own.shape))
     finished = lax.all_to_all(copies, "x", 0, 0, tiled=True).reshape(row_count, cut)
-    taps = taps + swapped(taps, "zp")
-    taps_there = swapped(taps, "zb")
-
     late_there = swapped(late_sent, "zb")
 
-    reduced, finished, late_there, taps_there = lax.optimization_barrier(
-        (reduced, finished, late_there, taps_there)
+    reduced, finished, late_there = lax.optimization_barrier(
+        (reduced, finished, late_there)
     )
     pieces = lax.all_to_all(reduced, Z, 0, 0, tiled=True)
-    pieces = pieces.reshape(2, 2, shard_rows, 2 * wide).astype(jnp.float32)
+    pieces = pieces.reshape(2, 2, shard_rows + EXTRA, 2 * wide).astype(jnp.float32)
     pieces = jnp.sum(pieces, axis=0)
+    taps = pieces[:, shard_rows : shard_rows + 3] + pieces[:, shard_rows + 3 : shard_rows + 6]
+    pieces = pieces[:, :shard_rows]
 
     def both(mine, other):
         return joined(pick(first_z, mine, other), pick(first_z, other, mine))
@@ -378,8 +370,8 @@
         early_grad,
         gate_grad_sum + joined(pieces[0, :, :wide], pieces[1, :, :wide]),
         up_grad_sum + joined(pieces[0, :, wide:], pieces[1, :, wide:]),
-        gate_taps_sum + both(taps[:3, :wide], taps_there[:3, :wide]),
-        up_taps_sum + both(taps[:3, wide:], taps_there[:3, wide:]),
+        gate_taps_sum + joined(taps[0, :, :wide], taps[1, :, :wide]),
+        up_taps_sum + joined(taps[0, :, wide:], taps[1, :, wide:]),
     )
 
 

time: 169 us -> 165 us (0.976)
  starting transfers between devices: 47.1 us -> 29.8 us
  waiting for transfers between devices: 53.3 us -> 67.5 us
    ppermute x3 -> x0, starting transfers between devices: 11.9 us -> none  [taps_over(): lax.ppermute(values, 'y', [(k, k ^ step) for k in range(n_y)])]
    all_to_all x1, waiting for transfers between devices: 0.01 us -> 7.84 us  [per_device(): lax.all_to_all(chip.reshape(2 * n_x, row_count // n_x, cut), ('zb', 'x'),...]
    ppermute x8 -> x6, starting transfers between devices: 20.6 us -> 13.6 us  [swapped(): return lax.ppermute(values, axis, [(0, 1), (1, 0)])]
    ppermute x3 -> x0, waiting for transfers between devices: 6.02 us -> none  [taps_over(): lax.ppermute(values, 'y', [(k, k ^ step) for k in range(n_y)])]
    reduce_scatter x1, waiting for transfers between devices: 0.01 us -> 5.54 us  [per_device(): reduced = lax.psum_scatter(terms, 'y', scatter_dimension=0, tiled=True)]
    all_to_all x1, waiting for transfers between devices: 3.36 us -> 7.51 us  [per_device(): pieces = lax.all_to_all(reduced, Z, 0, 0, tiled=True)]
    ppermute x8 -> x6, waiting for transfers between devices: 35.6 us -> 38.2 us  [swapped(): return lax.ppermute(values, axis, [(0, 1), (1, 0)])]
    select_n x11 -> x8, other arithmetic: 4.41 us -> 4.38 us  [pick(): return jnp.where(flag, first, second)]
  transfers between devices with their start and end apart: 16 -> 11, of which waited for: 8 -> 9; matrix products, arithmetic and copies ran while one was open for 8% -> 8% of each run, Pallas kernels for 3% -> 3%
where the time goes in v8:
time: 165 us; the launch traced here: 164 us
  waiting for transfers between devices  67.5 us (41%)
  starting transfers between devices  29.8 us (18%)
  blocking collectives  19 us (12%)
  Pallas kernels  16.1 us (10%)
  between operations  14.4 us (9%)
  other arithmetic  10.6 us (6%)
  local copies, waits for them, and re-layouts  4.05 us (2%)
  matrix products  2.96 us (2%)
    ppermute x6, waiting for transfers between devices, swapped(): return lax.ppermute(values, axis, [(0, 1), (1, 0)])  38.2 us
    all_to_all x1, blocking collectives, per_device(): block = lax.all_to_all(for_z, Z, 0, 0, tiled=True)  19 us
    ppermute x6, starting transfers between devices, swapped(): return lax.ppermute(values, axis, [(0, 1), (1, 0)])  13.6 us
    pallas_call x1, Pallas kernels, early_pass(): pl.pallas_call(functools.partial(early_kernel, scale), out_shape=(jax.Sha...  8.83 us
    all_gather x1, waiting for transfers between devices, per_device(): weight = lax.all_gather(block, 'y').reshape(n_y, n_z, shard_rows, 2 * wide)  8.31 us
    all_to_all x1, waiting for transfers between devices, per_device(): lax.all_to_all(chip.reshape(2 * n_x, row_count // n_x, cut), ('zb', 'x'),...  7.84 us
    all_to_all x1, waiting for transfers between devices, per_device(): pieces = lax.all_to_all(reduced, Z, 0, 0, tiled=True)  7.51 us
    all_to_all x1, starting transfers between devices, per_device(): lax.all_to_all(chip.reshape(2 * n_x, row_count // n_x, cut), ('zb', 'x'),...  5.88 us
  transfers between devices with their start and end apart: 11, of which 9 were waited for; matrix products, arithmetic and copies ran while one was open for 8% of the time, Pallas kernels for 3%

profile of v8, /device:TPU:6, one launch (start us, length us, event | category | flops | bytes accessed | tf_op | source)
XLA Modules:
  0.0 164.4 jit_solution(1982876366124999047)
XLA Ops:
  7.2 1.8 %pack_halves.1 = bf16[4,64,768]{2,1,0:T(8,128)(2,1)} custom-call(bf16[64,704]{1,0:T(8,128)(2,1)} %gate.1, bf16[64,704]{1,0:T(8,128)(2,1)} %up.1), custom_call_target="tpu_custom_call" | custom-call | tf_op jit(solution)/shard_map/pack_halves/pallas_call | solution.py:259
  9.0 19.0 %all_to_all.20 = bf16[4,64,768]{2,1,0:T(8,128)(2,1)} all-to-all(bf16[4,64,768]{2,1,0:T(8,128)(2,1)} %pack_halves.1), channel_id=1, replica_groups=mesh['rep'=2,'zp'=2,'zb'=2,'y'=8,'x'=4,'c'=2] {'zp','zb'}, dimensions={0} | all-to-all | bytes 786432 | tf_op jit(solution)/shard_map/all_to_all | solution.py:305
  29.6 2.3 %collective-permute-start = (bf16[256,2048]{1,0:T(8,128)(2,1)S(1)}, bf16[256,2048]{1,0:T(8,128)(2,1)S(1)}, u32[]{:S(2)}, u32[]{:S(2)}) collective-permute-start(bf16[256,2048]{1,0:T(8,128)(2,1)S(1)} %pad_maximum_fusion), channel_id=1, source_target_pairs={{0,64},{64,0},{1,65},{65,1},{2,66},{66,2},{3,67},{67,3},{4,68},{68... | collective-permute-start | bytes 3145736 | tf_op jit(solution)/shard_map/ppermute | solution.py:23
  31.9 23.6 %collective-permute-done = bf16[256,2048]{1,0:T(8,128)(2,1)S(1)} collective-permute-done((bf16[256,2048]{1,0:T(8,128)(2,1)S(1)}, bf16[256,2048]{1,0:T(8,128)(2,1)S(1)}, u32[]{:S(2)}, u32[]{:S(2)}) %collective-permute-start) | collective-permute-done | bytes 1048608 | tf_op jit(solution)/shard_map/ppermute | solution.py:23
  55.5 1.9 %collective-permute-start.1 = (bf16[256,2048]{1,0:T(8,128)(2,1)S(1)}, bf16[256,2048]{1,0:T(8,128)(2,1)S(1)}, u32[]{:S(2)}, u32[]{:S(2)}) collective-permute-start(bf16[256,2048]{1,0:T(8,128)(2,1)S(1)} %collective-permute-done), channel_id=1, source_target_pairs={{0,1},{1,0},{2,3},{3,2},{4,5},{5,4},{6,7},{7,6},{8,9},{9,8},{10,11... | collective-permute-start | bytes 3145736 | tf_op jit(solution)/shard_map/ppermute | solution.py:23
  57.9 2.2 %collective-permute-start.2 = (bf16[256,384]{1,0:T(8,128)(2,1)S(1)}, bf16[256,384]{1,0:T(8,128)(2,1)S(1)}, u32[]{:S(2)}, u32[]{:S(2)}) collective-permute-start(bf16[256,384]{1,0:T(8,128)(2,1)S(1)} %get-tuple-element.49), channel_id=1, source_target_pairs={{0,64},{64,0},{1,65},{65,1},{2,66},{66,2},{3,67},{67,3},{4,68},{68... | collective-permute-start | bytes 589832 | tf_op jit(solution)/shard_map/ppermute | solution.py:23
  60.7 6.3 %collective-permute-done.2 = bf16[256,384]{1,0:T(8,128)(2,1)S(1)} collective-permute-done((bf16[256,384]{1,0:T(8,128)(2,1)S(1)}, bf16[256,384]{1,0:T(8,128)(2,1)S(1)}, u32[]{:S(2)}, u32[]{:S(2)}) %collective-permute-start.2) | collective-permute-done | bytes 196640 | tf_op jit(solution)/shard_map/ppermute | solution.py:23
  67.9 1.5 broadcast_select_fusion
  69.3 8.3 %all-gather.2.cloned.1.call-done = bf16[8,256,768]{2,1,0:T(8,128)(2,1)} async-done(((bf16[1,256,768]{2,1,0:T(8,128)(2,1)}), bf16[8,256,768]{2,1,0:T(8,128)(2,1)}) %all-gather.2.cloned.1.call-update) | async-done | bytes 3145744 | tf_op jit(solution)/shard_map/all_gather | solution.py:319
  77.6 8.8 %early_pass.1 = (bf16[4,8,64,768]{3,2,1,0:T(8,128)(2,1)}, bf16[512,768]{1,0:T(8,128)(2,1)}, bf16[8,4,72,768]{3,2,1,0:T(8,128)(2,1)}) custom-call(bf16[8,4,64,768]{3,2,1,0:T(8,128)(2,1)} %bitcast.51, bf16[256,2048]{1,0:T(8,128)(2,1)} %own_in.2, bf16[256,2048]{1,0:T(8,128)(2,1)} %get-tuple-element.41.low_in, bf16[256,2048]{1,0:T(8,128)(2,1)} %get-tuple-element.40.high_in, ...), custom_call_target="tpu_custom_call" | custom-call | flops 3221225472 | bytes 11534336 | tf_op jit(solution)/shard_map/early_pass/pallas_call | solution.py:146
  86.5 1.9 %copy-done.1 = bf16[4,8,64,768]{3,2,1,0:T(8,128)(2,1)S(1)} copy-done((bf16[4,8,64,768]{3,2,1,0:T(8,128)(2,1)S(1)}, bf16[4,8,64,768]{3,2,1,0:T(8,128)(2,1)}, u32[]{:S(2)}) %copy-start.1) | copy-done | bytes 3145752
  88.3 3.0 %convolution_convert_fusion = bf16[512,2048]{1,0:T(8,128)(2,1)S(1)} fusion(bf16[512,768]{1,0:T(8,128)(2,1)} %get-tuple-element.17, bf16[2048,768]{1,0:T(8,128)(2,1)S(1)} %bitcast.38), kind=kOutput, calls=%fused_computation | convolution fusion | flops 1611661312 | bytes 6029312 | tf_op jit(solution)/shard_map/dot_general | solution.py:327
  91.4 1.9 %collective-permute-start.3 = (bf16[512,1024]{1,0:T(8,128)(2,1)S(1)}, bf16[512,1024]{1,0:T(8,128)(2,1)S(1)}, u32[]{:S(2)}, u32[]{:S(2)}) collective-permute-start(bf16[512,1024]{1,0:T(8,128)(2,1)S(1)} %broadcast_select_fusion.2), channel_id=1, source_target_pairs={{0,1},{1,0},{2,3},{3,2},{4,5},{5,4},{6,7},{7,6},{8,9},{9,8},{10,11... | collective-permute-start | bytes 3145736 | tf_op jit(solution)/shard_map/ppermute | solution.py:23
  93.4 2.6 %collective-permute-done.3 = bf16[512,1024]{1,0:T(8,128)(2,1)S(1)} collective-permute-done((bf16[512,1024]{1,0:T(8,128)(2,1)S(1)}, bf16[512,1024]{1,0:T(8,128)(2,1)S(1)}, u32[]{:S(2)}, u32[]{:S(2)}) %collective-permute-start.3) | collective-permute-done | bytes 1048608 | tf_op jit(solution)/shard_map/ppermute | solution.py:23
  97.8 5.9 %all-to-all-start.1 = ((bf16[8,64,1024]{2,1,0:T(8,128)(2,1)}), bf16[8,64,1024]{2,1,0:T(8,128)(2,1)S(1)}, u32[]{:S(2)}, u32[]{:S(2)}) async-start(bf16[8,64,1024]{2,1,0:T(8,128)(2,1)} %bitcast.7), calls=%async_computation.1 | async-start | bytes 2097152 | tf_op jit(solution)/shard_map/all_to_all | solution.py:337
  103.6 5.5 %late_pass.1 = (bf16[256,384]{1,0:T(8,128)(2,1)}, bf16[256,384]{1,0:T(8,128)(2,1)}) custom-call(bf16[2048,768]{1,0:T(8,128)(2,1)} %bitcast.37, bf16[256,2048]{1,0:T(8,128)(2,1)} %own_in.3, bf16[256,2048]{1,0:T(8,128)(2,1)} %get-tuple-element.41.low_in, bf16[256,2048]{1,0:T(8,128)(2,1)} %get-tuple-element.40.high_in, f32[8,768]{1,0:T(8,128)} %fusion.3.filters_in), custom_call_target="tpu_custom_call" | custom-call | flops 1610612736 | bytes 5242880 | tf_op jit(solution)/shard_map/late_pass/pallas_call | solution.py:224
  109.2 7.8 %all-to-all-done.1 = bf16[8,64,1024]{2,1,0:T(8,128)(2,1)S(1)} async-done(((bf16[8,64,1024]{2,1,0:T(8,128)(2,1)}), bf16[8,64,1024]{2,1,0:T(8,128)(2,1)S(1)}, u32[]{:S(2)}, u32[]{:S(2)}) %all-to-all-start.1) | async-done | bytes 1048608 | tf_op jit(solution)/shard_map/all_to_all | solution.py:337
  118.1 5.2 %all-to-all-start.2 = ((bf16[4,64,1024]{2,1,0:T(8,128)(2,1)}), bf16[4,64,1024]{2,1,0:T(8,128)(2,1)S(1)}, u32[]{:S(2)}, u32[]{:S(2)}) async-start(bf16[4,64,1024]{2,1,0:T(8,128)(2,1)} %broadcast_in_dim.2), calls=%async_computation.3 | async-start | bytes 1048576 | tf_op jit(solution)/shard_map/all_to_all | solution.py:346
  123.2 3.4 %collective-permute-start.4 = (bf16[256,384]{1,0:T(8,128)(2,1)S(1)}, bf16[256,384]{1,0:T(8,128)(2,1)S(1)}, u32[]{:S(2)}, u32[]{:S(2)}) collective-permute-start(bf16[256,384]{1,0:T(8,128)(2,1)S(1)} %copy-done.9), channel_id=1, source_target_pairs={{0,64},{64,0},{1,65},{65,1},{2,66},{66,2},{3,67},{67,3},{4,68},{68... | collective-permute-start | bytes 589832 | tf_op jit(solution)/shard_map/ppermute | solution.py:23
  126.6 4.9 %collective-permute-done.4 = bf16[256,384]{1,0:T(8,128)(2,1)S(1)} collective-permute-done((bf16[256,384]{1,0:T(8,128)(2,1)S(1)}, bf16[256,384]{1,0:T(8,128)(2,1)S(1)}, u32[]{:S(2)}, u32[]{:S(2)}) %collective-permute-start.4) | collective-permute-done | bytes 196640 | tf_op jit(solution)/shard_map/ppermute | solution.py:23
  131.5 5.5 %reduce-scatter.2.cloned.1.call-done = bf16[288,768]{1,0:T(8,128)(2,1)} async-done(((bf16[2304,768]{1,0:T(8,128)(2,1)}), bf16[288,768]{1,0:T(8,128)(2,1)}) %reduce-scatter.2.cloned.1.call-update) | async-done | bytes 442384 | tf_op jit(solution)/shard_map/reduce_scatter | solution.py:325
  137.0 5.1 %all-to-all-start.3 = ((bf16[4,72,768]{2,1,0:T(8,128)(2,1)}), bf16[4,72,768]{2,1,0:T(8,128)(2,1)S(1)}, u32[]{:S(2)}, u32[]{:S(2)}) async-start(bf16[4,72,768]{2,1,0:T(8,128)(2,1)} %bitcast.45), calls=%async_computation.4 | async-start | bytes 884736 | tf_op jit(solution)/shard_map/all_to_all | solution.py:352
  142.1 1.9 %collective-permute-start.5 = (bf16[256,1024]{1,0:T(8,128)(2,1)S(1)}, bf16[256,1024]{1,0:T(8,128)(2,1)S(1)}, u32[]{:S(2)}, u32[]{:S(2)}) collective-permute-start(bf16[256,1024]{1,0:T(8,128)(2,1)S(1)} %bitcast.39), channel_id=1, source_target_pairs={{0,1},{1,0},{2,3},{3,2},{4,5},{5,4},{6,7},{7,6},{8,9},{9,8},{10,11... | collective-permute-start | bytes 1572872 | tf_op jit(solution)/shard_map/ppermute | solution.py:23
  147.3 7.5 %all-to-all-done.3 = bf16[4,72,768]{2,1,0:T(8,128)(2,1)S(1)} async-done(((bf16[4,72,768]{2,1,0:T(8,128)(2,1)}), bf16[4,72,768]{2,1,0:T(8,128)(2,1)S(1)}, u32[]{:S(2)}, u32[]{:S(2)}) %all-to-all-start.3) | async-done | bytes 442400 | tf_op jit(solution)/shard_map/all_to_all | solution.py:352
  (61 shorter events, 12.3 us)
Async XLA Ops:
  7.2 21.0 %copy-start = (bf16[256,2048]{1,0:T(8,128)(2,1)S(1)}, bf16[256,2048]{1,0:T(8,128)(2,1)}, u32[]{:S(2)}) copy-start(bf16[256,2048]{1,0:T(8,128)(2,1)} %own_in.3) | copy-start | bytes 3145732
  7.2 70.4 %all-gather.2.cloned.1.call-start = ((), (), s32[]{:S(2)}) async-start(), calls=%async_computation.5 | async-start | bytes 3538944 | tf_op jit(solution)/shard_map/all_gather | solution.py:319
  28.1 108.9 %reduce-scatter.2.cloned.1.call-start = ((), (), s32[]{:S(2)}) async-start(), calls=%async_computation.6 | async-start | bytes 3981312 | tf_op jit(solution)/shard_map/reduce_scatter | solution.py:325
  29.5 27.9 %slice-start = ((bf16[256,704]{0,1:T(8,128)(2,1)}), bf16[256,320]{0,1:T(8,128)(2,1)S(1)}, s32[]{:S(2)}) async-start(bf16[256,704]{0,1:T(8,128)(2,1)} %param.13), calls=%async_computation.7 | async-start | bytes 327680 | tf_op jit(solution)/shard_map/slice | solution.py:295
  29.5 28.1 %slice-start.1 = ((bf16[256,704]{0,1:T(8,128)(2,1)}), bf16[256,384]{0,1:T(8,128)(2,1)S(1)}, s32[]{:S(2)}) async-start(bf16[256,704]{0,1:T(8,128)(2,1)} %param.13), calls=%async_computation.8 | async-start | bytes 393216 | tf_op jit(solution)/shard_map/slice | solution.py:295
  29.5 30.6 %copy-start.5 = (bf16[3,704]{1,0:T(4,128)(2,1)S(1)}, bf16[3,704]{1,0:T(4,128)(2,1)}, u32[]{:S(2)}) copy-start(bf16[3,704]{1,0:T(4,128)(2,1)} %param.16) | copy-start | bytes 12676
  29.5 30.6 %slice-start.2 = ((bf16[3,704]{1,0:T(4,128)(2,1)}), bf16[3,320]{1,0:T(4,128)(2,1)S(1)}, s32[]{:S(2)}) async-start(bf16[3,704]{1,0:T(4,128)(2,1)} %param.16), calls=%async_computation.9 | async-start | bytes 6144 | tf_op jit(solution)/shard_map/slice | solution.py:295
  29.5 30.6 %copy-start.6 = (bf16[3,704]{1,0:T(4,128)(2,1)S(1)}, bf16[3,704]{1,0:T(4,128)(2,1)}, u32[]{:S(2)}) copy-start(bf16[3,704]{1,0:T(4,128)(2,1)} %param.17) | copy-start | bytes 12676
  29.5 30.6 %slice-start.3 = ((bf16[3,704]{1,0:T(4,128)(2,1)}), bf16[3,320]{1,0:T(4,128)(2,1)S(1)}, s32[]{:S(2)}) async-start(bf16[3,704]{1,0:T(4,128)(2,1)} %param.17), calls=%async_computation.10 | async-start | bytes 6144 | tf_op jit(solution)/shard_map/slice | solution.py:295
  29.6 25.8 %collective-permute-start = (bf16[256,2048]{1,0:T(8,128)(2,1)S(1)}, bf16[256,2048]{1,0:T(8,128)(2,1)S(1)}, u32[]{:S(2)}, u32[]{:S(2)}) collective-permute-start(bf16[256,2048]{1,0:T(8,128)(2,1)S(1)} %pad_maximum_fusion), channel_id=1, source_target_pairs={{0,64},{64,0},{1,65},{65,1},{2,66},{66,2},{3,67},{67,3},{4,68},{68... | collective-permute-start | bytes 3145736 | tf_op jit(solution)/shard_map/ppermute | solution.py:23
  55.5 12.4 %collective-permute-start.1 = (bf16[256,2048]{1,0:T(8,128)(2,1)S(1)}, bf16[256,2048]{1,0:T(8,128)(2,1)S(1)}, u32[]{:S(2)}, u32[]{:S(2)}) collective-permute-start(bf16[256,2048]{1,0:T(8,128)(2,1)S(1)} %collective-permute-done), channel_id=1, source_target_pairs={{0,1},{1,0},{2,3},{3,2},{4,5},{5,4},{6,7},{7,6},{8,9},{9,8},{10,11... | collective-permute-start | bytes 3145736 | tf_op jit(solution)/shard_map/ppermute | solution.py:23
  57.9 9.2 %collective-permute-start.2 = (bf16[256,384]{1,0:T(8,128)(2,1)S(1)}, bf16[256,384]{1,0:T(8,128)(2,1)S(1)}, u32[]{:S(2)}, u32[]{:S(2)}) collective-permute-start(bf16[256,384]{1,0:T(8,128)(2,1)S(1)} %get-tuple-element.49), channel_id=1, source_target_pairs={{0,64},{64,0},{1,65},{65,1},{2,66},{66,2},{3,67},{67,3},{4,68},{68... | collective-permute-start | bytes 589832 | tf_op jit(solution)/shard_map/ppermute | solution.py:23
  91.4 4.6 %collective-permute-start.3 = (bf16[512,1024]{1,0:T(8,128)(2,1)S(1)}, bf16[512,1024]{1,0:T(8,128)(2,1)S(1)}, u32[]{:S(2)}, u32[]{:S(2)}) collective-permute-start(bf16[512,1024]{1,0:T(8,128)(2,1)S(1)} %broadcast_select_fusion.2), channel_id=1, source_target_pairs={{0,1},{1,0},{2,3},{3,2},{4,5},{5,4},{6,7},{7,6},{8,9},{9,8},{10,11... | collective-permute-start | bytes 3145736 | tf_op jit(solution)/shard_map/ppermute | solution.py:23
  97.8 19.3 %all-to-all-start.1 = ((bf16[8,64,1024]{2,1,0:T(8,128)(2,1)}), bf16[8,64,1024]{2,1,0:T(8,128)(2,1)S(1)}, u32[]{:S(2)}, u32[]{:S(2)}) async-start(bf16[8,64,1024]{2,1,0:T(8,128)(2,1)} %bitcast.7), calls=%async_computation.1 | async-start | bytes 2097152 | tf_op jit(solution)/shard_map/all_to_all | solution.py:337
  109.2 14.1 %copy-start.9 = (bf16[256,384]{1,0:T(8,128)(2,1)S(1)}, bf16[256,384]{1,0:T(8,128)(2,1)}, u32[]{:S(2)}) copy-start(bf16[256,384]{1,0:T(8,128)(2,1)} %get-tuple-element.24) | copy-start | bytes 589828
  109.2 34.8 %copy-start.2 = (bf16[256,384]{1,0:T(8,128)(2,1)S(1)}, bf16[256,384]{1,0:T(8,128)(2,1)}, u32[]{:S(2)}) copy-start(bf16[256,384]{1,0:T(8,128)(2,1)} %get-tuple-element.21) | copy-start | bytes 589828
  118.1 13.4 %all-to-all-start.2 = ((bf16[4,64,1024]{2,1,0:T(8,128)(2,1)}), bf16[4,64,1024]{2,1,0:T(8,128)(2,1)S(1)}, u32[]{:S(2)}, u32[]{:S(2)}) async-start(bf16[4,64,1024]{2,1,0:T(8,128)(2,1)} %broadcast_in_dim.2), calls=%async_computation.3 | async-start | bytes 1048576 | tf_op jit(solution)/shard_map/all_to_all | solution.py:346
  123.2 8.2 %collective-permute-start.4 = (bf16[256,384]{1,0:T(8,128)(2,1)S(1)}, bf16[256,384]{1,0:T(8,128)(2,1)S(1)}, u32[]{:S(2)}, u32[]{:S(2)}) collective-permute-start(bf16[256,384]{1,0:T(8,128)(2,1)S(1)} %copy-done.9), channel_id=1, source_target_pairs={{0,64},{64,0},{1,65},{65,1},{2,66},{66,2},{3,67},{67,3},{4,68},{68... | collective-permute-start | bytes 589832 | tf_op jit(solution)/shard_map/ppermute | solution.py:23
  137.0 17.7 %all-to-all-start.3 = ((bf16[4,72,768]{2,1,0:T(8,128)(2,1)}), bf16[4,72,768]{2,1,0:T(8,128)(2,1)S(1)}, u32[]{:S(2)}, u32[]{:S(2)}) async-start(bf16[4,72,768]{2,1,0:T(8,128)(2,1)} %bitcast.45), calls=%async_computation.4 | async-start | bytes 884736 | tf_op jit(solution)/shard_map/all_to_all | solution.py:352
  142.1 3.8 %collective-permute-start.5 = (bf16[256,1024]{1,0:T(8,128)(2,1)S(1)}, bf16[256,1024]{1,0:T(8,128)(2,1)S(1)}, u32[]{:S(2)}, u32[]{:S(2)}) collective-permute-start(bf16[256,1024]{1,0:T(8,128)(2,1)S(1)} %bitcast.39), channel_id=1, source_target_pairs={{0,1},{1,0},{2,3},{3,2},{4,5},{5,4},{6,7},{7,6},{8,9},{9,8},{10,11... | collective-permute-start | bytes 1572872 | tf_op jit(solution)/shard_map/ppermute | solution.py:23
  145.1 9.8 %copy-start.3 = (f32[64,704]{1,0:T(8,128)S(1)}, f32[64,704]{1,0:T(8,128)}, u32[]{:S(2)}) copy-start(f32[64,704]{1,0:T(8,128)} %param.19) | copy-start | bytes 540676
  145.1 10.6 %copy-start.7 = (f32[3,704]{1,0:T(4,128)S(1)}, f32[3,704]{1,0:T(4,128)}, u32[]{:S(2)}) copy-start(f32[3,704]{1,0:T(4,128)} %param.21) | copy-start | bytes 25348
  145.1 11.2 %copy-start.8 = (f32[3,704]{1,0:T(4,128)S(1)}, f32[3,704]{1,0:T(4,128)}, u32[]{:S(2)}) copy-start(f32[3,704]{1,0:T(4,128)} %param.20) | copy-start | bytes 25348
  145.1 11.8 %copy-start.4 = (f32[64,704]{1,0:T(8,128)S(1)}, f32[64,704]{1,0:T(8,128)}, u32[]{:S(2)}) copy-start(f32[64,704]{1,0:T(8,128)} %param.18) | copy-start | bytes 540676
  (1 other events, 1.9 us)
Sparse Core Ops, SparseCore 0:
  28.2 49.3 all-gather.1
  86.6 50.3 reduce-scatter.1

commit v9 on v8

--- a/solution.py
+++ b/solution.py
@@ -62,8 +62,8 @@
     wide = columns // 2
     span = n_y * shard_rows
     fetches = [
-        pltpu.make_async_copy(gathered.at[y], weight.at[:, y], in_sems.at[y])
-        for y in range(n_y)
+        pltpu.make_async_copy(gathered.at[:, z], weight.at[z], in_sems.at[z])
+        for z in range(n_z)
     ]
     pairs = (
         (own_in, own),
@@ -73,12 +73,23 @@
         (high_in.at[:cut], other.at[cut:]),
     )
     fetches += [
-        pltpu.make_async_copy(source, target, in_sems.at[n_y + at])
+        pltpu.make_async_copy(source, target, in_sems.at[n_z + at])
         for at, (source, target) in enumerate(pairs)
     ]
-    for fetch in fetches:
+    blocks, mine, later = fetches[:n_z], fetches[n_z], fetches[n_z + 1 :]
+    mine.start()
+    for fetch in blocks + later:
         fetch.start()
-    for fetch in fetches:
+    first_pre = jnp.zeros((length, columns), jnp.float32)
+    mine.wait()
+    for z, fetch in enumerate(blocks):
+        fetch.wait()
+        first_pre = first_pre + jnp.dot(
+            own[:, z * span : (z + 1) * span],
+            weight[z].reshape(span, columns),
+            preferred_element_type=jnp.float32,
+        )
+    for fetch in later:
         fetch.wait()
     first, second, third = filters[0:1, :], filters[1:2, :], filters[2:3, :]
     slope = math.sqrt(2.0 / math.pi)
@@ -86,11 +97,13 @@
     stores = [pltpu.make_async_copy(weight, weight_out, out_sems.at[0])]
     stores[0].start()
     for part, rows in enumerate((own, other)):
-        pre = jnp.dot(
-            rows[...],
-            weight[...].reshape(n_z * span, columns),
-            preferred_element_type=jnp.float32,
-        )
+        pre = first_pre
+        if part:
+            pre = jnp.dot(
+                rows[...],
+                weight[...].reshape(n_z * span, columns),
+                preferred_element_type=jnp.float32,
+            )
         pre = pre.astype(jnp.bfloat16).astype(jnp.float32)
         one_back, two_back = moved(pre, 1), moved(pre, 2)
         mixed = first * two_back + second * one_back + third * pre
@@ -160,7 +173,7 @@
             pltpu.VMEM(own.shape, jnp.bfloat16),
             pltpu.VMEM(cotangent.shape, jnp.bfloat16),
             pltpu.VMEM((8, columns), jnp.float32),
-            pltpu.SemaphoreType.DMA((n_y + 5,)),
+            pltpu.SemaphoreType.DMA((n_z + 5,)),
             pltpu.SemaphoreType.DMA((2 + n_z,)),
         ],
         compiler_params=pltpu.CompilerParams(vmem_limit_bytes=57 * 1024 * 1024),
@@ -261,8 +274,41 @@
         out_shape=jax.ShapeDtypeStruct((count, gate.shape[0], 2 * wide), gate.dtype),
         in_specs=[whole] * 2,
         out_specs=whole,
+        compiler_params=pltpu.CompilerParams(vmem_limit_bytes=4 * 1024 * 1024),
         name="pack_halves",
     )(gate, up)
+
+
+def closing_kernel(pieces, gate, up, gate_taps, up_taps, *outs):
+    wide = pieces.shape[2] // 2
+    shard_rows, width = gate.shape
+    rest = width - wide
+    sums = [
+        pieces[side].astype(jnp.float32) + pieces[2 + side].astype(jnp.float32)
+        for side in (0, 1)
+    ]
+    for source, taps, out, taps_out, at in (
+        (gate, gate_taps, outs[0], outs[2], 0),
+        (up, up_taps, outs[1], outs[3], wide),
+    ):
+        for total, start, count in ((sums[0], 0, wide), (sums[1], wide, rest)):
+            part = total[:, at : at + count]
+            columns = slice(start, start + count)
+            out[:, columns] = source[:, columns] + part[:shard_rows]
+            extra = part[shard_rows:]
+            taps_out[:, columns] = taps[:, columns] + (extra[:3] + extra[3:6])
+
+
+def closing(pieces, *sums):
+    whole = pl.BlockSpec(memory_space=pltpu.VMEM)
+    return pl.pallas_call(
+        closing_kernel,
+        out_shape=tuple(jax.ShapeDtypeStruct(a.shape, a.dtype) for a in sums),
+        in_specs=[whole] * 5,
+        out_specs=(whole,) * 4,
+        compiler_params=pltpu.CompilerParams(vmem_limit_bytes=4 * 1024 * 1024),
+        name="closing",
+    )(pieces, *sums)
 
 
 def per_device(
@@ -350,10 +396,7 @@
         (reduced, finished, late_there)
     )
     pieces = lax.all_to_all(reduced, Z, 0, 0, tiled=True)
-    pieces = pieces.reshape(2, 2, shard_rows + EXTRA, 2 * wide).astype(jnp.float32)
-    pieces = jnp.sum(pieces, axis=0)
-    taps = pieces[:, shard_rows : shard_rows + 3] + pieces[:, shard_rows + 3 : shard_rows + 6]
-    pieces = pieces[:, :shard_rows]
+    closed = closing(pieces, gate_grad_sum, up_grad_sum, gate_taps_sum, up_taps_sum)
 
     def both(mine, other):
         return joined(pick(first_z, mine, other), pick(first_z, other, mine))
@@ -368,10 +411,7 @@
     return (
         late_hidden,
         early_grad,
-        gate_grad_sum + joined(pieces[0, :, :wide], pieces[1, :, :wide]),
-        up_grad_sum + joined(pieces[0, :, wide:], pieces[1, :, wide:]),
-        gate_taps_sum + joined(taps[0, :, :wide], taps[1, :, :wide]),
-        up_taps_sum + joined(taps[0, :, wide:], taps[1, :, wide:]),
+        *closed,
     )
 
 

time: 165 us -> 163 us (0.988)
  other arithmetic: 10.6 us -> 7.9 us
  local copies, waits for them, and re-layouts: 4.05 us -> 5.8 us
    add x5 -> x0, other arithmetic: 2.63 us -> none  [the longest x1 0.71 us: per_device(): up_grad_sum + joined(pieces[0, :, wide:], pieces[1, :, wide:])]
    unnamed x23 -> x27, local copies, waits for them, and re-layouts: 3.14 us -> 4.92 us
    pallas_call x1, Pallas kernels: 1.8 us -> 0.04 us  [packed_halves(): pl.pallas_call(pack_kernel, out_shape=jax.ShapeDtypeStruct((count, gate.s...]
where the time goes in v9:
time: 163 us
  waiting for transfers between devices  67.4 us (41%)
  starting transfers between devices  29.8 us (18%)
  blocking collectives  19 us (12%)
  Pallas kernels  15.4 us (9%)
  between operations  14.4 us (9%)
  other arithmetic  7.9 us (5%)
  local copies, waits for them, and re-layouts  5.8 us (4%)
  matrix products  2.96 us (2%)
    ppermute x6, waiting for transfers between devices, swapped(): return lax.ppermute(values, axis, [(0, 1), (1, 0)])  38.2 us
    all_to_all x1, blocking collectives, per_device(): block = lax.all_to_all(for_z, Z, 0, 0, tiled=True)  19 us
    ppermute x6, starting transfers between devices, swapped(): return lax.ppermute(values, axis, [(0, 1), (1, 0)])  13.6 us
    pallas_call x1, Pallas kernels, early_pass(): pl.pallas_call(functools.partial(early_kernel, scale), out_shape=(jax.Sha...  9.06 us
    all_gather x1, waiting for transfers between devices, per_device(): weight = lax.all_gather(block, 'y').reshape(n_y, n_z, shard_rows, 2 * wide)  8.31 us
    all_to_all x1, waiting for transfers between devices, per_device(): lax.all_to_all(chip.reshape(2 * n_x, row_count // n_x, cut), ('zb', 'x'),...  7.85 us
    all_to_all x1, waiting for transfers between devices, per_device(): pieces = lax.all_to_all(reduced, Z, 0, 0, tiled=True)  7.51 us
    all_to_all x1, starting transfers between devices, per_device(): lax.all_to_all(chip.reshape(2 * n_x, row_count // n_x, cut), ('zb', 'x'),...  5.88 us
  transfers between devices with their start and end apart: 11, of which 9 were waited for; matrix products, arithmetic and copies ran while one was open for 8% of the time, Pallas kernels for 3%

profile of v9, /device:TPU:6, one launch (start us, length us, event | category | flops | bytes accessed | tf_op | source)
XLA Modules:
  0.0 162.6 jit_solution(9487353443627806259)
XLA Ops:
  9.0 19.0 %all_to_all.20 = bf16[4,64,768]{2,1,0:T(8,128)(2,1)} all-to-all(bf16[4,64,768]{2,1,0:T(8,128)(2,1)S(1)} %pack_halves.1), channel_id=1, replica_groups=mesh['rep'=2,'zp'=2,'zb'=2,'y'=8,'x'=4,'c'=2] {'zp','zb'}, dimensions={0} | all-to-all | bytes 786432 | tf_op jit(solution)/shard_map/all_to_all | solution.py:351
  29.6 2.3 %collective-permute-start = (bf16[256,2048]{1,0:T(8,128)(2,1)S(1)}, bf16[256,2048]{1,0:T(8,128)(2,1)S(1)}, u32[]{:S(2)}, u32[]{:S(2)}) collective-permute-start(bf16[256,2048]{1,0:T(8,128)(2,1)S(1)} %pad_maximum_fusion), channel_id=1, source_target_pairs={{0,64},{64,0},{1,65},{65,1},{2,66},{66,2},{3,67},{67,3},{4,68},{68... | collective-permute-start | bytes 3145736 | tf_op jit(solution)/shard_map/ppermute | solution.py:23
  31.9 23.6 %collective-permute-done = bf16[256,2048]{1,0:T(8,128)(2,1)S(1)} collective-permute-done((bf16[256,2048]{1,0:T(8,128)(2,1)S(1)}, bf16[256,2048]{1,0:T(8,128)(2,1)S(1)}, u32[]{:S(2)}, u32[]{:S(2)}) %collective-permute-start) | collective-permute-done | bytes 1048608 | tf_op jit(solution)/shard_map/ppermute | solution.py:23
  55.4 1.9 %collective-permute-start.1 = (bf16[256,2048]{1,0:T(8,128)(2,1)S(1)}, bf16[256,2048]{1,0:T(8,128)(2,1)S(1)}, u32[]{:S(2)}, u32[]{:S(2)}) collective-permute-start(bf16[256,2048]{1,0:T(8,128)(2,1)S(1)} %collective-permute-done), channel_id=1, source_target_pairs={{0,1},{1,0},{2,3},{3,2},{4,5},{5,4},{6,7},{7,6},{8,9},{9,8},{10,11... | collective-permute-start | bytes 3145736 | tf_op jit(solution)/shard_map/ppermute | solution.py:23
  57.8 2.2 %collective-permute-start.2 = (bf16[256,384]{1,0:T(8,128)(2,1)S(1)}, bf16[256,384]{1,0:T(8,128)(2,1)S(1)}, u32[]{:S(2)}, u32[]{:S(2)}) collective-permute-start(bf16[256,384]{1,0:T(8,128)(2,1)S(1)} %get-tuple-element.53), channel_id=1, source_target_pairs={{0,64},{64,0},{1,65},{65,1},{2,66},{66,2},{3,67},{67,3},{4,68},{68... | collective-permute-start | bytes 589832 | tf_op jit(solution)/shard_map/ppermute | solution.py:23
  60.7 6.3 %collective-permute-done.2 = bf16[256,384]{1,0:T(8,128)(2,1)S(1)} collective-permute-done((bf16[256,384]{1,0:T(8,128)(2,1)S(1)}, bf16[256,384]{1,0:T(8,128)(2,1)S(1)}, u32[]{:S(2)}, u32[]{:S(2)}) %collective-permute-start.2) | collective-permute-done | bytes 196640 | tf_op jit(solution)/shard_map/ppermute | solution.py:23
  67.8 1.5 broadcast_select_fusion
  69.3 8.3 %all-gather.2.cloned.1.call-done = bf16[8,256,768]{2,1,0:T(8,128)(2,1)} async-done(((bf16[1,256,768]{2,1,0:T(8,128)(2,1)}), bf16[8,256,768]{2,1,0:T(8,128)(2,1)}) %all-gather.2.cloned.1.call-update) | async-done | bytes 3145744 | tf_op jit(solution)/shard_map/all_gather | solution.py:365
  77.6 9.1 %early_pass.1 = (bf16[4,8,64,768]{3,2,1,0:T(8,128)(2,1)}, bf16[512,768]{1,0:T(8,128)(2,1)}, bf16[8,4,72,768]{3,2,1,0:T(8,128)(2,1)}) custom-call(bf16[8,4,64,768]{3,2,1,0:T(8,128)(2,1)} %bitcast.24, bf16[256,2048]{1,0:T(8,128)(2,1)} %own_in.2, bf16[256,2048]{1,0:T(8,128)(2,1)} %get-tuple-element.49.low_in, bf16[256,2048]{1,0:T(8,128)(2,1)} %get-tuple-element.48.high_in, ...), custom_call_target="tpu_custom_call" | custom-call | flops 3221225472 | bytes 11534336 | tf_op jit(solution)/shard_map/early_pass/pallas_call | solution.py:159
  86.7 1.9 %copy-done.7 = bf16[4,8,64,768]{3,2,1,0:T(8,128)(2,1)S(1)} copy-done((bf16[4,8,64,768]{3,2,1,0:T(8,128)(2,1)S(1)}, bf16[4,8,64,768]{3,2,1,0:T(8,128)(2,1)}, u32[]{:S(2)}) %copy-start.7) | copy-done | bytes 3145752
  88.5 3.0 %convolution_convert_fusion = bf16[512,2048]{1,0:T(8,128)(2,1)S(1)} fusion(bf16[512,768]{1,0:T(8,128)(2,1)} %get-tuple-element.21, bf16[2048,768]{1,0:T(8,128)(2,1)S(1)} %bitcast.16), kind=kOutput, calls=%fused_computation | convolution fusion | flops 1611661312 | bytes 6029312 | tf_op jit(solution)/shard_map/dot_general | solution.py:373
  91.6 1.9 %collective-permute-start.3 = (bf16[512,1024]{1,0:T(8,128)(2,1)S(1)}, bf16[512,1024]{1,0:T(8,128)(2,1)S(1)}, u32[]{:S(2)}, u32[]{:S(2)}) collective-permute-start(bf16[512,1024]{1,0:T(8,128)(2,1)S(1)} %broadcast_select_fusion.2), channel_id=1, source_target_pairs={{0,1},{1,0},{2,3},{3,2},{4,5},{5,4},{6,7},{7,6},{8,9},{9,8},{10,11... | collective-permute-start | bytes 3145736 | tf_op jit(solution)/shard_map/ppermute | solution.py:23
  93.5 2.6 %collective-permute-done.3 = bf16[512,1024]{1,0:T(8,128)(2,1)S(1)} collective-permute-done((bf16[512,1024]{1,0:T(8,128)(2,1)S(1)}, bf16[512,1024]{1,0:T(8,128)(2,1)S(1)}, u32[]{:S(2)}, u32[]{:S(2)}) %collective-permute-start.3) | collective-permute-done | bytes 1048608 | tf_op jit(solution)/shard_map/ppermute | solution.py:23
  98.0 5.9 %all-to-all-start.1 = ((bf16[8,64,1024]{2,1,0:T(8,128)(2,1)}), bf16[8,64,1024]{2,1,0:T(8,128)(2,1)S(1)}, u32[]{:S(2)}, u32[]{:S(2)}) async-start(bf16[8,64,1024]{2,1,0:T(8,128)(2,1)} %bitcast.7), calls=%async_computation.1 | async-start | bytes 2097152 | tf_op jit(solution)/shard_map/all_to_all | solution.py:383
  103.8 5.5 %late_pass.1 = (bf16[256,384]{1,0:T(8,128)(2,1)}, bf16[256,384]{1,0:T(8,128)(2,1)}) custom-call(bf16[2048,768]{1,0:T(8,128)(2,1)} %bitcast.15, bf16[256,2048]{1,0:T(8,128)(2,1)} %own_in.3, bf16[256,2048]{1,0:T(8,128)(2,1)} %get-tuple-element.49.low_in, bf16[256,2048]{1,0:T(8,128)(2,1)} %get-tuple-element.48.high_in, f32[8,768]{1,0:T(8,128)} %fusion.3.filters_in), custom_call_target="tpu_custom_call" | custom-call | flops 1610612736 | bytes 5242880 | tf_op jit(solution)/shard_map/late_pass/pallas_call | solution.py:237
  109.4 7.8 %all-to-all-done.1 = bf16[8,64,1024]{2,1,0:T(8,128)(2,1)S(1)} async-done(((bf16[8,64,1024]{2,1,0:T(8,128)(2,1)}), bf16[8,64,1024]{2,1,0:T(8,128)(2,1)S(1)}, u32[]{:S(2)}, u32[]{:S(2)}) %all-to-all-start.1) | async-done | bytes 1048608 | tf_op jit(solution)/shard_map/all_to_all | solution.py:383
  118.2 5.2 %all-to-all-start.2 = ((bf16[4,64,1024]{2,1,0:T(8,128)(2,1)}), bf16[4,64,1024]{2,1,0:T(8,128)(2,1)S(1)}, u32[]{:S(2)}, u32[]{:S(2)}) async-start(bf16[4,64,1024]{2,1,0:T(8,128)(2,1)} %broadcast_in_dim.2), calls=%async_computation.3 | async-start | bytes 1048576 | tf_op jit(solution)/shard_map/all_to_all | solution.py:392
  123.4 3.4 %collective-permute-start.4 = (bf16[256,384]{1,0:T(8,128)(2,1)S(1)}, bf16[256,384]{1,0:T(8,128)(2,1)S(1)}, u32[]{:S(2)}, u32[]{:S(2)}) collective-permute-start(bf16[256,384]{1,0:T(8,128)(2,1)S(1)} %copy-done.11), channel_id=1, source_target_pairs={{0,64},{64,0},{1,65},{65,1},{2,66},{66,2},{3,67},{67,3},{4,68},{68... | collective-permute-start | bytes 589832 | tf_op jit(solution)/shard_map/ppermute | solution.py:23
  126.8 4.9 %collective-permute-done.4 = bf16[256,384]{1,0:T(8,128)(2,1)S(1)} collective-permute-done((bf16[256,384]{1,0:T(8,128)(2,1)S(1)}, bf16[256,384]{1,0:T(8,128)(2,1)S(1)}, u32[]{:S(2)}, u32[]{:S(2)}) %collective-permute-start.4) | collective-permute-done | bytes 196640 | tf_op jit(solution)/shard_map/ppermute | solution.py:23
  131.7 5.5 %reduce-scatter.2.cloned.1.call-done = bf16[288,768]{1,0:T(8,128)(2,1)} async-done(((bf16[2304,768]{1,0:T(8,128)(2,1)}), bf16[288,768]{1,0:T(8,128)(2,1)}) %reduce-scatter.2.cloned.1.call-update) | async-done | bytes 442384 | tf_op jit(solution)/shard_map/reduce_scatter | solution.py:371
  137.2 5.1 %all-to-all-start.3 = ((bf16[4,72,768]{2,1,0:T(8,128)(2,1)}), bf16[4,72,768]{2,1,0:T(8,128)(2,1)S(1)}, u32[]{:S(2)}, u32[]{:S(2)}) async-start(bf16[4,72,768]{2,1,0:T(8,128)(2,1)} %bitcast.22), calls=%async_computation.4 | async-start | bytes 884736 | tf_op jit(solution)/shard_map/all_to_all | solution.py:398
  142.3 1.9 %collective-permute-start.5 = (bf16[256,1024]{1,0:T(8,128)(2,1)S(1)}, bf16[256,1024]{1,0:T(8,128)(2,1)S(1)}, u32[]{:S(2)}, u32[]{:S(2)}) collective-permute-start(bf16[256,1024]{1,0:T(8,128)(2,1)S(1)} %bitcast.17), channel_id=1, source_target_pairs={{0,1},{1,0},{2,3},{3,2},{4,5},{5,4},{6,7},{7,6},{8,9},{9,8},{10,11... | collective-permute-start | bytes 1572872 | tf_op jit(solution)/shard_map/ppermute | solution.py:23
  146.1 1.4 maximum_select_fusion
  147.4 7.5 %all-to-all-done.3.pieces = bf16[4,72,768]{2,1,0:T(8,128)(2,1)S(1)} async-done(((bf16[4,72,768]{2,1,0:T(8,128)(2,1)}), bf16[4,72,768]{2,1,0:T(8,128)(2,1)S(1)}, u32[]{:S(2)}, u32[]{:S(2)}) %all-to-all-start.3) | async-done | bytes 442400 | tf_op jit(solution)/shard_map/all_to_all | solution.py:398
  (58 shorter events, 10.7 us)
Async XLA Ops:
  7.2 70.4 %all-gather.2.cloned.1.call-start = ((), (), s32[]{:S(2)}) async-start(), calls=%async_computation.5 | async-start | bytes 3538944 | tf_op jit(solution)/shard_map/all_gather | solution.py:365
  9.0 19.1 %copy-start.6 = (bf16[256,2048]{1,0:T(8,128)(2,1)S(1)}, bf16[256,2048]{1,0:T(8,128)(2,1)}, u32[]{:S(2)}) copy-start(bf16[256,2048]{1,0:T(8,128)(2,1)} %own_in.3) | copy-start | bytes 3145732
  28.0 109.1 %reduce-scatter.2.cloned.1.call-start = ((), (), s32[]{:S(2)}) async-start(), calls=%async_computation.6 | async-start | bytes 3981312 | tf_op jit(solution)/shard_map/reduce_scatter | solution.py:371
  29.4 27.9 %slice-start = ((bf16[256,704]{0,1:T(8,128)(2,1)}), bf16[256,320]{0,1:T(8,128)(2,1)S(1)}, s32[]{:S(2)}) async-start(bf16[256,704]{0,1:T(8,128)(2,1)} %param.13), calls=%async_computation.7 | async-start | bytes 327680 | tf_op jit(solution)/shard_map/slice | solution.py:341
  29.4 28.1 %slice-start.1 = ((bf16[256,704]{0,1:T(8,128)(2,1)}), bf16[256,384]{0,1:T(8,128)(2,1)S(1)}, s32[]{:S(2)}) async-start(bf16[256,704]{0,1:T(8,128)(2,1)} %param.13), calls=%async_computation.8 | async-start | bytes 393216 | tf_op jit(solution)/shard_map/slice | solution.py:341
  29.4 30.6 %copy-start.9 = (bf16[3,704]{1,0:T(4,128)(2,1)S(1)}, bf16[3,704]{1,0:T(4,128)(2,1)}, u32[]{:S(2)}) copy-start(bf16[3,704]{1,0:T(4,128)(2,1)} %param.16) | copy-start | bytes 12676
  29.5 30.6 %slice-start.2 = ((bf16[3,704]{1,0:T(4,128)(2,1)}), bf16[3,320]{1,0:T(4,128)(2,1)S(1)}, s32[]{:S(2)}) async-start(bf16[3,704]{1,0:T(4,128)(2,1)} %param.16), calls=%async_computation.9 | async-start | bytes 6144 | tf_op jit(solution)/shard_map/slice | solution.py:341
  29.5 30.6 %copy-start.10 = (bf16[3,704]{1,0:T(4,128)(2,1)S(1)}, bf16[3,704]{1,0:T(4,128)(2,1)}, u32[]{:S(2)}) copy-start(bf16[3,704]{1,0:T(4,128)(2,1)} %param.17) | copy-start | bytes 12676
  29.5 30.6 %slice-start.3 = ((bf16[3,704]{1,0:T(4,128)(2,1)}), bf16[3,320]{1,0:T(4,128)(2,1)S(1)}, s32[]{:S(2)}) async-start(bf16[3,704]{1,0:T(4,128)(2,1)} %param.17), calls=%async_computation.10 | async-start | bytes 6144 | tf_op jit(solution)/shard_map/slice | solution.py:341
  29.6 25.8 %collective-permute-start = (bf16[256,2048]{1,0:T(8,128)(2,1)S(1)}, bf16[256,2048]{1,0:T(8,128)(2,1)S(1)}, u32[]{:S(2)}, u32[]{:S(2)}) collective-permute-start(bf16[256,2048]{1,0:T(8,128)(2,1)S(1)} %pad_maximum_fusion), channel_id=1, source_target_pairs={{0,64},{64,0},{1,65},{65,1},{2,66},{66,2},{3,67},{67,3},{4,68},{68... | collective-permute-start | bytes 3145736 | tf_op jit(solution)/shard_map/ppermute | solution.py:23
  55.4 12.4 %collective-permute-start.1 = (bf16[256,2048]{1,0:T(8,128)(2,1)S(1)}, bf16[256,2048]{1,0:T(8,128)(2,1)S(1)}, u32[]{:S(2)}, u32[]{:S(2)}) collective-permute-start(bf16[256,2048]{1,0:T(8,128)(2,1)S(1)} %collective-permute-done), channel_id=1, source_target_pairs={{0,1},{1,0},{2,3},{3,2},{4,5},{5,4},{6,7},{7,6},{8,9},{9,8},{10,11... | collective-permute-start | bytes 3145736 | tf_op jit(solution)/shard_map/ppermute | solution.py:23
  57.8 9.2 %collective-permute-start.2 = (bf16[256,384]{1,0:T(8,128)(2,1)S(1)}, bf16[256,384]{1,0:T(8,128)(2,1)S(1)}, u32[]{:S(2)}, u32[]{:S(2)}) collective-permute-start(bf16[256,384]{1,0:T(8,128)(2,1)S(1)} %get-tuple-element.53), channel_id=1, source_target_pairs={{0,64},{64,0},{1,65},{65,1},{2,66},{66,2},{3,67},{67,3},{4,68},{68... | collective-permute-start | bytes 589832 | tf_op jit(solution)/shard_map/ppermute | solution.py:23
  91.6 4.6 %collective-permute-start.3 = (bf16[512,1024]{1,0:T(8,128)(2,1)S(1)}, bf16[512,1024]{1,0:T(8,128)(2,1)S(1)}, u32[]{:S(2)}, u32[]{:S(2)}) collective-permute-start(bf16[512,1024]{1,0:T(8,128)(2,1)S(1)} %broadcast_select_fusion.2), channel_id=1, source_target_pairs={{0,1},{1,0},{2,3},{3,2},{4,5},{5,4},{6,7},{7,6},{8,9},{9,8},{10,11... | collective-permute-start | bytes 3145736 | tf_op jit(solution)/shard_map/ppermute | solution.py:23
  98.0 19.3 %all-to-all-start.1 = ((bf16[8,64,1024]{2,1,0:T(8,128)(2,1)}), bf16[8,64,1024]{2,1,0:T(8,128)(2,1)S(1)}, u32[]{:S(2)}, u32[]{:S(2)}) async-start(bf16[8,64,1024]{2,1,0:T(8,128)(2,1)} %bitcast.7), calls=%async_computation.1 | async-start | bytes 2097152 | tf_op jit(solution)/shard_map/all_to_all | solution.py:383
  109.3 14.1 %copy-start.11 = (bf16[256,384]{1,0:T(8,128)(2,1)S(1)}, bf16[256,384]{1,0:T(8,128)(2,1)}, u32[]{:S(2)}) copy-start(bf16[256,384]{1,0:T(8,128)(2,1)} %get-tuple-element.28) | copy-start | bytes 589828
  109.4 34.8 %copy-start.8 = (bf16[256,384]{1,0:T(8,128)(2,1)S(1)}, bf16[256,384]{1,0:T(8,128)(2,1)}, u32[]{:S(2)}) copy-start(bf16[256,384]{1,0:T(8,128)(2,1)} %get-tuple-element.25) | copy-start | bytes 589828
  118.2 13.4 %all-to-all-start.2 = ((bf16[4,64,1024]{2,1,0:T(8,128)(2,1)}), bf16[4,64,1024]{2,1,0:T(8,128)(2,1)S(1)}, u32[]{:S(2)}, u32[]{:S(2)}) async-start(bf16[4,64,1024]{2,1,0:T(8,128)(2,1)} %broadcast_in_dim.2), calls=%async_computation.3 | async-start | bytes 1048576 | tf_op jit(solution)/shard_map/all_to_all | solution.py:392
  123.4 8.2 %collective-permute-start.4 = (bf16[256,384]{1,0:T(8,128)(2,1)S(1)}, bf16[256,384]{1,0:T(8,128)(2,1)S(1)}, u32[]{:S(2)}, u32[]{:S(2)}) collective-permute-start(bf16[256,384]{1,0:T(8,128)(2,1)S(1)} %copy-done.11), channel_id=1, source_target_pairs={{0,64},{64,0},{1,65},{65,1},{2,66},{66,2},{3,67},{67,3},{4,68},{68... | collective-permute-start | bytes 589832 | tf_op jit(solution)/shard_map/ppermute | solution.py:23
  137.2 17.8 %all-to-all-start.3 = ((bf16[4,72,768]{2,1,0:T(8,128)(2,1)}), bf16[4,72,768]{2,1,0:T(8,128)(2,1)S(1)}, u32[]{:S(2)}, u32[]{:S(2)}) async-start(bf16[4,72,768]{2,1,0:T(8,128)(2,1)} %bitcast.22), calls=%async_computation.4 | async-start | bytes 884736 | tf_op jit(solution)/shard_map/all_to_all | solution.py:398
  142.3 3.8 %collective-permute-start.5 = (bf16[256,1024]{1,0:T(8,128)(2,1)S(1)}, bf16[256,1024]{1,0:T(8,128)(2,1)S(1)}, u32[]{:S(2)}, u32[]{:S(2)}) collective-permute-start(bf16[256,1024]{1,0:T(8,128)(2,1)S(1)} %bitcast.17), channel_id=1, source_target_pairs={{0,1},{1,0},{2,3},{3,2},{4,5},{5,4},{6,7},{7,6},{8,9},{9,8},{10,11... | collective-permute-start | bytes 1572872 | tf_op jit(solution)/shard_map/ppermute | solution.py:23
  144.2 10.7 %copy-start = (f32[64,704]{1,0:T(8,128)S(1)}, f32[64,704]{1,0:T(8,128)}, u32[]{:S(2)}) copy-start(f32[64,704]{1,0:T(8,128)} %gate.3) | copy-start | bytes 540676
  144.2 10.7 %copy-start.1 = (f32[64,704]{1,0:T(8,128)S(1)}, f32[64,704]{1,0:T(8,128)}, u32[]{:S(2)}) copy-start(f32[64,704]{1,0:T(8,128)} %up.3) | copy-start | bytes 540676
  144.3 10.7 %copy-start.4 = (f32[3,704]{1,0:T(4,128)S(1)}, f32[3,704]{1,0:T(4,128)}, u32[]{:S(2)}) copy-start(f32[3,704]{1,0:T(4,128)} %gate_taps.1) | copy-start | bytes 25348
  144.3 10.7 %copy-start.5 = (f32[3,704]{1,0:T(4,128)S(1)}, f32[3,704]{1,0:T(4,128)}, u32[]{:S(2)}) copy-start(f32[3,704]{1,0:T(4,128)} %up_taps.1) | copy-start | bytes 25348
  (3 other events, 3.7 us)
Sparse Core Ops, SparseCore 0:
  28.2 49.3 all-gather.1
  86.8 50.3 reduce-scatter.1

commit v10 on v9

--- a/solution.py
+++ b/solution.py
@@ -80,15 +80,14 @@
     mine.start()
     for fetch in blocks + later:
         fetch.start()
-    first_pre = jnp.zeros((length, columns), jnp.float32)
     mine.wait()
-    for z, fetch in enumerate(blocks):
+    for fetch in blocks:
         fetch.wait()
-        first_pre = first_pre + jnp.dot(
-            own[:, z * span : (z + 1) * span],
-            weight[z].reshape(span, columns),
-            preferred_element_type=jnp.float32,
-        )
+    first_pre = jnp.dot(
+        own[...],
+        weight[...].reshape(n_z * span, columns),
+        preferred_element_type=jnp.float32,
+    )
     for fetch in later:
         fetch.wait()
     first, second, third = filters[0:1, :], filters[1:2, :], filters[2:3, :]
@@ -392,8 +391,9 @@
     finished = lax.all_to_all(copies, "x", 0, 0, tiled=True).reshape(row_count, cut)
     late_there = swapped(late_sent, "zb")
 
-    reduced, finished, late_there = lax.optimization_barrier(
-        (reduced, finished, late_there)
+    beside = swapped(finished, "c")
+    reduced, finished, beside, late_there = lax.optimization_barrier(
+        (reduced, finished, beside, late_there)
     )
     pieces = lax.all_to_all(reduced, Z, 0, 0, tiled=True)
     closed = closing(pieces, gate_grad_sum, up_grad_sum, gate_taps_sum, up_taps_sum)
@@ -401,7 +401,6 @@
     def both(mine, other):
         return joined(pick(first_z, mine, other), pick(first_z, other, mine))
 
-    beside = swapped(finished, "c")
     early_grad = pick(
         first_c,
         jnp.concatenate([finished, beside], axis=1),

time: 163 us -> 168 us (1.031); the launches traced: 163 us -> 166 us
  blocking collectives: 19 us -> 30.8 us
  starting transfers between devices: 29.8 us -> 24.5 us
  waiting for transfers between devices: 67.4 us -> 64.6 us
    all_to_all x0 -> x1, blocking collectives: none -> 11.8 us  [per_device(): lax.all_to_all(copies, 'x', 0, 0, tiled=True).reshape(row_count, cut)]
    reduce_scatter x1, waiting for transfers between devices: 5.51 us -> 0.01 us  [per_device(): reduced = lax.psum_scatter(terms, 'y', scatter_dimension=0, tiled=True)]
    all_to_all x1 -> x0, starting transfers between devices: 5.17 us -> none  [per_device(): lax.all_to_all(copies, 'x', 0, 0, tiled=True).reshape(row_count, cut)]
    all_to_all x1, waiting for transfers between devices: 7.51 us -> 10.1 us  [per_device(): pieces = lax.all_to_all(reduced, Z, 0, 0, tiled=True)]
  transfers between devices with their start and end apart: 11 -> 10, of which waited for: 9 -> 7; matrix products, arithmetic and copies ran while one was open for 8% -> 7% of each run, Pallas kernels for 3% -> 3%
where the time goes in v10:
time: 168 us; the launch traced here: 166 us
  waiting for transfers between devices  64.6 us (38%)
  blocking collectives  30.8 us (18%)
  starting transfers between devices  24.5 us (15%)
  Pallas kernels  15.8 us (9%)
  between operations  14.4 us (9%)
  other arithmetic  7.91 us (5%)
  local copies, waits for them, and re-layouts  5 us (3%)
  matrix products  2.96 us (2%)
    ppermute x6, waiting for transfers between devices, swapped(): return lax.ppermute(values, axis, [(0, 1), (1, 0)])  38.3 us
    all_to_all x1, blocking collectives, per_device(): block = lax.all_to_all(for_z, Z, 0, 0, tiled=True)  19 us
    ppermute x6, starting transfers between devices, swapped(): return lax.ppermute(values, axis, [(0, 1), (1, 0)])  13.6 us
    all_to_all x1, blocking collectives, per_device(): lax.all_to_all(copies, 'x', 0, 0, tiled=True).reshape(row_count, cut)  11.8 us
    all_to_all x1, waiting for transfers between devices, per_device(): pieces = lax.all_to_all(reduced, Z, 0, 0, tiled=True)  10.1 us
    pallas_call x1, Pallas kernels, early_pass(): pl.pallas_call(functools.partial(early_kernel, scale), out_shape=(jax.Sha...  9.43 us
    all_gather x1, waiting for transfers between devices, per_device(): weight = lax.all_gather(block, 'y').reshape(n_y, n_z, shard_rows, 2 * wide)  8.27 us
    all_to_all x1, waiting for transfers between devices, per_device(): lax.all_to_all(chip.reshape(2 * n_x, row_count // n_x, cut), ('zb', 'x'),...  7.85 us
  transfers between devices with their start and end apart: 10, of which 7 were waited for; matrix products, arithmetic and copies ran while one was open for 7% of the time, Pallas kernels for 3%

profile of v10, /device:TPU:6, one launch (start us, length us, event | category | flops | bytes accessed | tf_op | source)
XLA Modules:
  0.0 165.9 jit_solution(12817584392824661843)
XLA Ops:
  9.0 19.0 %all_to_all.20 = bf16[4,64,768]{2,1,0:T(8,128)(2,1)} all-to-all(bf16[4,64,768]{2,1,0:T(8,128)(2,1)S(1)} %pack_halves.1), channel_id=1, replica_groups=mesh['rep'=2,'zp'=2,'zb'=2,'y'=8,'x'=4,'c'=2] {'zp','zb'}, dimensions={0} | all-to-all | bytes 786432 | tf_op jit(solution)/shard_map/all_to_all | solution.py:350
  28.1 1.3 slice_select_fusion
  29.6 2.3 %collective-permute-start = (bf16[256,2048]{1,0:T(8,128)(2,1)S(1)}, bf16[256,2048]{1,0:T(8,128)(2,1)S(1)}, u32[]{:S(2)}, u32[]{:S(2)}) collective-permute-start(bf16[256,2048]{1,0:T(8,128)(2,1)S(1)} %pad_maximum_fusion), channel_id=1, source_target_pairs={{0,64},{64,0},{1,65},{65,1},{2,66},{66,2},{3,67},{67,3},{4,68},{68... | collective-permute-start | bytes 3145736 | tf_op jit(solution)/shard_map/ppermute | solution.py:23
  31.9 23.6 %collective-permute-done = bf16[256,2048]{1,0:T(8,128)(2,1)S(1)} collective-permute-done((bf16[256,2048]{1,0:T(8,128)(2,1)S(1)}, bf16[256,2048]{1,0:T(8,128)(2,1)S(1)}, u32[]{:S(2)}, u32[]{:S(2)}) %collective-permute-start) | collective-permute-done | bytes 1048608 | tf_op jit(solution)/shard_map/ppermute | solution.py:23
  55.4 1.9 %collective-permute-start.1 = (bf16[256,2048]{1,0:T(8,128)(2,1)S(1)}, bf16[256,2048]{1,0:T(8,128)(2,1)S(1)}, u32[]{:S(2)}, u32[]{:S(2)}) collective-permute-start(bf16[256,2048]{1,0:T(8,128)(2,1)S(1)} %collective-permute-done), channel_id=1, source_target_pairs={{0,1},{1,0},{2,3},{3,2},{4,5},{5,4},{6,7},{7,6},{8,9},{9,8},{10,11... | collective-permute-start | bytes 3145736 | tf_op jit(solution)/shard_map/ppermute | solution.py:23
  57.8 2.2 %collective-permute-start.2 = (bf16[256,384]{1,0:T(8,128)(2,1)S(1)}, bf16[256,384]{1,0:T(8,128)(2,1)S(1)}, u32[]{:S(2)}, u32[]{:S(2)}) collective-permute-start(bf16[256,384]{1,0:T(8,128)(2,1)S(1)} %get-tuple-element.55), channel_id=1, source_target_pairs={{0,64},{64,0},{1,65},{65,1},{2,66},{66,2},{3,67},{67,3},{4,68},{68... | collective-permute-start | bytes 589832 | tf_op jit(solution)/shard_map/ppermute | solution.py:23
  60.7 6.3 %collective-permute-done.2 = bf16[256,384]{1,0:T(8,128)(2,1)S(1)} collective-permute-done((bf16[256,384]{1,0:T(8,128)(2,1)S(1)}, bf16[256,384]{1,0:T(8,128)(2,1)S(1)}, u32[]{:S(2)}, u32[]{:S(2)}) %collective-permute-start.2) | collective-permute-done | bytes 196640 | tf_op jit(solution)/shard_map/ppermute | solution.py:23
  67.8 1.5 broadcast_select_fusion
  69.3 8.3 %all-gather.2.cloned.1.call-done = bf16[8,256,768]{2,1,0:T(8,128)(2,1)} async-done(((bf16[1,256,768]{2,1,0:T(8,128)(2,1)}), bf16[8,256,768]{2,1,0:T(8,128)(2,1)}) %all-gather.2.cloned.1.call-update) | async-done | bytes 3145744 | tf_op jit(solution)/shard_map/all_gather | solution.py:364
  77.6 9.4 %early_pass.1 = (bf16[4,8,64,768]{3,2,1,0:T(8,128)(2,1)}, bf16[512,768]{1,0:T(8,128)(2,1)}, bf16[8,4,72,768]{3,2,1,0:T(8,128)(2,1)}) custom-call(bf16[8,4,64,768]{3,2,1,0:T(8,128)(2,1)} %bitcast.24, bf16[256,2048]{1,0:T(8,128)(2,1)} %own_in.2, bf16[256,2048]{1,0:T(8,128)(2,1)} %get-tuple-element.51.low_in, bf16[256,2048]{1,0:T(8,128)(2,1)} %get-tuple-element.50.high_in, ...), custom_call_target="tpu_custom_call" | custom-call | flops 3221225472 | bytes 11534336 | tf_op jit(solution)/shard_map/early_pass/pallas_call | solution.py:158
  87.0 1.9 %copy-done.7 = bf16[4,8,64,768]{3,2,1,0:T(8,128)(2,1)S(1)} copy-done((bf16[4,8,64,768]{3,2,1,0:T(8,128)(2,1)S(1)}, bf16[4,8,64,768]{3,2,1,0:T(8,128)(2,1)}, u32[]{:S(2)}) %copy-start.7) | copy-done | bytes 3145752
  88.9 3.0 %convolution_convert_fusion = bf16[512,2048]{1,0:T(8,128)(2,1)S(1)} fusion(bf16[512,768]{1,0:T(8,128)(2,1)} %get-tuple-element.22, bf16[2048,768]{1,0:T(8,128)(2,1)S(1)} %bitcast.16), kind=kOutput, calls=%fused_computation | convolution fusion | flops 1611661312 | bytes 6029312 | tf_op jit(solution)/shard_map/dot_general | solution.py:372
  92.0 1.9 %collective-permute-start.3 = (bf16[512,1024]{1,0:T(8,128)(2,1)S(1)}, bf16[512,1024]{1,0:T(8,128)(2,1)S(1)}, u32[]{:S(2)}, u32[]{:S(2)}) collective-permute-start(bf16[512,1024]{1,0:T(8,128)(2,1)S(1)} %broadcast_select_fusion.2), channel_id=1, source_target_pairs={{0,1},{1,0},{2,3},{3,2},{4,5},{5,4},{6,7},{7,6},{8,9},{9,8},{10,11... | collective-permute-start | bytes 3145736 | tf_op jit(solution)/shard_map/ppermute | solution.py:23
  93.9 2.6 %collective-permute-done.3 = bf16[512,1024]{1,0:T(8,128)(2,1)S(1)} collective-permute-done((bf16[512,1024]{1,0:T(8,128)(2,1)S(1)}, bf16[512,1024]{1,0:T(8,128)(2,1)S(1)}, u32[]{:S(2)}, u32[]{:S(2)}) %collective-permute-start.3) | collective-permute-done | bytes 1048608 | tf_op jit(solution)/shard_map/ppermute | solution.py:23
  98.3 5.9 %all-to-all-start.1 = ((bf16[8,64,1024]{2,1,0:T(8,128)(2,1)}), bf16[8,64,1024]{2,1,0:T(8,128)(2,1)S(1)}, u32[]{:S(2)}, u32[]{:S(2)}) async-start(bf16[8,64,1024]{2,1,0:T(8,128)(2,1)} %bitcast.7), calls=%async_computation.1 | async-start | bytes 2097152 | tf_op jit(solution)/shard_map/all_to_all | solution.py:382
  104.2 5.5 %late_pass.1 = (bf16[256,384]{1,0:T(8,128)(2,1)}, bf16[256,384]{1,0:T(8,128)(2,1)}) custom-call(bf16[2048,768]{1,0:T(8,128)(2,1)} %bitcast.15, bf16[256,2048]{1,0:T(8,128)(2,1)} %own_in.3, bf16[256,2048]{1,0:T(8,128)(2,1)} %get-tuple-element.51.low_in, bf16[256,2048]{1,0:T(8,128)(2,1)} %get-tuple-element.50.high_in, f32[8,768]{1,0:T(8,128)} %fusion.3.filters_in), custom_call_target="tpu_custom_call" | custom-call | flops 1610612736 | bytes 5242880 | tf_op jit(solution)/shard_map/late_pass/pallas_call | solution.py:236
  109.7 7.8 %all-to-all-done.1 = bf16[8,64,1024]{2,1,0:T(8,128)(2,1)S(1)} async-done(((bf16[8,64,1024]{2,1,0:T(8,128)(2,1)}), bf16[8,64,1024]{2,1,0:T(8,128)(2,1)S(1)}, u32[]{:S(2)}, u32[]{:S(2)}) %all-to-all-start.1) | async-done | bytes 1048608 | tf_op jit(solution)/shard_map/all_to_all | solution.py:382
  117.8 11.8 %all_to_all.21 = bf16[4,64,1024]{2,1,0:T(8,128)(2,1)S(1)} all-to-all(bf16[4,64,1024]{2,1,0:T(8,128)(2,1)S(1)} %broadcast_in_dim.2), channel_id=1, replica_groups=mesh['rep'=2,'zp'=2,'zb'=2,'y'=8,'x'=4,'c'=2] {'x'}, dimensions={0} | all-to-all | bytes 1048576 | tf_op jit(solution)/shard_map/all_to_all | solution.py:391
  129.6 1.9 %collective-permute-start.4 = (bf16[256,1024]{1,0:T(8,128)(2,1)S(1)}, bf16[256,1024]{1,0:T(8,128)(2,1)S(1)}, u32[]{:S(2)}, u32[]{:S(2)}) collective-permute-start(bf16[256,1024]{1,0:T(8,128)(2,1)S(1)} %bitcast.17), channel_id=1, source_target_pairs={{0,1},{1,0},{2,3},{3,2},{4,5},{5,4},{6,7},{7,6},{8,9},{9,8},{10,11... | collective-permute-start | bytes 1572872 | tf_op jit(solution)/shard_map/ppermute | solution.py:23
  131.5 3.4 %collective-permute-start.5 = (bf16[256,384]{1,0:T(8,128)(2,1)S(1)}, bf16[256,384]{1,0:T(8,128)(2,1)S(1)}, u32[]{:S(2)}, u32[]{:S(2)}) collective-permute-start(bf16[256,384]{1,0:T(8,128)(2,1)S(1)} %copy-done.11), channel_id=1, source_target_pairs={{0,64},{64,0},{1,65},{65,1},{2,66},{66,2},{3,67},{67,3},{4,68},{68... | collective-permute-start | bytes 589832 | tf_op jit(solution)/shard_map/ppermute | solution.py:23
  135.0 5.8 %collective-permute-done.5 = bf16[256,384]{1,0:T(8,128)(2,1)S(1)} collective-permute-done((bf16[256,384]{1,0:T(8,128)(2,1)S(1)}, bf16[256,384]{1,0:T(8,128)(2,1)S(1)}, u32[]{:S(2)}, u32[]{:S(2)}) %collective-permute-start.5) | collective-permute-done | bytes 196640 | tf_op jit(solution)/shard_map/ppermute | solution.py:23
  140.7 4.9 %all-to-all-start.3 = ((bf16[4,72,768]{2,1,0:T(8,128)(2,1)}), bf16[4,72,768]{2,1,0:T(8,128)(2,1)S(1)}, u32[]{:S(2)}, u32[]{:S(2)}) async-start(bf16[4,72,768]{2,1,0:T(8,128)(2,1)} %bitcast.22), calls=%async_computation.4 | async-start | bytes 884736 | tf_op jit(solution)/shard_map/all_to_all | solution.py:398
  146.8 1.4 maximum_select_fusion
  148.1 10.1 %all-to-all-done.3.pieces = bf16[4,72,768]{2,1,0:T(8,128)(2,1)S(1)} async-done(((bf16[4,72,768]{2,1,0:T(8,128)(2,1)}), bf16[4,72,768]{2,1,0:T(8,128)(2,1)S(1)}, u32[]{:S(2)}, u32[]{:S(2)}) %all-to-all-start.3) | async-done | bytes 442400 | tf_op jit(solution)/shard_map/all_to_all | solution.py:398
  (57 shorter events, 7.9 us)
Async XLA Ops:
  7.2 70.4 %all-gather.2.cloned.1.call-start = ((), (), s32[]{:S(2)}) async-start(), calls=%async_computation.5 | async-start | bytes 3538944 | tf_op jit(solution)/shard_map/all_gather | solution.py:364
  9.0 19.1 %copy-start.6 = (bf16[256,2048]{1,0:T(8,128)(2,1)S(1)}, bf16[256,2048]{1,0:T(8,128)(2,1)}, u32[]{:S(2)}) copy-start(bf16[256,2048]{1,0:T(8,128)(2,1)} %own_in.3) | copy-start | bytes 3145732
  28.0 112.7 %reduce-scatter.2.cloned.1.call-start = ((), (), s32[]{:S(2)}) async-start(), calls=%async_computation.6 | async-start | bytes 3981312 | tf_op jit(solution)/shard_map/reduce_scatter | solution.py:370
  29.4 27.9 %slice-start = ((bf16[256,704]{0,1:T(8,128)(2,1)}), bf16[256,320]{0,1:T(8,128)(2,1)S(1)}, s32[]{:S(2)}) async-start(bf16[256,704]{0,1:T(8,128)(2,1)} %param.13), calls=%async_computation.7 | async-start | bytes 327680 | tf_op jit(solution)/shard_map/slice | solution.py:340
  29.4 28.1 %slice-start.1 = ((bf16[256,704]{0,1:T(8,128)(2,1)}), bf16[256,384]{0,1:T(8,128)(2,1)S(1)}, s32[]{:S(2)}) async-start(bf16[256,704]{0,1:T(8,128)(2,1)} %param.13), calls=%async_computation.8 | async-start | bytes 393216 | tf_op jit(solution)/shard_map/slice | solution.py:340
  29.4 30.6 %copy-start.9 = (bf16[3,704]{1,0:T(4,128)(2,1)S(1)}, bf16[3,704]{1,0:T(4,128)(2,1)}, u32[]{:S(2)}) copy-start(bf16[3,704]{1,0:T(4,128)(2,1)} %param.16) | copy-start | bytes 12676
  29.5 30.6 %slice-start.2 = ((bf16[3,704]{1,0:T(4,128)(2,1)}), bf16[3,320]{1,0:T(4,128)(2,1)S(1)}, s32[]{:S(2)}) async-start(bf16[3,704]{1,0:T(4,128)(2,1)} %param.16), calls=%async_computation.9 | async-start | bytes 6144 | tf_op jit(solution)/shard_map/slice | solution.py:340
  29.5 30.6 %copy-start.10 = (bf16[3,704]{1,0:T(4,128)(2,1)S(1)}, bf16[3,704]{1,0:T(4,128)(2,1)}, u32[]{:S(2)}) copy-start(bf16[3,704]{1,0:T(4,128)(2,1)} %param.17) | copy-start | bytes 12676
  29.5 30.6 %slice-start.3 = ((bf16[3,704]{1,0:T(4,128)(2,1)}), bf16[3,320]{1,0:T(4,128)(2,1)S(1)}, s32[]{:S(2)}) async-start(bf16[3,704]{1,0:T(4,128)(2,1)} %param.17), calls=%async_computation.10 | async-start | bytes 6144 | tf_op jit(solution)/shard_map/slice | solution.py:340
  29.6 25.8 %collective-permute-start = (bf16[256,2048]{1,0:T(8,128)(2,1)S(1)}, bf16[256,2048]{1,0:T(8,128)(2,1)S(1)}, u32[]{:S(2)}, u32[]{:S(2)}) collective-permute-start(bf16[256,2048]{1,0:T(8,128)(2,1)S(1)} %pad_maximum_fusion), channel_id=1, source_target_pairs={{0,64},{64,0},{1,65},{65,1},{2,66},{66,2},{3,67},{67,3},{4,68},{68... | collective-permute-start | bytes 3145736 | tf_op jit(solution)/shard_map/ppermute | solution.py:23
  55.4 12.4 %collective-permute-start.1 = (bf16[256,2048]{1,0:T(8,128)(2,1)S(1)}, bf16[256,2048]{1,0:T(8,128)(2,1)S(1)}, u32[]{:S(2)}, u32[]{:S(2)}) collective-permute-start(bf16[256,2048]{1,0:T(8,128)(2,1)S(1)} %collective-permute-done), channel_id=1, source_target_pairs={{0,1},{1,0},{2,3},{3,2},{4,5},{5,4},{6,7},{7,6},{8,9},{9,8},{10,11... | collective-permute-start | bytes 3145736 | tf_op jit(solution)/shard_map/ppermute | solution.py:23
  57.8 9.2 %collective-permute-start.2 = (bf16[256,384]{1,0:T(8,128)(2,1)S(1)}, bf16[256,384]{1,0:T(8,128)(2,1)S(1)}, u32[]{:S(2)}, u32[]{:S(2)}) collective-permute-start(bf16[256,384]{1,0:T(8,128)(2,1)S(1)} %get-tuple-element.55), channel_id=1, source_target_pairs={{0,64},{64,0},{1,65},{65,1},{2,66},{66,2},{3,67},{67,3},{4,68},{68... | collective-permute-start | bytes 589832 | tf_op jit(solution)/shard_map/ppermute | solution.py:23
  87.0 1.9 %copy-start.7 = (bf16[4,8,64,768]{3,2,1,0:T(8,128)(2,1)S(1)}, bf16[4,8,64,768]{3,2,1,0:T(8,128)(2,1)}, u32[]{:S(2)}) copy-start(bf16[4,8,64,768]{3,2,1,0:T(8,128)(2,1)} %get-tuple-element.23) | copy-start | bytes 9437188
  92.0 4.6 %collective-permute-start.3 = (bf16[512,1024]{1,0:T(8,128)(2,1)S(1)}, bf16[512,1024]{1,0:T(8,128)(2,1)S(1)}, u32[]{:S(2)}, u32[]{:S(2)}) collective-permute-start(bf16[512,1024]{1,0:T(8,128)(2,1)S(1)} %broadcast_select_fusion.2), channel_id=1, source_target_pairs={{0,1},{1,0},{2,3},{3,2},{4,5},{5,4},{6,7},{7,6},{8,9},{9,8},{10,11... | collective-permute-start | bytes 3145736 | tf_op jit(solution)/shard_map/ppermute | solution.py:23
  98.3 19.3 %all-to-all-start.1 = ((bf16[8,64,1024]{2,1,0:T(8,128)(2,1)}), bf16[8,64,1024]{2,1,0:T(8,128)(2,1)S(1)}, u32[]{:S(2)}, u32[]{:S(2)}) async-start(bf16[8,64,1024]{2,1,0:T(8,128)(2,1)} %bitcast.7), calls=%async_computation.1 | async-start | bytes 2097152 | tf_op jit(solution)/shard_map/all_to_all | solution.py:382
  109.7 21.8 %copy-start.11 = (bf16[256,384]{1,0:T(8,128)(2,1)S(1)}, bf16[256,384]{1,0:T(8,128)(2,1)}, u32[]{:S(2)}) copy-start(bf16[256,384]{1,0:T(8,128)(2,1)} %get-tuple-element.29) | copy-start | bytes 589828
  109.7 36.0 %copy-start.8 = (bf16[256,384]{1,0:T(8,128)(2,1)S(1)}, bf16[256,384]{1,0:T(8,128)(2,1)}, u32[]{:S(2)}) copy-start(bf16[256,384]{1,0:T(8,128)(2,1)} %get-tuple-element.26) | copy-start | bytes 589828
  129.6 11.1 %collective-permute-start.4 = (bf16[256,1024]{1,0:T(8,128)(2,1)S(1)}, bf16[256,1024]{1,0:T(8,128)(2,1)S(1)}, u32[]{:S(2)}, u32[]{:S(2)}) collective-permute-start(bf16[256,1024]{1,0:T(8,128)(2,1)S(1)} %bitcast.17), channel_id=1, source_target_pairs={{0,1},{1,0},{2,3},{3,2},{4,5},{5,4},{6,7},{7,6},{8,9},{9,8},{10,11... | collective-permute-start | bytes 1572872 | tf_op jit(solution)/shard_map/ppermute | solution.py:23
  131.5 9.2 %collective-permute-start.5 = (bf16[256,384]{1,0:T(8,128)(2,1)S(1)}, bf16[256,384]{1,0:T(8,128)(2,1)S(1)}, u32[]{:S(2)}, u32[]{:S(2)}) collective-permute-start(bf16[256,384]{1,0:T(8,128)(2,1)S(1)} %copy-done.11), channel_id=1, source_target_pairs={{0,64},{64,0},{1,65},{65,1},{2,66},{66,2},{3,67},{67,3},{4,68},{68... | collective-permute-start | bytes 589832 | tf_op jit(solution)/shard_map/ppermute | solution.py:23
  140.7 17.5 %all-to-all-start.3 = ((bf16[4,72,768]{2,1,0:T(8,128)(2,1)}), bf16[4,72,768]{2,1,0:T(8,128)(2,1)S(1)}, u32[]{:S(2)}, u32[]{:S(2)}) async-start(bf16[4,72,768]{2,1,0:T(8,128)(2,1)} %bitcast.22), calls=%async_computation.4 | async-start | bytes 884736 | tf_op jit(solution)/shard_map/all_to_all | solution.py:398
  145.7 12.5 %copy-start = (f32[64,704]{1,0:T(8,128)S(1)}, f32[64,704]{1,0:T(8,128)}, u32[]{:S(2)}) copy-start(f32[64,704]{1,0:T(8,128)} %gate.3) | copy-start | bytes 540676
  145.7 12.5 %copy-start.1 = (f32[64,704]{1,0:T(8,128)S(1)}, f32[64,704]{1,0:T(8,128)}, u32[]{:S(2)}) copy-start(f32[64,704]{1,0:T(8,128)} %up.3) | copy-start | bytes 540676
  145.7 12.5 %copy-start.4 = (f32[3,704]{1,0:T(4,128)S(1)}, f32[3,704]{1,0:T(4,128)}, u32[]{:S(2)}) copy-start(f32[3,704]{1,0:T(4,128)} %gate_taps.1) | copy-start | bytes 25348
  145.8 12.5 %copy-start.5 = (f32[3,704]{1,0:T(4,128)S(1)}, f32[3,704]{1,0:T(4,128)}, u32[]{:S(2)}) copy-start(f32[3,704]{1,0:T(4,128)} %up_taps.1) | copy-start | bytes 25348
  (2 other events, 1.8 us)
Sparse Core Ops, SparseCore 0:
  28.2 49.3 all-gather.1
  87.2 50.3 reduce-scatter.1
